TPU v7x, 128 devices: a whole 4x4x4 slice. The times are simulated.
128 devices in a mesh: sp: 16 (over z, y), tp: 8 (over x, core).
Axes of the slice: x: 4, y: 4, z: 4, core: 2. Of those that a mesh axis runs over, the one named last changes fastest.
Arguments:
- inputs: bfloat16 [16384, 4, 2048], P('sp'), may hold values from -6 to 6
- norm_gain: float32 [2048], replicated, may hold values from 0.1 to 1.9
- pool_proj: bfloat16 [2048, 1024], P(None, 'tp'), may hold values from -0.125 to 0.125
- pool_gate_proj: bfloat16 [2048, 1024], P(None, 'tp'), may hold values from -0.125 to 0.125
- pool_mix: bfloat16 [8, 128, 128], P('tp'), may hold values from -0.5 to 0.5
- query_proj: bfloat16 [2048, 1024], P(None, 'tp'), may hold values from -0.125 to 0.125
- key_proj: bfloat16 [2048, 512], P(None, 'tp'), may hold values from -0.125 to 0.125
- value_proj: bfloat16 [2048, 512], P(None, 'tp'), may hold values from -0.125 to 0.125
- attn_gate_proj: bfloat16 [2048, 1024], P(None, 'tp'), may hold values from -0.125 to 0.125
- query_gain: float32 [64], replicated, may hold values from 0.1 to 1.9
- key_gain: float32 [64], replicated, may hold values from 0.1 to 1.9
- sink_logit: float32 [16], P('tp'), may hold values from -12 to 240
- out_pool: bfloat16 [1024, 2048], P('sp'), may hold values from -0.125 to 0.125
- out_attn: bfloat16 [1024, 2048], P('sp'), may hold values from -0.125 to 0.125
Outputs:
- mixed_out: bfloat16 [16384, 4, 2048], P(('sp', 'tp'))
- log_weight_sum: float32 [16384, 4, 16], P('sp', None, 'tp')
All inputs are finite; a program needn't handle non-finite values.
Results may differ from a plain program's by a relative error of at most 0.015.
Values may be sent and summed in bfloat16 or wider, within the bound.
No kernel may reach another device: no remote copies, remote signals or barrier semaphores. Data moves between devices by JAX's collectives and lax.ppermute only.
A program may use at most 192 MiB of HBM per device.

v0:
```python
import math

import jax
import jax.numpy as jnp
from jax import lax
from jax.experimental import pallas as pl
from jax.experimental.pallas import tpu as pltpu
from jax.sharding import PartitionSpec as P

HEADS = 16
HEAD_DIM = 64
WINDOW = 128
REACH = 8
EPS = 1e-06
NEG = -1e30
LOG2E = math.log2(math.e)
F32 = jnp.float32
BF16 = jnp.bfloat16
BLOCK = 128


def row_scale(x):
    width = x.shape[1]
    acc = None
    for c in range(0, width, 128):
        part = x[:, c : c + 128].astype(F32)
        part = part * part
        acc = part if acc is None else acc + part
    total = jnp.sum(acc, axis=-1, keepdims=True)
    return lax.rsqrt(total * (1.0 / width) + EPS)


def silu(v):
    return v / (1.0 + jnp.exp(-v))


def edge_kernel(x_ref, w_ref, kv_ref, scr):
    half = x_ref.shape[0]
    x = x_ref.reshape(half * 4, x_ref.shape[2])[...]
    scale = row_scale(x)
    cols = jnp.dot(x, w_ref[...], preferred_element_type=F32) * scale
    scr[0] = cols[:, :128]
    scr[1] = cols[:, 128:]
    step = pl.program_id(0)
    for part in range(2):

        @pl.when(step % 2 == part)
        def _():
            for s in range(4):
                rows = scr[1, pl.ds(s, half, stride=4), :]
                kv_ref[0, s, part * half : (part + 1) * half, :] = rows.astype(BF16)

    @pl.when(step == 0)
    def _():
        for s in range(4):
            kv_ref[0, s, 128 : 128 + REACH, :] = scr[0, pl.ds(s, REACH, stride=4), :].astype(BF16)

    @pl.when(step == 3)
    def _():
        for s in range(4):
            tail = scr[0, pl.ds(s + 4 * (half - REACH), REACH, stride=4), :]
            kv_ref[0, s, 128 : 128 + REACH, :] = tail.astype(BF16)


def edges(x, w):
    half = 64
    last = x.shape[0] // half
    return pl.pallas_call(
        edge_kernel,
        grid=(4,),
        in_specs=[
            pl.BlockSpec((half, 4, x.shape[2]), lambda i: (i + (last - 4) * (i // 2), 0, 0)),
            pl.BlockSpec(w.shape, lambda i: (0, 0)),
        ],
        out_specs=pl.BlockSpec((1, 4, 136, 128), lambda i: (i // 2, 0, 0, 0)),
        out_shape=jax.ShapeDtypeStruct((2, 4, 136, 128), BF16),
        scratch_shapes=[pltpu.VMEM((2, half * 4, 128), F32)],
        compiler_params=pltpu.CompilerParams(dimension_semantics=("arbitrary",)),
        cost_estimate=pl.CostEstimate(flops=2 * 1024 * 2048 * 256, transcendentals=0, bytes_accessed=5 << 20),
        name="edge_rows",
    )(x, w)


def pool_kernel(ids, x_ref, w_ref, mix_ref, before_ref, after_ref, y_ref, pool, gate):
    step = pl.program_id(0)
    blocks = pl.num_programs(0) - 1
    rows = BLOCK * 4
    pad = 64
    total_rows = blocks * rows

    @pl.when(step == 0)
    def _():
        for s in range(4):
            pool[pl.ds(pad - 4 * REACH + s, REACH, stride=4), :] = before_ref[s, 128 : 128 + REACH, :].astype(F32)
            pool[pl.ds(pad + total_rows + s, REACH, stride=4), :] = after_ref[s, 128 : 128 + REACH, :].astype(F32)

    @pl.when(step < blocks)
    def _():
        x = x_ref.reshape(rows, x_ref.shape[2])[...]
        scale = row_scale(x)
        both = jnp.dot(x, w_ref[...], preferred_element_type=F32) * scale
        at = pl.multiple_of(step * rows, rows)
        pool[pl.ds(pad + at, rows), :] = both[:, :128]
        gate[pl.ds(at, rows), :] = both[:, 128:]

    @pl.when(step > 0)
    def _():
        at = pl.multiple_of((step - 1) * rows, rows)
        own = pool[pl.ds(pad + at, rows), :]
        sp, log_half, total_len = ids[0], ids[1], ids[2]
        position = sp * (blocks * BLOCK) + (step - 1) * BLOCK + lax.broadcasted_iota(jnp.int32, (rows, 128), 0) // 4

        def finish(half):
            window = pool[pl.ds(pad + at - 4 * REACH, rows + 8 * REACH), :]
            length = rows + 8 * REACH
            sums, width = window, 1
            while width < 2 * half:
                length -= 4 * width
                sums = sums[:length] + sums[4 * width : 4 * width + length]
                width *= 2
            begin = 4 * (REACH - half)
            window_sum = sums[begin : begin + rows]
            low = jnp.maximum(position - half, 0)
            high = jnp.minimum(position + half - 1, total_len - 1)
            count = (high - low + 1).astype(F32)
            pooled = (window_sum / count - own).astype(BF16)
            mixed = jnp.dot(pooled, mix_ref[0], preferred_element_type=F32)
            y_ref[0] = (mixed * silu(gate[pl.ds(at, rows), :])).astype(BF16)

        for k in range(4):

            @pl.when(log_half == k)
            def _(k=k):
                finish(2**k)


def pool_branch(ids, x, w, mix, before, after):
    length, _, width = x.shape
    blocks = length // BLOCK
    rows = BLOCK * 4
    return pl.pallas_call(
        pool_kernel,
        grid=(blocks + 1,),
        in_specs=[
            pl.BlockSpec(memory_space=pltpu.SMEM),
            pl.BlockSpec((BLOCK, 4, width), lambda i: (jnp.minimum(i, blocks - 1), 0, 0)),
            pl.BlockSpec(w.shape, lambda i: (0, 0)),
            pl.BlockSpec(mix.shape, lambda i: (0, 0, 0)),
            pl.BlockSpec(before.shape, lambda i: (0, 0, 0)),
            pl.BlockSpec(after.shape, lambda i: (0, 0, 0)),
        ],
        out_specs=pl.BlockSpec((1, rows, 128), lambda i: (jnp.maximum(i - 1, 0), 0, 0)),
        out_shape=jax.ShapeDtypeStruct((blocks, rows, 128), BF16),
        scratch_shapes=[
            pltpu.VMEM((length * 4 + 128, 128), F32),
            pltpu.VMEM((length * 4, 128), F32),
        ],
        compiler_params=pltpu.CompilerParams(dimension_semantics=("arbitrary",)),
        cost_estimate=pl.CostEstimate(flops=2 * 4096 * 2048 * 256, transcendentals=0, bytes_accessed=18 << 20),
        name="pool_branch",
    )(ids, x, w, mix, before, after)


def attn_kernel(ids, scal, x_ref, w_ref, gain_ref, before_ref, after_ref, y_ref, lse_ref, proj, qs, ks, vs, gate, bias, att):
    step = pl.program_id(0)
    blocks = pl.num_programs(0) - 1
    rows = BLOCK * 4
    lane = lax.broadcasted_iota(jnp.int32, (BLOCK, 128), 1)
    low_lanes = lane < HEAD_DIM

    @pl.when(step == 0)
    def _():
        query = lax.broadcasted_iota(jnp.int32, (BLOCK, 3 * BLOCK), 0)
        key = lax.broadcasted_iota(jnp.int32, (BLOCK, 3 * BLOCK), 1) - BLOCK
        distance = jnp.abs(query - key)
        for h in range(2):
            line = -scal[h] * distance.astype(F32) - scal[2 + h]
            bias[h * BLOCK : (h + 1) * BLOCK, :] = jnp.where(distance <= WINDOW, line, NEG)
        key_gain = gain_ref[:, 128:256]
        for side, ref in enumerate((before_ref, after_ref)):
            at = 0 if side == 0 else (blocks + 1) * BLOCK
            live = ids[3 + side].astype(F32)
            for s in range(4):
                kv = ref[s, 0:128, :].astype(F32)
                turned = pltpu.roll(kv, HEAD_DIM, 1)
                kk = jnp.where(low_lanes, kv, turned)
                vv = jnp.where(low_lanes, turned, kv)
                mean = jnp.sum(jnp.where(low_lanes, kv * kv, 0.0), axis=-1, keepdims=True) * (1.0 / HEAD_DIM)
                ks[s, at : at + BLOCK, :] = (kk * lax.rsqrt(mean + EPS) * key_gain).astype(BF16)
                vs[s, at : at + BLOCK, 0:128] = vv.astype(BF16)
                vs[s, at : at + BLOCK, 128:256] = jnp.full((BLOCK, 128), live, F32).astype(BF16)

    @pl.when(step < blocks)
    def _():
        x = x_ref.reshape(rows, x_ref.shape[2])[...]
        scale = row_scale(x)
        all_cols = jnp.dot(x, w_ref[...], preferred_element_type=F32) * scale
        qk = all_cols[:, :256]
        r = lax.broadcasted_iota(jnp.int32, (256, 256), 0) // HEAD_DIM
        c = lax.broadcasted_iota(jnp.int32, (256, 256), 1) // HEAD_DIM
        same = jnp.where(r == c, 1.0, 0.0).astype(BF16)
        squares = jnp.dot((qk * qk).astype(BF16), same, preferred_element_type=F32)
        normed = qk * lax.rsqrt(squares * (1.0 / HEAD_DIM) + EPS) * gain_ref[...]
        proj[0] = normed[:, :128]
        proj[1] = normed[:, 128:]
        proj[2] = all_cols[:, 256:384]
        at = pl.multiple_of(step * BLOCK, BLOCK)
        gate[pl.ds(pl.multiple_of(step * rows, rows), rows), :] = all_cols[:, 384:]
        for s in range(4):
            mine = pl.ds(s, BLOCK, stride=4)
            qs[s, pl.ds(at, BLOCK), :] = proj[0, mine, :].astype(BF16)
            ks[s, pl.ds(at + BLOCK, BLOCK), :] = proj[1, mine, :].astype(BF16)
            vs[s, pl.ds(at + BLOCK, BLOCK), 0:128] = proj[2, mine, :].astype(BF16)
            vs[s, pl.ds(at + BLOCK, BLOCK), 128:256] = jnp.ones((BLOCK, 128), BF16)

    @pl.when(step > 0)
    def _():
        at = pl.multiple_of((step - 1) * BLOCK, BLOCK)
        row_low = lax.broadcasted_iota(jnp.int32, (1, 128), 1) < HEAD_DIM
        sink_part = jnp.where(row_low, scal[4], scal[5])
        for s in range(4):
            q = qs[s, pl.ds(at, BLOCK), :]
            zero = jnp.zeros_like(q)
            two = jnp.concatenate([jnp.where(low_lanes, q, zero), jnp.where(low_lanes, zero, q)], axis=0)
            keys = ks[s, pl.ds(at, 3 * BLOCK), :]
            score = lax.dot_general(two, keys, (((1,), (1,)), ((), ())), preferred_element_type=F32)
            weight = jnp.exp2(score + bias[...]).astype(BF16)
            out = jnp.dot(weight, vs[s, pl.ds(at, 3 * BLOCK), :], preferred_element_type=F32)
            total = jnp.where(low_lanes, out[:BLOCK, 128:], out[BLOCK:, 128:]) + sink_part
            value = jnp.where(low_lanes, out[:BLOCK, :128], out[BLOCK:, :128])
            att[pl.ds(s, BLOCK, stride=4), :] = value / total
            turned = total.T
            lse_ref[s, 0:1, :] = jnp.log(turned[0:1, :]) + scal[6]
            lse_ref[s, 1:2, :] = jnp.log(turned[HEAD_DIM : HEAD_DIM + 1, :]) + scal[7]
        g = gate[pl.ds(pl.multiple_of((step - 1) * rows, rows), rows), :]
        y_ref[0] = (att[...] * silu(g)).astype(BF16)


def attn_branch(ids, scal, x, w, gain, before, after):
    length, _, width = x.shape
    blocks = length // BLOCK
    rows = BLOCK * 4
    return pl.pallas_call(
        attn_kernel,
        grid=(blocks + 1,),
        in_specs=[
            pl.BlockSpec(memory_space=pltpu.SMEM),
            pl.BlockSpec(memory_space=pltpu.SMEM),
            pl.BlockSpec((BLOCK, 4, width), lambda i: (jnp.minimum(i, blocks - 1), 0, 0)),
            pl.BlockSpec(w.shape, lambda i: (0, 0)),
            pl.BlockSpec(gain.shape, lambda i: (0, 0)),
            pl.BlockSpec(before.shape, lambda i: (0, 0, 0)),
            pl.BlockSpec(after.shape, lambda i: (0, 0, 0)),
        ],
        out_specs=(
            pl.BlockSpec((1, rows, 128), lambda i: (jnp.maximum(i - 1, 0), 0, 0)),
            pl.BlockSpec((4, 2, BLOCK), lambda i: (0, 0, jnp.maximum(i - 1, 0))),
        ),
        out_shape=(
            jax.ShapeDtypeStruct((blocks, rows, 128), BF16),
            jax.ShapeDtypeStruct((4, 2, length), F32),
        ),
        scratch_shapes=[
            pltpu.VMEM((3, rows, 128), F32),
            pltpu.VMEM((4, length, 128), BF16),
            pltpu.VMEM((4, length + 2 * BLOCK, 128), BF16),
            pltpu.VMEM((4, length + 2 * BLOCK, 256), BF16),
            pltpu.VMEM((length * 4, 128), F32),
            pltpu.VMEM((2 * BLOCK, 3 * BLOCK), F32),
            pltpu.VMEM((rows, 128), F32),
        ],
        compiler_params=pltpu.CompilerParams(dimension_semantics=("arbitrary",)),
        cost_estimate=pl.CostEstimate(flops=2 * 4096 * 2048 * 768, transcendentals=3 << 20, bytes_accessed=20 << 20),
        name="attn_branch",
    )(ids, scal, x, w, gain, before, after)


def out_kernel(yp_ref, ya_ref, wp_ref, wa_ref, o_ref):
    rows = yp_ref.shape[1]
    lanes_p = jnp.concatenate([yp_ref[j] for j in range(yp_ref.shape[0])], axis=1)
    lanes_a = jnp.concatenate([ya_ref[j] for j in range(ya_ref.shape[0])], axis=1)
    acc = jnp.dot(lanes_p, wp_ref[...], preferred_element_type=F32)
    acc = acc + jnp.dot(lanes_a, wa_ref[...], preferred_element_type=F32)
    o_ref.reshape(rows, o_ref.shape[2])[...] = acc.astype(BF16)


def out_matmul(y_pool, y_attn, w):
    parts, rows, cols = y_pool.shape
    width = w.shape[1] // 2
    tile = 512
    steps = width // tile
    return pl.pallas_call(
        out_kernel,
        grid=(steps,),
        in_specs=[
            pl.BlockSpec(y_pool.shape, lambda n: (0, 0, 0)),
            pl.BlockSpec(y_attn.shape, lambda n: (0, 0, 0)),
            pl.BlockSpec((parts * cols, tile), lambda n: (0, n)),
            pl.BlockSpec((parts * cols, tile), lambda n: (0, n + steps)),
        ],
        out_specs=pl.BlockSpec((rows // 4, 4, tile), lambda n: (0, 0, n)),
        out_shape=jax.ShapeDtypeStruct((rows // 4, 4, width), BF16),
        compiler_params=pltpu.CompilerParams(dimension_semantics=("arbitrary",)),
        cost_estimate=pl.CostEstimate(flops=2 * 512 * 2048 * 2048, transcendentals=0, bytes_accessed=12 << 20),
        name="out_matmul",
    )(y_pool, y_attn, w, w)


def body(
    inputs,
    norm_gain,
    pool_proj,
    pool_gate_proj,
    pool_mix,
    query_proj,
    key_proj,
    value_proj,
    attn_gate_proj,
    query_gain,
    key_gain,
    sink_logit,
    out_pool,
    out_attn,
):
    sp = lax.axis_index("sp")
    tp = lax.axis_index("tp")
    sp_size = lax.axis_size("sp")
    length = inputs.shape[0]
    out_w = lax.all_gather(jnp.concatenate([out_pool, out_attn], axis=1), "sp", axis=0, tiled=True)
    gain_col = norm_gain[:, None]

    def weighted(parts):
        return (jnp.concatenate(parts, axis=1).astype(F32) * gain_col).astype(BF16)

    w_edge = weighted([pool_proj, key_proj, value_proj])
    w_pool = weighted([pool_proj, pool_gate_proj])
    w_attn = weighted([query_proj, key_proj, key_proj, value_proj, value_proj, attn_gate_proj])
    gains = jnp.concatenate([query_gain * (LOG2E * HEAD_DIM**-0.5)] * 2 + [key_gain] * 2)[None, :]
    heads = tp * 2 + jnp.arange(2, dtype=jnp.int32)
    slopes = 2.0 ** (-8.0 * (heads + 1).astype(F32) / HEADS)
    shift = jnp.maximum(sink_logit, 0.0)
    scal = jnp.concatenate([slopes * LOG2E, shift * LOG2E, jnp.exp(sink_logit - shift), shift])
    ids = jnp.stack(
        [
            sp,
            tp % 4,
            jnp.int32(length * sp_size),
            (sp > 0).astype(jnp.int32),
            (sp < sp_size - 1).astype(jnp.int32),
        ]
    )
    edge = edges(inputs, w_edge)
    up = [(i, i + 1) for i in range(sp_size - 1)]
    down = [(j, i) for i, j in up]
    before = lax.ppermute(edge[1], "sp", up)
    after = lax.ppermute(edge[0], "sp", down)
    y_pool = pool_branch(ids, inputs, w_pool, pool_mix, before, after)
    pool_rows = lax.all_to_all(y_pool, "tp", split_axis=0, concat_axis=0, tiled=True)
    y_attn, lse = attn_branch(ids, scal, inputs, w_attn, gains, before, after)
    attn_rows = lax.all_to_all(y_attn, "tp", split_axis=0, concat_axis=0, tiled=True)
    mixed = out_matmul(pool_rows, attn_rows, out_w)
    return mixed, jnp.transpose(lse, (2, 0, 1))


def solution(mesh):
    placed = (
        P("sp", None, None),
        P(),
        P(None, "tp"),
        P(None, "tp"),
        P("tp", None, None),
        P(None, "tp"),
        P(None, "tp"),
        P(None, "tp"),
        P(None, "tp"),
        P(),
        P(),
        P("tp"),
        P("sp", None),
        P("sp", None),
    )
    return jax.shard_map(
        body,
        mesh=mesh,
        in_specs=placed,
        out_specs=(P(("sp", "tp"), None, None), P("sp", None, "tp")),
        check_vma=False,
    )
```

profile of v0, /device:TPU:96, one launch (start us, length us, event | category | flops | bytes accessed | tf_op | source)
XLA Modules:
  0.0 120.3 jit_solution(3485420369876877216)
XLA Ops:
  7.2 0.0 copy-start.3
  7.2 0.0 copy-start.4
  7.2 0.0 copy-start.1
  7.2 0.0 copy-start.2
  7.2 0.0 all-gather.2.cloned.1.call-start
  7.3 1.9 %pad_maximum_fusion.2 = bf16[64,4096]{1,0:T(8,128)(2,1)} fusion(bf16[64,2048]{1,0:T(8,128)(2,1)} %param.27, bf16[64,2048]{1,0:T(8,128)(2,1)} %param.26), kind=kLoop, calls=%fused_computation.6 | loop fusion | flops 1048576 | bytes 1048576 | tf_op jit(solution)/shard_map/concatenate | solution.py:329
  9.2 0.0 all-gather.2.cloned.1.call-update
  9.2 1.2 %copy.16 = bf16[2048,64]{1,0:T(8,128)(2,1)S(1)} copy(bf16[2048,64]{0,1:T(8,128)(2,1)} %param.20) | data formatting | bytes 524288 | tf_op args[6]
  10.5 0.0 copy-done.3
  10.5 0.3 copy.17
  10.7 0.0 copy-done.4
  10.8 0.0 copy-done.1
  10.8 0.0 copy-done.2
  10.8 1.7 %multiply_convert_fusion.1 = (bf16[2048,256]{1,0:T(8,128)(2,1)}, bf16[2048,256]{1,0:T(8,128)(2,1)}) fusion(bf16[2048,128]{1,0:T(8,128)(2,1)S(1)} %copy-done.1, bf16[2048,64]{1,0:T(8,128)(2,1)S(1)} %copy.17, bf16[2048,64]{1,0:T(8,128)(2,1)S(1)} %copy.16, f32[2048]{0:T(1024)S(1)} %copy-done.4, bf16[2048,128]{1,0:T(8,128)(2,1)S(1)} %copy-done.2), kind=kLoop, calls=%fused_computation.1 | loop fusion | flops 6815744 | bytes 3678208 | tf_op jit(solution)/shard_map/convert_element_type | solution.py:333
  12.5 5.9 %edge_rows.1 = bf16[2,4,136,128]{3,2,1,0:T(8,128)(2,1)} custom-call(bf16[1024,4,2048]{2,1,0:T(4,128)(2,1)} %x_ref.5, bf16[2048,256]{1,0:T(8,128)(2,1)} %get-tuple-element.6.w_ref), custom_call_target="tpu_custom_call" | custom-call | flops 1073741824 | bytes 5242880 | tf_op jit(solution)/shard_map/edge_rows/pallas_call | solution.py:68
  18.4 1.0 slice_bitcast_fusion
  19.4 3.5 %collective-permute-start = (bf16[4,136,128]{2,1,0:T(8,128)(2,1)S(1)}, bf16[4,136,128]{2,1,0:T(8,128)(2,1)}, u32[]{:S(2)}, u32[]{:S(2)}) collective-permute-start(bf16[4,136,128]{2,1,0:T(8,128)(2,1)S(1)} %get-tuple-element.9), channel_id=1, source_target_pairs={{0,8},{8,16},{16,24},{24,32},{32,40},{40,48},{48,56},{56,64},{64,7... | collective-permute-start | bytes 417800 | tf_op jit(solution)/shard_map/ppermute | solution.py:355
  22.9 4.5 %collective-permute-start.1 = (bf16[4,136,128]{2,1,0:T(8,128)(2,1)S(1)}, bf16[4,136,128]{2,1,0:T(8,128)(2,1)}, u32[]{:S(2)}, u32[]{:S(2)}) collective-permute-start(bf16[4,136,128]{2,1,0:T(8,128)(2,1)S(1)} %get-tuple-element.8), channel_id=1, source_target_pairs={{8,0},{16,8},{24,16},{32,24},{40,32},{48,40},{56,48},{64,56},{72,6... | collective-permute-start | bytes 417800 | tf_op jit(solution)/shard_map/ppermute | solution.py:356
  27.4 0.0 copy-start.7
  27.4 0.0 copy-start.5
  27.4 5.0 %concatenate.21 = bf16[2048,512]{1,0:T(8,128)(2,1)S(1)} concatenate(bf16[2048,128]{1,0:T(8,128)(2,1)} %param.19, bf16[2048,64]{1,0:T(8,128)(2,1)S(1)} %copy.16, bf16[2048,64]{1,0:T(8,128)(2,1)S(1)} %copy.16, bf16[2048,64]{1,0:T(8,128)(2,1)S(1)} %copy.17, bf16[2048,64]{1,0:T(8,128)(2,1)S(1)} %copy.17, bf16[2048,128]{1,0:T(8,128)(2,1)} %param.22), dimensions={1} | concatenate | bytes 4194304 | tf_op jit(solution)/shard_map/concatenate | solution.py:333
  32.4 0.0 copy-done.7
  32.4 0.0 copy-done.5
  32.5 0.0 copy-start.6
  32.5 1.8 %multiply_convert_fusion.w_ref = bf16[2048,512]{1,0:T(8,128)(2,1)} fusion(bf16[2048,512]{1,0:T(8,128)(2,1)S(1)} %concatenate.21, f32[2048]{0:T(1024)S(1)} %copy-done.4), kind=kLoop, calls=%fused_computation | loop fusion | flops 3145728 | bytes 4202496 | tf_op jit(solution)/shard_map/convert_element_type | solution.py:333
  34.3 0.6 pad_maximum_fusion.4.scal
  34.9 0.6 stack.27.ids
  35.4 0.0 copy-done.6
  35.4 0.6 pad_maximum_fusion.3
  36.1 0.0 collective-permute-done.before_ref
  36.1 0.0 collective-permute-done.1.after_ref
  36.1 26.8 %attn_branch.1 = (bf16[8,512,128]{2,1,0:T(8,128)(2,1)}, f32[4,2,1024]{2,1,0:T(2,128)}) custom-call(s32[5]{0:T(128)} %stack.27.ids, f32[8]{0:T(128)} %pad_maximum_fusion.4.scal, bf16[1024,4,2048]{2,1,0:T(4,128)(2,1)} %x_ref.5, bf16[2048,512]{1,0:T(8,128)(2,1)} %multiply_convert_fusion.w_ref, f32[1,256]{1,0:T(1,128)} %bitcast.10, ...), custom_call_target="tpu_custom_call" | custom-call | flops 12884901888 | bytes 20971520 | tf_op jit(solution)/shard_map/attn_branch/pallas_call | solution.py:243
  62.8 4.3 %all-to-all-start.1 = ((bf16[8,512,128]{2,1,0:T(8,128)(2,1)}), bf16[8,512,128]{2,1,0:T(8,128)(2,1)S(1)}, u32[]{:S(2)}, u32[]{:S(2)}) async-start(bf16[8,512,128]{2,1,0:T(8,128)(2,1)} %get-tuple-element.4), calls=%async_computation.1 | async-start | bytes 2097152 | tf_op jit(solution)/shard_map/all_to_all | solution.py:360
  67.1 16.7 %pool_branch.1 = bf16[8,512,128]{2,1,0:T(8,128)(2,1)} custom-call(s32[5]{0:T(128)} %stack.27.ids, bf16[1024,4,2048]{2,1,0:T(4,128)(2,1)} %x_ref.5, bf16[2048,256]{1,0:T(8,128)(2,1)} %get-tuple-element.7.w_ref, bf16[1,128,128]{2,1,0:T(8,128)(2,1)} %mix_ref.1, bf16[4,136,128]{2,1,0:T(8,128)(2,1)} %collective-permute-done.before_ref, ...), custom_call_target="tpu_custom_call" | custom-call | flops 4294967296 | bytes 18874368 | tf_op jit(solution)/shard_map/pool_branch/pallas_call | solution.py:141
  83.8 0.0 all-to-all-done.1.ya_ref
  83.8 0.0 copy-start
  83.9 20.9 %all_to_all.10.yp_ref = bf16[8,512,128]{2,1,0:T(8,128)(2,1)} all-to-all(bf16[8,512,128]{2,1,0:T(8,128)(2,1)} %pool_branch.1), channel_id=1, replica_groups=mesh['sp'=16,'tp'=8] {'tp'}, dimensions={0} | all-to-all | bytes 2097152 | tf_op jit(solution)/shard_map/all_to_all | solution.py:358
  104.8 0.0 all-gather.2.cloned.1.call-done.wp_ref.wa_ref
  104.8 0.0 copy-done
  104.8 8.6 %out_matmul.1 = bf16[128,4,2048]{2,1,0:T(4,128)(2,1)} custom-call(bf16[8,512,128]{2,1,0:T(8,128)(2,1)} %all_to_all.10.yp_ref, bf16[8,512,128]{2,1,0:T(8,128)(2,1)} %copy-done, bf16[1024,4096]{1,0:T(8,128)(2,1)} %all-gather.2.cloned.1.call-done.wp_ref.wa_ref, bf16[1024,4096]{1,0:T(8,128)(2,1)} %all-gather.2.cloned.1.call-done.wp_ref.wa_ref), custom_call_target="tpu_custom_call" | custom-call | flops 4294967296 | bytes 12582912 | tf_op jit(solution)/shard_map/out_matmul/pallas_call | solution.py:292
  (3 shorter events, 0.0 us)
Async XLA Ops:
  7.2 3.3 %copy-start.3 = (bf16[2048,64]{0,1:T(8,128)(2,1)S(1)}, bf16[2048,64]{0,1:T(8,128)(2,1)}, u32[]{:S(2)}) copy-start(bf16[2048,64]{0,1:T(8,128)(2,1)} %param.21) | copy-start | bytes 786436
  7.2 3.6 %copy-start.4 = (f32[2048]{0:T(1024)S(1)}, f32[2048]{0:T(1024)}, u32[]{:S(2)}) copy-start(f32[2048]{0:T(1024)} %param.15) | copy-start | bytes 24580
  7.2 3.6 %copy-start.1 = (bf16[2048,128]{1,0:T(8,128)(2,1)S(1)}, bf16[2048,128]{1,0:T(8,128)(2,1)}, u32[]{:S(2)}) copy-start(bf16[2048,128]{1,0:T(8,128)(2,1)} %param.16) | copy-start | bytes 1572868
  7.2 3.6 %copy-start.2 = (bf16[2048,128]{1,0:T(8,128)(2,1)S(1)}, bf16[2048,128]{1,0:T(8,128)(2,1)}, u32[]{:S(2)}) copy-start(bf16[2048,128]{1,0:T(8,128)(2,1)} %param.17) | copy-start | bytes 1572868
  7.2 97.6 %all-gather.2.cloned.1.call-start = ((), (), s32[]{:S(2)}) async-start(), calls=%async_computation.2 | async-start | bytes 8912896 | tf_op jit(solution)/shard_map/all_gather | solution.py:329
  19.4 16.7 %collective-permute-start = (bf16[4,136,128]{2,1,0:T(8,128)(2,1)S(1)}, bf16[4,136,128]{2,1,0:T(8,128)(2,1)}, u32[]{:S(2)}, u32[]{:S(2)}) collective-permute-start(bf16[4,136,128]{2,1,0:T(8,128)(2,1)S(1)} %get-tuple-element.9), channel_id=1, source_target_pairs={{0,8},{8,16},{16,24},{24,32},{32,40},{40,48},{48,56},{56,64},{64,7... | collective-permute-start | bytes 417800 | tf_op jit(solution)/shard_map/ppermute | solution.py:355
  22.9 13.2 %collective-permute-start.1 = (bf16[4,136,128]{2,1,0:T(8,128)(2,1)S(1)}, bf16[4,136,128]{2,1,0:T(8,128)(2,1)}, u32[]{:S(2)}, u32[]{:S(2)}) collective-permute-start(bf16[4,136,128]{2,1,0:T(8,128)(2,1)S(1)} %get-tuple-element.8), channel_id=1, source_target_pairs={{8,0},{16,8},{24,16},{32,24},{40,32},{48,40},{56,48},{64,56},{72,6... | collective-permute-start | bytes 417800 | tf_op jit(solution)/shard_map/ppermute | solution.py:356
  27.4 5.1 %copy-start.7 = (f32[64]{0:T(128)S(1)}, f32[64]{0:T(128)}, u32[]{:S(2)}) copy-start(f32[64]{0:T(128)} %param.23) | copy-start | bytes 772
  27.4 5.1 %copy-start.5 = (f32[2]{0:T(128)S(1)}, f32[2]{0:T(128)}, u32[]{:S(2)}) copy-start(f32[2]{0:T(128)} %param.25) | copy-start | bytes 28
  32.5 3.0 %copy-start.6 = (f32[64]{0:T(128)S(1)}, f32[64]{0:T(128)}, u32[]{:S(2)}) copy-start(f32[64]{0:T(128)} %param.24) | copy-start | bytes 772
  62.8 21.0 %all-to-all-start.1 = ((bf16[8,512,128]{2,1,0:T(8,128)(2,1)}), bf16[8,512,128]{2,1,0:T(8,128)(2,1)S(1)}, u32[]{:S(2)}, u32[]{:S(2)}) async-start(bf16[8,512,128]{2,1,0:T(8,128)(2,1)} %get-tuple-element.4), calls=%async_computation.1 | async-start | bytes 2097152 | tf_op jit(solution)/shard_map/all_to_all | solution.py:360
  83.8 20.9 %copy-start = (bf16[8,512,128]{2,1,0:T(8,128)(2,1)}, bf16[8,512,128]{2,1,0:T(8,128)(2,1)S(1)}, u32[]{:S(2)}) copy-start(bf16[8,512,128]{2,1,0:T(8,128)(2,1)S(1)} %all-to-all-done.1.ya_ref) | copy-start | bytes 3145732
Sparse Core Ops, SparseCore 0:
  10.2 74.1 all-gather.1
where the time goes:
time: 121 us; the launch traced here: 120 us
  Pallas kernels  58 us (48%)
  blocking collectives  20.9 us (17%)
  between operations  14.2 us (12%)
  starting transfers between devices  12.3 us (10%)
  local copies, waits for them, and re-layouts  8.13 us (7%)
  other arithmetic  6.72 us (6%)
    pallas_call x1, Pallas kernels, attn_branch(): pl.pallas_call(attn_kernel, grid=(blocks + 1,), in_specs=[pl.BlockSpec(me...  26.8 us
    all_to_all x1, blocking collectives, body(): lax.all_to_all(y_pool, 'tp', split_axis=0, concat_axis=0, tiled=True)  20.9 us
    pallas_call x1, Pallas kernels, pool_branch(): pl.pallas_call(pool_kernel, grid=(blocks + 1,), in_specs=[pl.BlockSpec(me...  16.7 us
    pallas_call x1, Pallas kernels, out_matmul(): pl.pallas_call(out_kernel, grid=(steps,), in_specs=[pl.BlockSpec(y_pool.s...  8.65 us
    pallas_call x1, Pallas kernels, edges(): pl.pallas_call(edge_kernel, grid=(4,), in_specs=[pl.BlockSpec((half, 4, x...  5.86 us
    concatenate x1, local copies, waits for them, and re-layouts, weighted(): return (jnp.concatenate(parts, axis=1).astype(F32) * gain_col).astype(BF16)  5.03 us
    ppermute x1, starting transfers between devices, body(): after = lax.ppermute(edge[0], 'sp', down)  4.47 us
    all_to_all x1, starting transfers between devices, body(): lax.all_to_all(y_attn, 'tp', split_axis=0, concat_axis=0, tiled=True)  4.3 us
  transfers between devices with their start and end apart: 4, of which 0 were waited for; matrix products, arithmetic and copies ran while one was open for 11% of the time, Pallas kernels for 41%

commit v1 on v0

v1 whole, which is shorter than its diff:
```python
import functools
import math

import jax
import jax.numpy as jnp
from jax import lax
from jax.experimental import pallas as pl
from jax.experimental.pallas import tpu as pltpu
from jax.sharding import PartitionSpec as P


HEAD_DIM = 64
WINDOW = 128
REACH = 8
EPS = 1e-06
NEG = -1e30
LOG2E = math.log2(math.e)
F32 = jnp.float32
BF16 = jnp.bfloat16
BLOCK = 128


def row_scale(x):
    width = x.shape[1]
    acc = None
    for c in range(0, width, 512):
        parts = [x[:, c + d : c + d + 128] for d in range(0, 512, 128)]
        parts = [p * p for p in parts]
        four = ((parts[0] + parts[1]) + (parts[2] + parts[3])).astype(F32)
        acc = four if acc is None else acc + four
    total = jnp.sum(acc, axis=-1, keepdims=True)
    return lax.rsqrt(total * (1.0 / width) + EPS)


def silu(v):
    return v / (1.0 + jnp.exp(-v))


def first_kernel(
    x_ref, gain_ref, pool_ref, pgate_ref, query_ref, keyt_ref, valuet_ref, agate_ref,
    head_ref, tail_ref, wp_ref, wa_ref, w_edge, scr, xs,
):
    half = x_ref.shape[0]
    step = pl.program_id(0)

    @pl.when(step == 0)
    def _():
        low = lax.broadcasted_iota(jnp.int32, (128, 128), 1) < HEAD_DIM
        for c in range(0, x_ref.shape[2], 128):
            rows = slice(c, c + 128)
            line = gain_ref[:, rows]
            column = jnp.broadcast_to(line, (128, 128)).T
            pool = (pool_ref[rows, :].astype(F32) * column).astype(BF16)
            wp_ref[rows, 0:128] = pool
            wp_ref[rows, 128:256] = (pgate_ref[rows, :].astype(F32) * column).astype(BF16)
            kv = (jnp.concatenate([keyt_ref[:, rows], valuet_ref[:, rows]], axis=0).astype(F32) * line).T
            turned = pltpu.roll(kv, HEAD_DIM, 1)
            wa_ref[rows, 0:128] = (query_ref[rows, :].astype(F32) * column).astype(BF16)
            wa_ref[rows, 128:256] = jnp.where(low, kv, turned).astype(BF16)
            wa_ref[rows, 256:384] = jnp.where(low, turned, kv).astype(BF16)
            wa_ref[rows, 384:512] = (agate_ref[rows, :].astype(F32) * column).astype(BF16)
            w_edge[rows, 0:128] = pool
            w_edge[rows, 128:256] = kv.astype(BF16)

    xs[...] = x_ref.reshape(half * 4, x_ref.shape[2])[...]
    x = xs[...]
    cols = jnp.dot(x, w_edge[...], preferred_element_type=F32) * row_scale(x)
    scr[0] = cols[:, :128]
    scr[1] = cols[:, 128:]
    for n in range(4):
        out = head_ref if n < 2 else tail_ref
        part = n % 2

        @pl.when(step == n)
        def _(n=n, out=out, part=part):
            for s in range(4):
                rows = scr[1, pl.ds(s, half, stride=4), :]
                out[s, part * half : (part + 1) * half, :] = rows.astype(BF16)
                if n == 0:
                    out[s, 128 : 128 + REACH, :] = scr[0, pl.ds(s, REACH, stride=4), :].astype(BF16)
                if n == 3:
                    rows = scr[0, pl.ds(s + 4 * (half - REACH), REACH, stride=4), :]
                    out[s, 128 : 128 + REACH, :] = rows.astype(BF16)


def first_rows(x, gain, pool, pgate, query, keyt, valuet, agate):
    half = 64
    width = x.shape[2]
    last = x.shape[0] // half
    whole = [gain, pool, pgate, query, keyt, valuet, agate]
    return pl.pallas_call(
        first_kernel,
        grid=(4,),
        in_specs=[pl.BlockSpec((half, 4, width), lambda i: (i + (last - 4) * (i // 2), 0, 0))]
        + [pl.BlockSpec(a.shape, lambda i: (0, 0)) for a in whole],
        out_specs=(
            pl.BlockSpec((4, 136, 128), lambda i: (0, 0, 0)),
            pl.BlockSpec((4, 136, 128), lambda i: (0, 0, 0)),
            pl.BlockSpec((width, 256), lambda i: (0, 0)),
            pl.BlockSpec((width, 512), lambda i: (0, 0)),
        ),
        out_shape=(
            jax.ShapeDtypeStruct((4, 136, 128), BF16),
            jax.ShapeDtypeStruct((4, 136, 128), BF16),
            jax.ShapeDtypeStruct((width, 256), BF16),
            jax.ShapeDtypeStruct((width, 512), BF16),
        ),
        scratch_shapes=[
            pltpu.VMEM((width, 256), BF16),
            pltpu.VMEM((2, half * 4, 128), F32),
            pltpu.VMEM((half * 4, width), BF16),
        ],
        compiler_params=pltpu.CompilerParams(dimension_semantics=("arbitrary",)),
        cost_estimate=pl.CostEstimate(flops=2 * 1024 * 2048 * 256, transcendentals=0, bytes_accessed=12 << 20),
        name="first_rows",
    )(x, *whole)


def pool_kernel(x_ref, w_ref, mix_ref, before_ref, after_ref, y_ref, pool, gate, inverse, xs, xv, sems):
    step = pl.program_id(0)
    blocks = pl.num_programs(0) - 1
    rows = BLOCK * 4
    pad = 64
    total_rows = blocks * rows
    length_blocks = xv.shape[0] // BLOCK
    power = lax.axis_index("tp") % 4
    half = jnp.left_shift(jnp.int32(1), power)

    def fetch(n):
        span = pl.ds(n * BLOCK, BLOCK)
        return pltpu.make_async_copy(x_ref.at[span], xv.at[span], sems.at[n])

    @pl.when(step == 0)
    def _():
        for n in range(length_blocks):
            fetch(n).start()
        for s in range(4):
            pool[pl.ds(pad - 4 * REACH + s, REACH, stride=4), :] = before_ref[s, 128 : 128 + REACH, :].astype(F32)
            pool[pl.ds(pad + total_rows + s, REACH, stride=4), :] = after_ref[s, 128 : 128 + REACH, :].astype(F32)
        length = blocks * BLOCK
        begin = lax.axis_index("sp") * length
        total = lax.axis_size("sp") * length
        for k in range(3):
            where = (0, BLOCK, length - BLOCK)[k]
            position = begin + where + lax.broadcasted_iota(jnp.int32, (rows, 128), 0) // 4
            count = jnp.minimum(position + half - 1, total - 1) - jnp.maximum(position - half, 0) + 1
            inverse[k] = 1.0 / count.astype(F32)

    def finish():
        at = pl.multiple_of((step - 1) * rows, rows)
        base = pad + at
        reach = 4 * REACH
        window = pool[pl.ds(base - reach, rows + 2 * reach), :]
        size = rows + 2 * reach - 8
        two = window[:size] + window[4 : size + 4]
        four = two[: size - 8] + two[8:]
        eight = four[: size - 24] + four[16 : size - 8]
        sixteen = eight[: size - 56] + eight[32 : size - 24]
        sums = jnp.where(
            power == 0,
            two[reach - 4 : reach - 4 + rows],
            jnp.where(
                power == 1,
                four[reach - 8 : reach - 8 + rows],
                jnp.where(power == 2, eight[reach - 16 : reach - 16 + rows], sixteen[:rows]),
            ),
        )
        kind = jnp.where(step == 1, 0, jnp.where(step == blocks, 2, 1))
        pooled = (sums * inverse[kind] - window[reach : reach + rows]).astype(BF16)
        mixed = jnp.dot(pooled, mix_ref[0], preferred_element_type=F32)
        y_ref[0] = (mixed * silu(gate[pl.ds(at, rows), :])).astype(BF16)

    def project():
        fetch(step).wait()
        xs[...] = xv.at[pl.ds(pl.multiple_of(step * BLOCK, BLOCK), BLOCK)].reshape(rows, xv.shape[2])[...]
        x = xs[...]
        both = jnp.dot(x, w_ref[...], preferred_element_type=F32) * row_scale(x)
        at = pl.multiple_of(step * rows, rows)
        pool[pl.ds(pad + at, rows), :] = both[:, :128]
        gate[pl.ds(at, rows), :] = both[:, 128:]

    @pl.when(step == 0)
    def _():
        project()

    @pl.when((step > 0) & (step < blocks))
    def _():
        project()
        finish()

    @pl.when(step == blocks)
    def _():
        finish()


def pool_branch(x, w, mix, before, after):
    length, _, width = x.shape
    blocks = length // BLOCK
    rows = BLOCK * 4
    return pl.pallas_call(
        pool_kernel,
        grid=(blocks + 1,),
        in_specs=[
            pl.BlockSpec(memory_space=pl.ANY),
            pl.BlockSpec(w.shape, lambda i: (0, 0)),
            pl.BlockSpec(mix.shape, lambda i: (0, 0, 0)),
            pl.BlockSpec(before.shape, lambda i: (0, 0, 0)),
            pl.BlockSpec(after.shape, lambda i: (0, 0, 0)),
        ],
        out_specs=pl.BlockSpec((1, rows, 128), lambda i: (jnp.maximum(i - 1, 0), 0, 0)),
        out_shape=jax.ShapeDtypeStruct((blocks, rows, 128), BF16),
        scratch_shapes=[
            pltpu.VMEM((length * 4 + 128, 128), F32),
            pltpu.VMEM((length * 4, 128), F32),
            pltpu.VMEM((3, rows, 128), F32),
            pltpu.VMEM((rows, width), BF16),
            pltpu.VMEM(x.shape, BF16),
            pltpu.SemaphoreType.DMA((blocks,)),
        ],
        compiler_params=pltpu.CompilerParams(dimension_semantics=("arbitrary",)),
        cost_estimate=pl.CostEstimate(flops=2 * 4096 * 2048 * 256, transcendentals=0, bytes_accessed=18 << 20),
        name="pool_branch",
    )(x, w, mix, before, after)


def attn_kernel(
    sink_ref, x_ref, w_ref, qgain_ref, kgain_ref, before_ref, after_ref, first_ref,
    y_ref, lse_ref, proj, qs, ks, vs, gate, bias, att, xs, sinks, gains,
):
    del first_ref
    step = pl.program_id(0)
    blocks = pl.num_programs(0) - 1
    rows = BLOCK * 4
    lane = lax.broadcasted_iota(jnp.int32, (BLOCK, 128), 1)
    low_lanes = lane < HEAD_DIM
    shifts = [jnp.maximum(sink_ref[h], 0.0) for h in range(2)]

    @pl.when(step == 0)
    def _():
        query = lax.broadcasted_iota(jnp.int32, (BLOCK, 3 * BLOCK), 0)
        key = lax.broadcasted_iota(jnp.int32, (BLOCK, 3 * BLOCK), 1) - BLOCK
        distance = jnp.abs(query - key)
        scale = lax.broadcasted_iota(jnp.int32, (BLOCK, 3 * BLOCK), 0) * 0 + jnp.left_shift(
            jnp.int32(1), lax.axis_index("tp")
        )
        for h in range(2):
            slope = ((0.5**0.5, 0.5)[h] * LOG2E) / scale.astype(F32)
            line = -slope * distance.astype(F32) - shifts[h] * LOG2E
            bias[h * BLOCK : (h + 1) * BLOCK, :] = jnp.where(distance <= WINDOW, line, NEG)
        shift_row = jnp.where(low_lanes, shifts[0], shifts[1])
        sink_row = jnp.where(low_lanes, sink_ref[0], sink_ref[1])
        sinks[...] = jnp.exp(sink_row - shift_row)
        qgain = qgain_ref[...] * (LOG2E * HEAD_DIM**-0.5)
        gains[...] = jnp.concatenate([qgain, qgain, kgain_ref[...], kgain_ref[...]], axis=1)
        key_gain = jnp.concatenate([kgain_ref[...], kgain_ref[...]], axis=1)
        sp = lax.axis_index("sp")
        for side, ref in enumerate((before_ref, after_ref)):
            at = 0 if side == 0 else (blocks + 1) * BLOCK
            live = (sp > 0) if side == 0 else (sp < lax.axis_size("sp") - 1)
            live = jnp.where(live, 1.0, 0.0)
            for s in range(4):
                kv = ref[s, 0:128, :].astype(F32)
                turned = pltpu.roll(kv, HEAD_DIM, 1)
                kk = jnp.where(low_lanes, kv, turned)
                vv = jnp.where(low_lanes, turned, kv)
                mean = jnp.sum(jnp.where(low_lanes, kv * kv, 0.0), axis=-1, keepdims=True) * (1.0 / HEAD_DIM)
                ks[s, pl.ds(at, BLOCK), :] = (kk * lax.rsqrt(mean + EPS) * key_gain).astype(BF16)
                vs[s, pl.ds(at, BLOCK), 0:128] = vv.astype(BF16)
                vs[s, pl.ds(at, BLOCK), 128:256] = jnp.full((BLOCK, 128), live, F32).astype(BF16)

    def project(part):
        size = rows // 2
        at = part * size
        xs[at : at + size, :] = x_ref.at[part * (BLOCK // 2) : (part + 1) * (BLOCK // 2)].reshape(size, x_ref.shape[2])[...]
        x = xs[at : at + size, :]
        cols = jnp.dot(x, w_ref[...], preferred_element_type=F32) * row_scale(x)
        qk = cols[:, :256]
        r = lax.broadcasted_iota(jnp.int32, (256, 256), 0) // HEAD_DIM
        c = lax.broadcasted_iota(jnp.int32, (256, 256), 1) // HEAD_DIM
        same = jnp.where(r == c, 1.0, 0.0).astype(BF16)
        squares = jnp.dot((qk * qk).astype(BF16), same, preferred_element_type=F32)
        normed = qk * lax.rsqrt(squares * (1.0 / HEAD_DIM) + EPS) * gains[...]
        proj[0, at : at + size] = normed[:, :128]
        proj[1, at : at + size] = normed[:, 128:]
        proj[2, at : at + size] = cols[:, 256:384]
        gate[step % 2, at : at + size, :] = cols[:, 384:]

    def separate():
        at = pl.multiple_of(step * BLOCK, BLOCK)
        for s in range(4):
            mine = pl.ds(s, BLOCK, stride=4)
            qs[step % 2, s] = proj[0, mine, :].astype(BF16)
            ks[s, pl.ds(at + BLOCK, BLOCK), :] = proj[1, mine, :].astype(BF16)
            vs[s, pl.ds(at + BLOCK, BLOCK), 0:128] = proj[2, mine, :].astype(BF16)
            vs[s, pl.ds(at + BLOCK, BLOCK), 128:256] = jnp.ones((BLOCK, 128), BF16)

    def attend(s):
        at = pl.multiple_of((step - 1) * BLOCK, BLOCK)
        q = qs[(step - 1) % 2, s]
        zero = jnp.zeros_like(q)
        two = jnp.concatenate([jnp.where(low_lanes, q, zero), jnp.where(low_lanes, zero, q)], axis=0)
        keys = ks[s, pl.ds(at, 3 * BLOCK), :]
        score = lax.dot_general(two, keys, (((1,), (1,)), ((), ())), preferred_element_type=F32)
        weight = jnp.exp2(score + bias[...]).astype(BF16)
        out = jnp.dot(weight, vs[s, pl.ds(at, 3 * BLOCK), :], preferred_element_type=F32)
        total = jnp.where(low_lanes, out[:BLOCK, 128:], out[BLOCK:, 128:]) + sinks[...]
        value = jnp.where(low_lanes, out[:BLOCK, :128], out[BLOCK:, :128])
        att[pl.ds(s, BLOCK, stride=4), :] = value / total
        turned = total.T
        lse_ref[s, 0:1, :] = jnp.log(turned[0:1, :]) + shifts[0]
        lse_ref[s, 1:2, :] = jnp.log(turned[HEAD_DIM : HEAD_DIM + 1, :]) + shifts[1]

    def close():
        y_ref[0] = (att[...] * silu(gate[(step - 1) % 2])).astype(BF16)

    @pl.when(step < blocks)
    def _():
        project(0)
        project(1)
        separate()

    @pl.when(step > 0)
    def _():
        for s in range(4):
            attend(s)
        close()


def attn_branch(sink, x, w, qgain, kgain, before, after, first):
    length, _, width = x.shape
    blocks = length // BLOCK
    rows = BLOCK * 4
    return pl.pallas_call(
        attn_kernel,
        grid=(blocks + 1,),
        in_specs=[
            pl.BlockSpec(memory_space=pltpu.SMEM),
            pl.BlockSpec((BLOCK, 4, width), lambda i: (jnp.minimum(i, blocks - 1), 0, 0)),
            pl.BlockSpec(w.shape, lambda i: (0, 0)),
            pl.BlockSpec(qgain.shape, lambda i: (0, 0)),
            pl.BlockSpec(kgain.shape, lambda i: (0, 0)),
            pl.BlockSpec(before.shape, lambda i: (0, 0, 0)),
            pl.BlockSpec(after.shape, lambda i: (0, 0, 0)),
            pl.BlockSpec(memory_space=pl.ANY),
        ],
        out_specs=(
            pl.BlockSpec((1, rows, 128), lambda i: (jnp.maximum(i - 1, 0), 0, 0)),
            pl.BlockSpec((4, 2, BLOCK), lambda i: (0, 0, jnp.maximum(i - 1, 0))),
        ),
        out_shape=(
            jax.ShapeDtypeStruct((blocks, rows, 128), BF16),
            jax.ShapeDtypeStruct((4, 2, length), F32),
        ),
        scratch_shapes=[
            pltpu.VMEM((3, rows, 128), F32),
            pltpu.VMEM((2, 4, BLOCK, 128), BF16),
            pltpu.VMEM((4, length + 2 * BLOCK, 128), BF16),
            pltpu.VMEM((4, length + 2 * BLOCK, 256), BF16),
            pltpu.VMEM((2, rows, 128), F32),
            pltpu.VMEM((2 * BLOCK, 3 * BLOCK), F32),
            pltpu.VMEM((rows, 128), F32),
            pltpu.VMEM((rows, width), BF16),
            pltpu.VMEM((BLOCK, 128), F32),
            pltpu.VMEM((1, 256), F32),
        ],
        compiler_params=pltpu.CompilerParams(dimension_semantics=("arbitrary",)),
        cost_estimate=pl.CostEstimate(flops=2 * 4096 * 2048 * 768, transcendentals=3 << 20, bytes_accessed=20 << 20),
        name="attn_branch",
    )(sink, x, w, qgain, kgain, before, after, first)


def half_kernel(which, y_ref, *rest):
    pieces, rest = rest[:8], rest[8:]
    add_ref, (o_ref, w, sems) = (None, rest) if which == 0 else (rest[0], rest[1:])
    tiles, _, tile = w.shape
    rows = y_ref.shape[1]
    step = pl.program_id(0)
    place = lax.axis_index("sp")
    z, y, core = place // 4, place % 4, lax.axis_index("tp") % 2

    def copies(n, side):
        for m in range(4):
            for k in range(4):
                a = (z + 4 - (m if which == 0 else k)) % 4
                b = (y + 4 - (k if which == 0 else m)) % 4
                row = pl.multiple_of((a * 4 + b) * 64, 64)
                yield pltpu.make_async_copy(
                    pieces[side * 4 + m].at[pl.ds(k * 64, 64), pl.ds(n * tile, tile)],
                    w.at[n, pl.ds(row, 64), :],
                    sems.at[n, m * 4 + k],
                )

    for side in range(2):

        @pl.when((step == 0) & (core == (which if side == 0 else 1 - which)))
        def _(side=side):
            for n in range(tiles):
                for copy in copies(n, side):
                    copy.start()

    for n in range(tiles):

        @pl.when(step == n)
        def _(n=n):
            for copy in copies(n, 0):
                copy.wait()

    lanes = jnp.concatenate([y_ref[j] for j in range(y_ref.shape[0])], axis=1)
    acc = jnp.dot(lanes, w[step], preferred_element_type=F32)
    if which == 0:
        o_ref[...] = acc
    else:
        o_ref.reshape(rows, tile)[...] = (acc + add_ref[...]).astype(BF16)


def half_matmul(which, y, pieces, add=None):
    parts, rows, cols = y.shape
    width = pieces[0].shape[1]
    tile = 512
    steps = width // tile
    if which == 0:
        out_spec = pl.BlockSpec((rows, tile), lambda n: (0, n))
        out_shape = jax.ShapeDtypeStruct((rows, width), F32)
    else:
        out_spec = pl.BlockSpec((rows // 4, 4, tile), lambda n: (0, 0, n))
        out_shape = jax.ShapeDtypeStruct((rows // 4, 4, width), BF16)
    return pl.pallas_call(
        functools.partial(half_kernel, which),
        grid=(steps,),
        in_specs=[pl.BlockSpec(y.shape, lambda n: (0, 0, 0))]
        + [pl.BlockSpec(memory_space=pl.ANY)] * 8
        + ([pl.BlockSpec((rows, tile), lambda n: (0, n))] if which else []),
        out_specs=out_spec,
        out_shape=out_shape,
        scratch_shapes=[
            pltpu.VMEM((steps, parts * cols, tile), BF16),
            pltpu.SemaphoreType.DMA((steps, 16)),
        ],
        compiler_params=pltpu.CompilerParams(dimension_semantics=("arbitrary",)),
        cost_estimate=pl.CostEstimate(flops=512 * 2048 * 2048, transcendentals=0, bytes_accessed=8 << 20),
    )(y, *pieces, *([add] if which else []))


def ring_pairs(shift, first):
    pairs = []
    for z in range(4):
        for y in range(4):
            for t in range(8):
                along_y = (t % 2 == 0) == first
                to = (z, (y + shift) % 4) if along_y else ((z + shift) % 4, y)
                pairs.append(((z * 4 + y) * 8 + t, (to[0] * 4 + to[1]) * 8 + t))
    return pairs


def gather_weights(out_pool, out_attn, core):
    both = ("sp", "tp")
    half = jnp.where(core == 0, out_pool, out_attn)
    return [half] + [lax.ppermute(half, both, ring_pairs(k, True)) for k in (1, 2, 3)]


def gather_rest(line):
    both = ("sp", "tp")
    block = jnp.concatenate(line, axis=0)
    mine = [block] + [lax.ppermute(block, both, ring_pairs(k, False)) for k in (1, 2, 3)]
    swap = [(i, i ^ 1) for i in range(8)]
    return mine + [lax.ppermute(piece, "tp", swap) for piece in mine]


def body(
    inputs,
    norm_gain,
    pool_proj,
    pool_gate_proj,
    pool_mix,
    query_proj,
    key_proj,
    value_proj,
    attn_gate_proj,
    query_gain,
    key_gain,
    sink_logit,
    out_pool,
    out_attn,
):
    tp = lax.axis_index("tp")
    sp_size = lax.axis_size("sp")
    core = tp % 2
    line = gather_weights(out_pool, out_attn, core)
    head, tail, w_pool, w_attn = first_rows(
        inputs, norm_gain[None, :], pool_proj, pool_gate_proj, query_proj, key_proj.T, value_proj.T, attn_gate_proj
    )
    up = [(i, i + 1) for i in range(sp_size - 1)]
    down = [(j, i) for i, j in up]
    *line, head, tail = lax.optimization_barrier((*line, head, tail))
    before = lax.ppermute(tail, "sp", up)
    after = lax.ppermute(head, "sp", down)
    pieces = gather_rest(line)
    y_pool = pool_branch(inputs, w_pool, pool_mix, before, after)
    pool_rows = lax.all_to_all(y_pool, "tp", split_axis=0, concat_axis=0, tiled=True)
    y_attn, lse = attn_branch(
        sink_logit, inputs, w_attn, query_gain[None, :], key_gain[None, :], before, after, y_pool
    )
    y_attn, pool_rows = lax.optimization_barrier((y_attn, pool_rows))
    attn_rows = lax.all_to_all(y_attn, "tp", split_axis=0, concat_axis=0, tiled=True)
    partial = half_matmul(0, pool_rows, pieces)
    mixed = half_matmul(1, attn_rows, pieces, partial)
    return mixed, jnp.transpose(lse, (2, 0, 1))


def solution(mesh):
    placed = (
        P("sp", None, None),
        P(),
        P(None, "tp"),
        P(None, "tp"),
        P("tp", None, None),
        P(None, "tp"),
        P(None, "tp"),
        P(None, "tp"),
        P(None, "tp"),
        P(),
        P(),
        P("tp"),
        P("sp", None),
        P("sp", None),
    )

    return jax.shard_map(
        body,
        mesh=mesh,
        in_specs=placed,
        out_specs=(P(("sp", "tp"), None, None), P("sp", None, "tp")),
        check_vma=False,
    )
```

time: 121 us -> 121 us (level)
  the two profiles are of different devices: /device:TPU:96 before, /device:TPU:24 now
where the time goes in v1:
time: 121 us; the launch traced here: 119 us
  Pallas kernels  61.6 us (51%)
  starting transfers between devices  38 us (31%)
  waiting for transfers between devices  15.7 us (13%)
  local copies, waits for them, and re-layouts  1.77 us (1%)
    pallas_call x1, Pallas kernels, attn_branch(): pl.pallas_call(attn_kernel, grid=(blocks + 1,), in_specs=[pl.BlockSpec(me...  24 us
    pallas_call x2, Pallas kernels, half_matmul(): pl.pallas_call(functools.partial(half_kernel, which), grid=(steps,), in_s...  15.3 us
    pallas_call x1, Pallas kernels, pool_branch(): pl.pallas_call(pool_kernel, grid=(blocks + 1,), in_specs=[pl.BlockSpec(me...  14.6 us
    ppermute x4, starting transfers between devices, gather_rest(): return mine + [lax.ppermute(piece, 'tp', swap) for piece in mine]  12.1 us
    all_to_all x1, waiting for transfers between devices, body(): lax.all_to_all(y_attn, 'tp', split_axis=0, concat_axis=0, tiled=True)  8.49 us
    pallas_call x1, Pallas kernels, first_rows(): pl.pallas_call(first_kernel, grid=(4,), in_specs=[pl.BlockSpec((half, 4,...  7.66 us
    ppermute x1, waiting for transfers between devices, body(): before = lax.ppermute(tail, 'sp', up)  7.13 us
    ppermute x1, starting transfers between devices, body(): before = lax.ppermute(tail, 'sp', up)  5.93 us
  transfers between devices with their start and end apart: 14, of which 2 were waited for; matrix products, arithmetic and copies ran while one was open for 0% of the time, Pallas kernels for 45%

profile of v1, /device:TPU:24, one launch (start us, length us, event | category | flops | bytes accessed | tf_op | source)
XLA Modules:
  0.0 118.8 jit_solution(14982959036526423108)
XLA Ops:
  0.6 1.0 broadcast_select_fusion
  1.6 0.8 collective-permute-start.2
  2.4 0.8 collective-permute-start.1
  3.3 2.3 %collective-permute-start = (bf16[64,2048]{1,0:T(8,128)(2,1)S(1)}, bf16[64,2048]{1,0:T(8,128)(2,1)S(1)}, u32[]{:S(2)}, u32[]{:S(2)}) collective-permute-start(bf16[64,2048]{1,0:T(8,128)(2,1)S(1)} %broadcast_select_fusion), channel_id=1, source_target_pairs={{0,8},{1,33},{2,10},{3,35},{4,12},{5,37},{6,14},{7,39},{8,16},{9,4... | collective-permute-start | bytes 786440 | tf_op jit(solution)/shard_map/ppermute | solution.py:458
  5.6 7.7 %first_rows.1 = (bf16[4,136,128]{2,1,0:T(8,128)(2,1)}, bf16[4,136,128]{2,1,0:T(8,128)(2,1)}, bf16[2048,256]{1,0:T(8,128)(2,1)}, bf16[2048,512]{1,0:T(8,128)(2,1)}) custom-call(bf16[1024,4,2048]{2,1,0:T(4,128)(2,1)} %x_ref.5, f32[1,2048]{1,0:T(1,128)} %bitcast.8, bf16[2048,128]{1,0:T(8,128)(2,1)} %pool_ref.1, bf16[2048,128]{1,0:T(8,128)(2,1)} %pgate_ref.1, ...), custom_call_target="tpu_custom_call" | custom-call | flops 1073741824 | bytes 12582912 | tf_op jit(solution)/shard_map/first_rows/pallas_call | solution.py:91
  13.2 0.0 collective-permute-done.2
  13.2 0.0 collective-permute-done.1
  13.2 0.0 collective-permute-done
  13.4 0.0 copy-start
  13.4 4.1 %collective-permute-start.7 = (bf16[256,2048]{1,0:T(8,128)(2,1)S(1)}, bf16[256,2048]{1,0:T(8,128)(2,1)}, u32[]{:S(2)}, u32[]{:S(2)}) collective-permute-start(bf16[256,2048]{1,0:T(8,128)(2,1)S(1)} %constant_dynamic-update-slice_fusion.rest_0_), channel_id=1, source_target_pairs={{0,96},{1,25},{2,98},{3,27},{4,100},{5,29},{6,102},{7,31},{8,104},... | collective-permute-start | bytes 3145736 | tf_op jit(solution)/shard_map/ppermute | solution.py:464
  17.5 0.0 collective-permute-start.6
  17.5 1.3 %collective-permute-start.5 = (bf16[256,2048]{1,0:T(8,128)(2,1)S(1)}, bf16[256,2048]{1,0:T(8,128)(2,1)}, u32[]{:S(2)}, u32[]{:S(2)}) collective-permute-start(bf16[256,2048]{1,0:T(8,128)(2,1)S(1)} %constant_dynamic-update-slice_fusion.rest_0_), channel_id=1, source_target_pairs={{0,32},{1,9},{2,34},{3,11},{4,36},{5,13},{6,38},{7,15},{8,40},{9,1... | collective-permute-start | bytes 3145736 | tf_op jit(solution)/shard_map/ppermute | solution.py:464
  18.7 5.9 %collective-permute-start.3 = (bf16[4,136,128]{2,1,0:T(8,128)(2,1)}, bf16[4,136,128]{2,1,0:T(8,128)(2,1)S(1)}, u32[]{:S(2)}, u32[]{:S(2)}) collective-permute-start(bf16[4,136,128]{2,1,0:T(8,128)(2,1)} %get-tuple-element.19), channel_id=1, source_target_pairs={{0,8},{8,16},{16,24},{24,32},{32,40},{40,48},{48,56},{56,64},{64,7... | collective-permute-start | bytes 417800 | tf_op jit(solution)/shard_map/ppermute | solution.py:495
  24.7 1.9 %collective-permute-start.4 = (bf16[4,136,128]{2,1,0:T(8,128)(2,1)}, bf16[4,136,128]{2,1,0:T(8,128)(2,1)S(1)}, u32[]{:S(2)}, u32[]{:S(2)}) collective-permute-start(bf16[4,136,128]{2,1,0:T(8,128)(2,1)} %get-tuple-element.20), channel_id=1, source_target_pairs={{8,0},{16,8},{24,16},{32,24},{40,32},{48,40},{56,48},{64,56},{72,6... | collective-permute-start | bytes 417800 | tf_op jit(solution)/shard_map/ppermute | solution.py:496
  26.6 7.1 %collective-permute-done.3.before_ref = bf16[4,136,128]{2,1,0:T(8,128)(2,1)S(1)} collective-permute-done((bf16[4,136,128]{2,1,0:T(8,128)(2,1)}, bf16[4,136,128]{2,1,0:T(8,128)(2,1)S(1)}, u32[]{:S(2)}, u32[]{:S(2)}) %collective-permute-start.3) | collective-permute-done | bytes 139296 | tf_op jit(solution)/shard_map/ppermute | solution.py:495
  33.7 0.0 copy-start.3
  33.7 11.1 %collective-permute-start.8 = (bf16[256,2048]{1,0:T(8,128)(2,1)S(1)}, bf16[256,2048]{1,0:T(8,128)(2,1)}, u32[]{:S(2)}, u32[]{:S(2)}) collective-permute-start(bf16[256,2048]{1,0:T(8,128)(2,1)S(1)} %constant_dynamic-update-slice_fusion.rest_0_), channel_id=1, source_target_pairs={{0,1},{1,0},{2,3},{3,2},{4,5},{5,4},{6,7},{7,6},{8,9},{9,8},{10,11... | collective-permute-start | bytes 3145736 | tf_op jit(solution)/shard_map/ppermute | solution.py:466
  44.8 0.0 collective-permute-done.4.after_ref
  44.8 0.0 copy-start.4
  44.8 0.0 copy-done.3
  44.8 0.6 copy-done.4
  45.5 14.6 %pool_branch.1.first_ref = bf16[8,512,128]{2,1,0:T(8,128)(2,1)} custom-call(bf16[1024,4,2048]{2,1,0:T(4,128)(2,1)} %x_ref.5, bf16[2048,256]{1,0:T(8,128)(2,1)} %get-tuple-element.21.w_ref, bf16[1,128,128]{2,1,0:T(8,128)(2,1)} %mix_ref.1, bf16[4,136,128]{2,1,0:T(8,128)(2,1)} %copy-done.3, bf16[4,136,128]{2,1,0:T(8,128)(2,1)} %copy-done.4), custom_call_target="tpu_custom_call" | custom-call | flops 4294967296 | bytes 18874368 | tf_op jit(solution)/shard_map/pool_branch/pallas_call | solution.py:200
  60.1 0.0 copy-done
  60.1 4.3 %all-to-all-start = ((bf16[8,512,128]{2,1,0:T(8,128)(2,1)}), bf16[8,512,128]{2,1,0:T(8,128)(2,1)S(1)}, u32[]{:S(2)}, u32[]{:S(2)}) async-start(bf16[8,512,128]{2,1,0:T(8,128)(2,1)} %pool_branch.1.first_ref), calls=%async_computation | async-start | bytes 2097152 | tf_op jit(solution)/shard_map/all_to_all | solution.py:499
  64.4 0.0 collective-permute-done.7.rest_3_
  64.4 0.5 collective-permute-start.11
  64.9 0.0 collective-permute-done.6.rest_2_
  64.9 0.1 collective-permute-start.10
  65.0 0.0 collective-permute-done.5.rest_1_
  65.0 0.4 collective-permute-start.9
  65.4 24.0 %attn_branch.1 = (bf16[8,512,128]{2,1,0:T(8,128)(2,1)}, f32[4,2,1024]{2,1,0:T(2,128)}) custom-call(f32[2]{0:T(128)} %sink_ref.1, bf16[1024,4,2048]{2,1,0:T(4,128)(2,1)} %x_ref.5, bf16[2048,512]{1,0:T(8,128)(2,1)} %get-tuple-element.16.w_ref, f32[1,64]{1,0:T(1,128)} %bitcast.9, f32[1,64]{1,0:T(1,128)} %bitcast.10, bf16[4,136,128]{2,1,0:T(8,128)(2,1)} %copy-done.3, ...), custom_call_target="tpu_custom_call" | custom-call | flops 12884901888 | bytes 20971520 | tf_op jit(solution)/shard_map/attn_branch/pallas_call | solution.py:333
  89.4 0.0 all-to-all-done.y_ref
  89.4 0.0 copy-start.1
  89.5 4.4 %all-to-all-start.1 = ((bf16[8,512,128]{2,1,0:T(8,128)(2,1)}), bf16[8,512,128]{2,1,0:T(8,128)(2,1)S(1)}, u32[]{:S(2)}, u32[]{:S(2)}) async-start(bf16[8,512,128]{2,1,0:T(8,128)(2,1)} %get-tuple-element.23), calls=%async_computation.1 | async-start | bytes 2097152 | tf_op jit(solution)/shard_map/all_to_all | solution.py:504
  93.9 0.0 collective-permute-done.8.rest_4_
  93.9 0.0 collective-permute-done.11.rest_7_
  93.9 0.0 collective-permute-done.10.rest_6_
  93.9 0.0 collective-permute-done.9.rest_5_
  93.9 0.0 copy-done.1
  93.9 7.4 %shard_map.149.rest_8_ = f32[512,2048]{1,0:T(8,128)} custom-call(bf16[8,512,128]{2,1,0:T(8,128)(2,1)} %copy-done.1, bf16[256,2048]{1,0:T(8,128)(2,1)} %copy-done, bf16[256,2048]{1,0:T(8,128)(2,1)} %collective-permute-done.5.rest_1_, bf16[256,2048]{1,0:T(8,128)(2,1)} %collective-permute-done.6.rest_2_, bf16[256,2048]{1,0:T(8,128)(2,1)} %collective-permute-done.7.rest_3_, ...), custom_call_target="tpu_custom_call" | custom-call | flops 2147483648 | bytes 8388608 | tf_op jit(solution)/shard_map/pallas_call | solution.py:427
  101.3 8.5 %all-to-all-done.1.y_ref = bf16[8,512,128]{2,1,0:T(8,128)(2,1)S(1)} async-done(((bf16[8,512,128]{2,1,0:T(8,128)(2,1)}), bf16[8,512,128]{2,1,0:T(8,128)(2,1)S(1)}, u32[]{:S(2)}, u32[]{:S(2)}) %all-to-all-start.1) | async-done | bytes 1048608 | tf_op jit(solution)/shard_map/all_to_all | solution.py:504
  109.8 0.0 copy-start.2
  109.8 1.0 copy-done.2
  110.9 7.9 %shard_map.150 = bf16[128,4,2048]{2,1,0:T(4,128)(2,1)} custom-call(bf16[8,512,128]{2,1,0:T(8,128)(2,1)} %copy-done.2, bf16[256,2048]{1,0:T(8,128)(2,1)} %copy-done, bf16[256,2048]{1,0:T(8,128)(2,1)} %collective-permute-done.5.rest_1_, bf16[256,2048]{1,0:T(8,128)(2,1)} %collective-permute-done.6.rest_2_, bf16[256,2048]{1,0:T(8,128)(2,1)} %collective-permute-done.7.rest_3_, ...), custom_call_target="tpu_custom_call" | custom-call | flops 2147483648 | bytes 8388608 | tf_op jit(solution)/shard_map/pallas_call | solution.py:427
  (4 shorter events, 0.1 us)
Async XLA Ops:
  1.6 11.6 %collective-permute-start.2 = (bf16[64,2048]{1,0:T(8,128)(2,1)S(1)}, bf16[64,2048]{1,0:T(8,128)(2,1)S(1)}, u32[]{:S(2)}, u32[]{:S(2)}) collective-permute-start(bf16[64,2048]{1,0:T(8,128)(2,1)S(1)} %broadcast_select_fusion), channel_id=1, source_target_pairs={{0,24},{1,97},{2,26},{3,99},{4,28},{5,101},{6,30},{7,103},{8,0},{9... | collective-permute-start | bytes 786440 | tf_op jit(solution)/shard_map/ppermute | solution.py:458
  2.4 10.8 %collective-permute-start.1 = (bf16[64,2048]{1,0:T(8,128)(2,1)S(1)}, bf16[64,2048]{1,0:T(8,128)(2,1)S(1)}, u32[]{:S(2)}, u32[]{:S(2)}) collective-permute-start(bf16[64,2048]{1,0:T(8,128)(2,1)S(1)} %broadcast_select_fusion), channel_id=1, source_target_pairs={{0,16},{1,65},{2,18},{3,67},{4,20},{5,69},{6,22},{7,71},{8,24},{9,... | collective-permute-start | bytes 786440 | tf_op jit(solution)/shard_map/ppermute | solution.py:458
  3.3 10.0 %collective-permute-start = (bf16[64,2048]{1,0:T(8,128)(2,1)S(1)}, bf16[64,2048]{1,0:T(8,128)(2,1)S(1)}, u32[]{:S(2)}, u32[]{:S(2)}) collective-permute-start(bf16[64,2048]{1,0:T(8,128)(2,1)S(1)} %broadcast_select_fusion), channel_id=1, source_target_pairs={{0,8},{1,33},{2,10},{3,35},{4,12},{5,37},{6,14},{7,39},{8,16},{9,4... | collective-permute-start | bytes 786440 | tf_op jit(solution)/shard_map/ppermute | solution.py:458
  13.4 46.7 %copy-start = (bf16[256,2048]{1,0:T(8,128)(2,1)}, bf16[256,2048]{1,0:T(8,128)(2,1)S(1)}, u32[]{:S(2)}) copy-start(bf16[256,2048]{1,0:T(8,128)(2,1)S(1)} %constant_dynamic-update-slice_fusion.rest_0_) | copy-start | bytes 3145732
  13.4 51.0 %collective-permute-start.7 = (bf16[256,2048]{1,0:T(8,128)(2,1)S(1)}, bf16[256,2048]{1,0:T(8,128)(2,1)}, u32[]{:S(2)}, u32[]{:S(2)}) collective-permute-start(bf16[256,2048]{1,0:T(8,128)(2,1)S(1)} %constant_dynamic-update-slice_fusion.rest_0_), channel_id=1, source_target_pairs={{0,96},{1,25},{2,98},{3,27},{4,100},{5,29},{6,102},{7,31},{8,104},... | collective-permute-start | bytes 3145736 | tf_op jit(solution)/shard_map/ppermute | solution.py:464
  17.5 47.4 %collective-permute-start.6 = (bf16[256,2048]{1,0:T(8,128)(2,1)S(1)}, bf16[256,2048]{1,0:T(8,128)(2,1)}, u32[]{:S(2)}, u32[]{:S(2)}) collective-permute-start(bf16[256,2048]{1,0:T(8,128)(2,1)S(1)} %constant_dynamic-update-slice_fusion.rest_0_), channel_id=1, source_target_pairs={{0,64},{1,17},{2,66},{3,19},{4,68},{5,21},{6,70},{7,23},{8,72},{9,... | collective-permute-start | bytes 3145736 | tf_op jit(solution)/shard_map/ppermute | solution.py:464
  17.5 47.5 %collective-permute-start.5 = (bf16[256,2048]{1,0:T(8,128)(2,1)S(1)}, bf16[256,2048]{1,0:T(8,128)(2,1)}, u32[]{:S(2)}, u32[]{:S(2)}) collective-permute-start(bf16[256,2048]{1,0:T(8,128)(2,1)S(1)} %constant_dynamic-update-slice_fusion.rest_0_), channel_id=1, source_target_pairs={{0,32},{1,9},{2,34},{3,11},{4,36},{5,13},{6,38},{7,15},{8,40},{9,1... | collective-permute-start | bytes 3145736 | tf_op jit(solution)/shard_map/ppermute | solution.py:464
  18.7 15.0 %collective-permute-start.3 = (bf16[4,136,128]{2,1,0:T(8,128)(2,1)}, bf16[4,136,128]{2,1,0:T(8,128)(2,1)S(1)}, u32[]{:S(2)}, u32[]{:S(2)}) collective-permute-start(bf16[4,136,128]{2,1,0:T(8,128)(2,1)} %get-tuple-element.19), channel_id=1, source_target_pairs={{0,8},{8,16},{16,24},{24,32},{32,40},{40,48},{48,56},{56,64},{64,7... | collective-permute-start | bytes 417800 | tf_op jit(solution)/shard_map/ppermute | solution.py:495
  24.7 20.2 %collective-permute-start.4 = (bf16[4,136,128]{2,1,0:T(8,128)(2,1)}, bf16[4,136,128]{2,1,0:T(8,128)(2,1)S(1)}, u32[]{:S(2)}, u32[]{:S(2)}) collective-permute-start(bf16[4,136,128]{2,1,0:T(8,128)(2,1)} %get-tuple-element.20), channel_id=1, source_target_pairs={{8,0},{16,8},{24,16},{32,24},{40,32},{48,40},{56,48},{64,56},{72,6... | collective-permute-start | bytes 417800 | tf_op jit(solution)/shard_map/ppermute | solution.py:496
  33.7 11.1 %copy-start.3 = (bf16[4,136,128]{2,1,0:T(8,128)(2,1)}, bf16[4,136,128]{2,1,0:T(8,128)(2,1)S(1)}, u32[]{:S(2)}) copy-start(bf16[4,136,128]{2,1,0:T(8,128)(2,1)S(1)} %collective-permute-done.3.before_ref) | copy-start | bytes 417796
  33.7 60.1 %collective-permute-start.8 = (bf16[256,2048]{1,0:T(8,128)(2,1)S(1)}, bf16[256,2048]{1,0:T(8,128)(2,1)}, u32[]{:S(2)}, u32[]{:S(2)}) collective-permute-start(bf16[256,2048]{1,0:T(8,128)(2,1)S(1)} %constant_dynamic-update-slice_fusion.rest_0_), channel_id=1, source_target_pairs={{0,1},{1,0},{2,3},{3,2},{4,5},{5,4},{6,7},{7,6},{8,9},{9,8},{10,11... | collective-permute-start | bytes 3145736 | tf_op jit(solution)/shard_map/ppermute | solution.py:466
  44.8 0.7 copy-start.4
  60.1 29.4 %all-to-all-start = ((bf16[8,512,128]{2,1,0:T(8,128)(2,1)}), bf16[8,512,128]{2,1,0:T(8,128)(2,1)S(1)}, u32[]{:S(2)}, u32[]{:S(2)}) async-start(bf16[8,512,128]{2,1,0:T(8,128)(2,1)} %pool_branch.1.first_ref), calls=%async_computation | async-start | bytes 2097152 | tf_op jit(solution)/shard_map/all_to_all | solution.py:499
  64.4 29.5 %collective-permute-start.11 = (bf16[256,2048]{1,0:T(8,128)(2,1)}, bf16[256,2048]{1,0:T(8,128)(2,1)}, u32[]{:S(2)}, u32[]{:S(2)}) collective-permute-start(bf16[256,2048]{1,0:T(8,128)(2,1)} %collective-permute-done.7.rest_3_), channel_id=1, source_target_pairs={{0,1},{1,0},{2,3},{3,2},{4,5},{5,4},{6,7},{7,6},{8,9},{9,8},{10,11... | collective-permute-start | bytes 3145736 | tf_op jit(solution)/shard_map/ppermute | solution.py:466
  64.9 29.0 %collective-permute-start.10 = (bf16[256,2048]{1,0:T(8,128)(2,1)}, bf16[256,2048]{1,0:T(8,128)(2,1)}, u32[]{:S(2)}, u32[]{:S(2)}) collective-permute-start(bf16[256,2048]{1,0:T(8,128)(2,1)} %collective-permute-done.6.rest_2_), channel_id=1, source_target_pairs={{0,1},{1,0},{2,3},{3,2},{4,5},{5,4},{6,7},{7,6},{8,9},{9,8},{10,11... | collective-permute-start | bytes 3145736 | tf_op jit(solution)/shard_map/ppermute | solution.py:466
  65.0 28.9 %collective-permute-start.9 = (bf16[256,2048]{1,0:T(8,128)(2,1)}, bf16[256,2048]{1,0:T(8,128)(2,1)}, u32[]{:S(2)}, u32[]{:S(2)}) collective-permute-start(bf16[256,2048]{1,0:T(8,128)(2,1)} %collective-permute-done.5.rest_1_), channel_id=1, source_target_pairs={{0,1},{1,0},{2,3},{3,2},{4,5},{5,4},{6,7},{7,6},{8,9},{9,8},{10,11... | collective-permute-start | bytes 3145736 | tf_op jit(solution)/shard_map/ppermute | solution.py:466
  89.4 4.5 %copy-start.1 = (bf16[8,512,128]{2,1,0:T(8,128)(2,1)}, bf16[8,512,128]{2,1,0:T(8,128)(2,1)S(1)}, u32[]{:S(2)}) copy-start(bf16[8,512,128]{2,1,0:T(8,128)(2,1)S(1)} %all-to-all-done.y_ref) | copy-start | bytes 3145732
  89.5 20.4 %all-to-all-start.1 = ((bf16[8,512,128]{2,1,0:T(8,128)(2,1)}), bf16[8,512,128]{2,1,0:T(8,128)(2,1)S(1)}, u32[]{:S(2)}, u32[]{:S(2)}) async-start(bf16[8,512,128]{2,1,0:T(8,128)(2,1)} %get-tuple-element.23), calls=%async_computation.1 | async-start | bytes 2097152 | tf_op jit(solution)/shard_map/all_to_all | solution.py:504
  109.8 1.0 copy-start.2

commit v2 on v1

--- a/solution.py
+++ b/solution.py
@@ -7,7 +7,6 @@
 from jax.experimental import pallas as pl
 from jax.experimental.pallas import tpu as pltpu
 from jax.sharding import PartitionSpec as P
-
 
 HEAD_DIM = 64
 WINDOW = 128
@@ -38,10 +37,11 @@
 
 def first_kernel(
     x_ref, gain_ref, pool_ref, pgate_ref, query_ref, keyt_ref, valuet_ref, agate_ref,
-    head_ref, tail_ref, wp_ref, wa_ref, w_edge, scr, xs,
+    head_ref, tail_ref, wp_out, wa_out, w_edge, scr, xs, wp_ref, wa_ref, sems,
 ):
     half = x_ref.shape[0]
     step = pl.program_id(0)
+    leave = [pltpu.make_async_copy(a, b, sems.at[n]) for n, (a, b) in enumerate(((wp_ref, wp_out), (wa_ref, wa_out)))]
 
     @pl.when(step == 0)
     def _():
@@ -61,6 +61,8 @@
             wa_ref[rows, 384:512] = (agate_ref[rows, :].astype(F32) * column).astype(BF16)
             w_edge[rows, 0:128] = pool
             w_edge[rows, 128:256] = kv.astype(BF16)
+        for copy in leave:
+            copy.start()
 
     xs[...] = x_ref.reshape(half * 4, x_ref.shape[2])[...]
     x = xs[...]
@@ -78,6 +80,9 @@
                 out[s, part * half : (part + 1) * half, :] = rows.astype(BF16)
                 if n == 0:
                     out[s, 128 : 128 + REACH, :] = scr[0, pl.ds(s, REACH, stride=4), :].astype(BF16)
+                if n == 3 and s == 0:
+                    for copy in leave:
+                        copy.wait()
                 if n == 3:
                     rows = scr[0, pl.ds(s + 4 * (half - REACH), REACH, stride=4), :]
                     out[s, 128 : 128 + REACH, :] = rows.astype(BF16)
@@ -96,8 +101,8 @@
         out_specs=(
             pl.BlockSpec((4, 136, 128), lambda i: (0, 0, 0)),
             pl.BlockSpec((4, 136, 128), lambda i: (0, 0, 0)),
-            pl.BlockSpec((width, 256), lambda i: (0, 0)),
-            pl.BlockSpec((width, 512), lambda i: (0, 0)),
+            pl.BlockSpec(memory_space=pl.ANY),
+            pl.BlockSpec(memory_space=pl.ANY),
         ),
         out_shape=(
             jax.ShapeDtypeStruct((4, 136, 128), BF16),
@@ -109,6 +114,9 @@
             pltpu.VMEM((width, 256), BF16),
             pltpu.VMEM((2, half * 4, 128), F32),
             pltpu.VMEM((half * 4, width), BF16),
+            pltpu.VMEM((width, 256), BF16),
+            pltpu.VMEM((width, 512), BF16),
+            pltpu.SemaphoreType.DMA((2,)),
         ],
         compiler_params=pltpu.CompilerParams(dimension_semantics=("arbitrary",)),
         cost_estimate=pl.CostEstimate(flops=2 * 1024 * 2048 * 256, transcendentals=0, bytes_accessed=12 << 20),
@@ -116,7 +124,7 @@
     )(x, *whole)
 
 
-def pool_kernel(x_ref, w_ref, mix_ref, before_ref, after_ref, y_ref, pool, gate, inverse, xs, xv, sems):
+def pool_kernel(x_ref, w_ref, mix_ref, before_ref, after_ref, y_ref, scale_ref, pool, gate, inverse, xs, xv, sems):
     step = pl.program_id(0)
     blocks = pl.num_programs(0) - 1
     rows = BLOCK * 4
@@ -174,7 +182,9 @@
         fetch(step).wait()
         xs[...] = xv.at[pl.ds(pl.multiple_of(step * BLOCK, BLOCK), BLOCK)].reshape(rows, xv.shape[2])[...]
         x = xs[...]
-        both = jnp.dot(x, w_ref[...], preferred_element_type=F32) * row_scale(x)
+        scale = row_scale(x)
+        scale_ref[...] = jnp.broadcast_to(scale, (rows, 128))
+        both = jnp.dot(x, w_ref[...], preferred_element_type=F32) * scale
         at = pl.multiple_of(step * rows, rows)
         pool[pl.ds(pad + at, rows), :] = both[:, :128]
         gate[pl.ds(at, rows), :] = both[:, 128:]
@@ -207,8 +217,14 @@
             pl.BlockSpec(before.shape, lambda i: (0, 0, 0)),
             pl.BlockSpec(after.shape, lambda i: (0, 0, 0)),
         ],
-        out_specs=pl.BlockSpec((1, rows, 128), lambda i: (jnp.maximum(i - 1, 0), 0, 0)),
-        out_shape=jax.ShapeDtypeStruct((blocks, rows, 128), BF16),
+        out_specs=(
+            pl.BlockSpec((1, rows, 128), lambda i: (jnp.maximum(i - 1, 0), 0, 0)),
+            pl.BlockSpec((rows, 128), lambda i: (jnp.minimum(i, blocks - 1), 0)),
+        ),
+        out_shape=(
+            jax.ShapeDtypeStruct((blocks, rows, 128), BF16),
+            jax.ShapeDtypeStruct((length * 4, 128), F32),
+        ),
         scratch_shapes=[
             pltpu.VMEM((length * 4 + 128, 128), F32),
             pltpu.VMEM((length * 4, 128), F32),
@@ -224,10 +240,9 @@
 
 
 def attn_kernel(
-    sink_ref, x_ref, w_ref, qgain_ref, kgain_ref, before_ref, after_ref, first_ref,
-    y_ref, lse_ref, proj, qs, ks, vs, gate, bias, att, xs, sinks, gains,
+    sink_ref, x_ref, scale_ref, w_ref, qgain_ref, kgain_ref, before_ref, after_ref,
+    y_ref, lse_ref, proj, qs, ks, vs, gate, bias, att, xs, sinks, gains, same,
 ):
-    del first_ref
     step = pl.program_id(0)
     blocks = pl.num_programs(0) - 1
     rows = BLOCK * 4
@@ -240,6 +255,9 @@
         query = lax.broadcasted_iota(jnp.int32, (BLOCK, 3 * BLOCK), 0)
         key = lax.broadcasted_iota(jnp.int32, (BLOCK, 3 * BLOCK), 1) - BLOCK
         distance = jnp.abs(query - key)
+        r = lax.broadcasted_iota(jnp.int32, (256, 256), 0) // HEAD_DIM
+        c = lax.broadcasted_iota(jnp.int32, (256, 256), 1) // HEAD_DIM
+        same[...] = jnp.where(r == c, 1.0, 0.0).astype(BF16)
         scale = lax.broadcasted_iota(jnp.int32, (BLOCK, 3 * BLOCK), 0) * 0 + jnp.left_shift(
             jnp.int32(1), lax.axis_index("tp")
         )
@@ -273,17 +291,15 @@
         at = part * size
         xs[at : at + size, :] = x_ref.at[part * (BLOCK // 2) : (part + 1) * (BLOCK // 2)].reshape(size, x_ref.shape[2])[...]
         x = xs[at : at + size, :]
-        cols = jnp.dot(x, w_ref[...], preferred_element_type=F32) * row_scale(x)
-        qk = cols[:, :256]
-        r = lax.broadcasted_iota(jnp.int32, (256, 256), 0) // HEAD_DIM
-        c = lax.broadcasted_iota(jnp.int32, (256, 256), 1) // HEAD_DIM
-        same = jnp.where(r == c, 1.0, 0.0).astype(BF16)
-        squares = jnp.dot((qk * qk).astype(BF16), same, preferred_element_type=F32)
+        cols = jnp.dot(x, w_ref[...], preferred_element_type=F32)
+        scale = scale_ref[at : at + size, :]
+        qk = cols[:, :256] * jnp.concatenate([scale, scale], axis=1)
+        squares = jnp.dot((qk * qk).astype(BF16), same[...], preferred_element_type=F32)
         normed = qk * lax.rsqrt(squares * (1.0 / HEAD_DIM) + EPS) * gains[...]
         proj[0, at : at + size] = normed[:, :128]
         proj[1, at : at + size] = normed[:, 128:]
-        proj[2, at : at + size] = cols[:, 256:384]
-        gate[step % 2, at : at + size, :] = cols[:, 384:]
+        proj[2, at : at + size] = cols[:, 256:384] * scale
+        gate[step % 2, at : at + size, :] = cols[:, 384:] * scale
 
     def separate():
         at = pl.multiple_of(step * BLOCK, BLOCK)
@@ -326,7 +342,7 @@
         close()
 
 
-def attn_branch(sink, x, w, qgain, kgain, before, after, first):
+def attn_branch(sink, x, scale, w, qgain, kgain, before, after):
     length, _, width = x.shape
     blocks = length // BLOCK
     rows = BLOCK * 4
@@ -336,12 +352,12 @@
         in_specs=[
             pl.BlockSpec(memory_space=pltpu.SMEM),
             pl.BlockSpec((BLOCK, 4, width), lambda i: (jnp.minimum(i, blocks - 1), 0, 0)),
+            pl.BlockSpec((rows, 128), lambda i: (jnp.minimum(i, blocks - 1), 0)),
             pl.BlockSpec(w.shape, lambda i: (0, 0)),
             pl.BlockSpec(qgain.shape, lambda i: (0, 0)),
             pl.BlockSpec(kgain.shape, lambda i: (0, 0)),
             pl.BlockSpec(before.shape, lambda i: (0, 0, 0)),
             pl.BlockSpec(after.shape, lambda i: (0, 0, 0)),
-            pl.BlockSpec(memory_space=pl.ANY),
         ],
         out_specs=(
             pl.BlockSpec((1, rows, 128), lambda i: (jnp.maximum(i - 1, 0), 0, 0)),
@@ -362,11 +378,12 @@
             pltpu.VMEM((rows, width), BF16),
             pltpu.VMEM((BLOCK, 128), F32),
             pltpu.VMEM((1, 256), F32),
+            pltpu.VMEM((256, 256), BF16),
         ],
         compiler_params=pltpu.CompilerParams(dimension_semantics=("arbitrary",)),
         cost_estimate=pl.CostEstimate(flops=2 * 4096 * 2048 * 768, transcendentals=3 << 20, bytes_accessed=20 << 20),
         name="attn_branch",
-    )(sink, x, w, qgain, kgain, before, after, first)
+    )(sink, x, scale, w, qgain, kgain, before, after)
 
 
 def half_kernel(which, y_ref, *rest):
@@ -427,7 +444,7 @@
     return pl.pallas_call(
         functools.partial(half_kernel, which),
         grid=(steps,),
-        in_specs=[pl.BlockSpec(y.shape, lambda n: (0, 0, 0))]
+        in_specs=[pl.BlockSpec(memory_space=pltpu.VMEM)]
         + [pl.BlockSpec(memory_space=pl.ANY)] * 8
         + ([pl.BlockSpec((rows, tile), lambda n: (0, n))] if which else []),
         out_specs=out_spec,
@@ -438,7 +455,7 @@
         ],
         compiler_params=pltpu.CompilerParams(dimension_semantics=("arbitrary",)),
         cost_estimate=pl.CostEstimate(flops=512 * 2048 * 2048, transcendentals=0, bytes_accessed=8 << 20),
-    )(y, *pieces, *([add] if which else []))
+    )(pltpu.with_memory_space_constraint(y, pltpu.VMEM), *pieces, *([add] if which else []))
 
 
 def ring_pairs(shift, first):
@@ -461,7 +478,10 @@
 def gather_rest(line):
     both = ("sp", "tp")
     block = jnp.concatenate(line, axis=0)
-    mine = [block] + [lax.ppermute(block, both, ring_pairs(k, False)) for k in (1, 2, 3)]
+    return [block] + [lax.ppermute(block, both, ring_pairs(k, False)) for k in (1, 2, 3)]
+
+
+def with_partner(mine):
     swap = [(i, i ^ 1) for i in range(8)]
     return mine + [lax.ppermute(piece, "tp", swap) for piece in mine]
 
@@ -494,13 +514,15 @@
     *line, head, tail = lax.optimization_barrier((*line, head, tail))
     before = lax.ppermute(tail, "sp", up)
     after = lax.ppermute(head, "sp", down)
-    pieces = gather_rest(line)
-    y_pool = pool_branch(inputs, w_pool, pool_mix, before, after)
+    y_pool, scale = pool_branch(inputs, w_pool, pool_mix, before, after)
+    *line, y_pool = lax.optimization_barrier((*line, y_pool))
+    mine = gather_rest(line)
     pool_rows = lax.all_to_all(y_pool, "tp", split_axis=0, concat_axis=0, tiled=True)
     y_attn, lse = attn_branch(
-        sink_logit, inputs, w_attn, query_gain[None, :], key_gain[None, :], before, after, y_pool
+        sink_logit, inputs, scale, w_attn, query_gain[None, :], key_gain[None, :], before, after
     )
-    y_attn, pool_rows = lax.optimization_barrier((y_attn, pool_rows))
+    y_attn, pool_rows, *mine = lax.optimization_barrier((y_attn, pool_rows, *mine))
+    pieces = with_partner(mine)
     attn_rows = lax.all_to_all(y_attn, "tp", split_axis=0, concat_axis=0, tiled=True)
     partial = half_matmul(0, pool_rows, pieces)
     mixed = half_matmul(1, attn_rows, pieces, partial)

time: 121 us -> 106 us (0.88); the launches traced: 119 us -> 105 us
  starting transfers between devices: 38 us -> 27 us
  Pallas kernels: 61.6 us -> 58.1 us
  waiting for transfers between devices: 15.7 us -> 17.4 us
    ppermute x4, starting transfers between devices: 12.1 us -> 1.18 us  [with_partner(): return mine + [lax.ppermute(piece, 'tp', swap) for piece in mine]]
    ppermute x1, waiting for transfers between devices: 0.01 us -> 6.37 us  [body(): after = lax.ppermute(head, 'sp', down)]
    ppermute x1, waiting for transfers between devices: 7.13 us -> 0.96 us  [body(): before = lax.ppermute(tail, 'sp', up)]
    pallas_call x1, Pallas kernels: 24 us -> 22.3 us  [attn_branch(): pl.pallas_call(attn_kernel, grid=(blocks + 1,), in_specs=[pl.BlockSpec(me...]
    ppermute x4, waiting for transfers between devices: 0.01 us -> 1.57 us  [with_partner(): return mine + [lax.ppermute(piece, 'tp', swap) for piece in mine]]
    pallas_call x2, Pallas kernels: 15.3 us -> 13.8 us  [half_matmul(): pl.pallas_call(functools.partial(half_kernel, which), grid=(steps,), in_s...]
  transfers between devices with their start and end apart: 14 -> 14, of which waited for: 2 -> 6; matrix products, arithmetic and copies ran while one was open for 0% -> 0% of each run, Pallas kernels for 45% -> 34%
where the time goes in v2:
time: 106 us; the launch traced here: 105 us
  Pallas kernels  58.1 us (55%)
  starting transfers between devices  27 us (25%)
  waiting for transfers between devices  17.4 us (16%)
    pallas_call x1, Pallas kernels, attn_branch(): pl.pallas_call(attn_kernel, grid=(blocks + 1,), in_specs=[pl.BlockSpec(me...  22.3 us
    pallas_call x1, Pallas kernels, pool_branch(): pl.pallas_call(pool_kernel, grid=(blocks + 1,), in_specs=[pl.BlockSpec(me...  15 us
    pallas_call x2, Pallas kernels, half_matmul(): pl.pallas_call(functools.partial(half_kernel, which), grid=(steps,), in_s...  13.8 us
    all_to_all x1, waiting for transfers between devices, body(): lax.all_to_all(y_attn, 'tp', split_axis=0, concat_axis=0, tiled=True)  8.16 us
    pallas_call x1, Pallas kernels, first_rows(): pl.pallas_call(first_kernel, grid=(4,), in_specs=[pl.BlockSpec((half, 4,...  7.05 us
    ppermute x1, waiting for transfers between devices, body(): after = lax.ppermute(head, 'sp', down)  6.37 us
    ppermute x1, starting transfers between devices, body(): before = lax.ppermute(tail, 'sp', up)  5.88 us
    ppermute x3, starting transfers between devices, gather_rest(): lax.ppermute(block, both, ring_pairs(k, False))  5.07 us
  transfers between devices with their start and end apart: 14, of which 6 were waited for; matrix products, arithmetic and copies ran while one was open for 0% of the time, Pallas kernels for 34%

profile of v2, /device:TPU:24, one launch (start us, length us, event | category | flops | bytes accessed | tf_op | source)
XLA Modules:
  0.0 105.1 jit_solution(5932380344290101573)
XLA Ops:
  0.6 1.0 broadcast_select_fusion
  1.6 0.8 collective-permute-start.2
  2.4 0.8 collective-permute-start.1
  3.3 2.3 %collective-permute-start = (bf16[64,2048]{1,0:T(8,128)(2,1)S(1)}, bf16[64,2048]{1,0:T(8,128)(2,1)S(1)}, u32[]{:S(2)}, u32[]{:S(2)}) collective-permute-start(bf16[64,2048]{1,0:T(8,128)(2,1)S(1)} %broadcast_select_fusion), channel_id=1, source_target_pairs={{0,8},{1,33},{2,10},{3,35},{4,12},{5,37},{6,14},{7,39},{8,16},{9,4... | collective-permute-start | bytes 786440 | tf_op jit(solution)/shard_map/ppermute | solution.py:475
  5.6 7.1 %first_rows.1 = (bf16[4,136,128]{2,1,0:T(8,128)(2,1)}, bf16[4,136,128]{2,1,0:T(8,128)(2,1)}, bf16[2048,256]{1,0:T(8,128)(2,1)}, bf16[2048,512]{1,0:T(8,128)(2,1)}) custom-call(bf16[1024,4,2048]{2,1,0:T(4,128)(2,1)} %x_ref.5, f32[1,2048]{1,0:T(1,128)} %bitcast.8, bf16[2048,128]{1,0:T(8,128)(2,1)} %pool_ref.1, bf16[2048,128]{1,0:T(8,128)(2,1)} %pgate_ref.1, ...), custom_call_target="tpu_custom_call" | custom-call | flops 1073741824 | bytes 12582912 | tf_op jit(solution)/shard_map/first_rows/pallas_call | solution.py:96
  12.6 0.0 collective-permute-done.2
  12.6 0.0 collective-permute-done.1
  12.7 0.3 collective-permute-done
  13.0 5.9 %collective-permute-start.3 = (bf16[4,136,128]{2,1,0:T(8,128)(2,1)}, bf16[4,136,128]{2,1,0:T(8,128)(2,1)S(1)}, u32[]{:S(2)}, u32[]{:S(2)}) collective-permute-start(bf16[4,136,128]{2,1,0:T(8,128)(2,1)} %get-tuple-element.30), channel_id=1, source_target_pairs={{0,8},{8,16},{16,24},{24,32},{32,40},{40,48},{48,56},{56,64},{64,7... | collective-permute-start | bytes 417800 | tf_op jit(solution)/shard_map/ppermute | solution.py:515
  18.9 1.9 %collective-permute-start.4 = (bf16[4,136,128]{2,1,0:T(8,128)(2,1)}, bf16[4,136,128]{2,1,0:T(8,128)(2,1)S(1)}, u32[]{:S(2)}, u32[]{:S(2)}) collective-permute-start(bf16[4,136,128]{2,1,0:T(8,128)(2,1)} %get-tuple-element.31), channel_id=1, source_target_pairs={{8,0},{16,8},{24,16},{32,24},{40,32},{48,40},{56,48},{64,56},{72,6... | collective-permute-start | bytes 417800 | tf_op jit(solution)/shard_map/ppermute | solution.py:516
  20.8 1.0 collective-permute-done.3.before_ref
  21.8 0.0 copy-start.1
  21.8 6.4 %collective-permute-done.4.after_ref = bf16[4,136,128]{2,1,0:T(8,128)(2,1)S(1)} collective-permute-done((bf16[4,136,128]{2,1,0:T(8,128)(2,1)}, bf16[4,136,128]{2,1,0:T(8,128)(2,1)S(1)}, u32[]{:S(2)}, u32[]{:S(2)}) %collective-permute-start.4) | collective-permute-done | bytes 139296 | tf_op jit(solution)/shard_map/ppermute | solution.py:516
  28.2 0.0 copy-start.2
  28.2 0.0 copy-done.1
  28.2 0.6 copy-done.2
  28.8 15.0 %pool_branch.1 = (bf16[8,512,128]{2,1,0:T(8,128)(2,1)}, f32[4096,128]{1,0:T(8,128)}) custom-call(bf16[1024,4,2048]{2,1,0:T(4,128)(2,1)} %x_ref.5, bf16[2048,256]{1,0:T(8,128)(2,1)} %get-tuple-element.27.w_ref, bf16[1,128,128]{2,1,0:T(8,128)(2,1)} %mix_ref.1, bf16[4,136,128]{2,1,0:T(8,128)(2,1)} %copy-done.1, bf16[4,136,128]{2,1,0:T(8,128)(2,1)} %copy-done.2), custom_call_target="tpu_custom_call" | custom-call | flops 4294967296 | bytes 18874368 | tf_op jit(solution)/shard_map/pool_branch/pallas_call | solution.py:210
  43.9 0.0 copy-start
  43.9 0.1 collective-permute-start.7
  44.0 4.0 %collective-permute-start.6 = (bf16[256,2048]{1,0:T(8,128)(2,1)S(1)}, bf16[256,2048]{1,0:T(8,128)(2,1)}, u32[]{:S(2)}, u32[]{:S(2)}) collective-permute-start(bf16[256,2048]{1,0:T(8,128)(2,1)S(1)} %constant_dynamic-update-slice_fusion.rest_0_), channel_id=1, source_target_pairs={{0,64},{1,17},{2,66},{3,19},{4,68},{5,21},{6,70},{7,23},{8,72},{9,... | collective-permute-start | bytes 3145736 | tf_op jit(solution)/shard_map/ppermute | solution.py:481
  48.0 1.0 collective-permute-start.5
  49.0 4.3 %all-to-all-start = ((bf16[8,512,128]{2,1,0:T(8,128)(2,1)}), bf16[8,512,128]{2,1,0:T(8,128)(2,1)S(1)}, u32[]{:S(2)}, u32[]{:S(2)}) async-start(bf16[8,512,128]{2,1,0:T(8,128)(2,1)} %get-tuple-element.40), calls=%async_computation | async-start | bytes 2097152 | tf_op jit(solution)/shard_map/all_to_all | solution.py:520
  53.3 22.3 %attn_branch.1 = (bf16[8,512,128]{2,1,0:T(8,128)(2,1)}, f32[4,2,1024]{2,1,0:T(2,128)}) custom-call(f32[2]{0:T(128)} %sink_ref.1, bf16[1024,4,2048]{2,1,0:T(4,128)(2,1)} %x_ref.5, f32[4096,128]{1,0:T(8,128)} %get-tuple-element.32.scale_ref, bf16[2048,512]{1,0:T(8,128)(2,1)} %get-tuple-element.33.w_ref, f32[1,64]{1,0:T(1,128)} %bitcast.9, f32[1,64]{1,0:T(1,128)} %bitcast.10, ...), custom_call_target="tpu_custom_call" | custom-call | flops 12884901888 | bytes 20971520 | tf_op jit(solution)/shard_map/attn_branch/pallas_call | solution.py:349
  75.6 0.0 all-to-all-done.y_ref
  75.6 0.0 collective-permute-done.7.rest_3_
  75.6 0.0 collective-permute-done.6.rest_2_
  75.6 0.0 collective-permute-done.5.rest_1_
  75.6 0.0 copy-done
  75.6 0.6 collective-permute-start.8
  76.2 0.1 collective-permute-start.9
  76.3 0.4 collective-permute-start.10
  76.7 0.1 collective-permute-start.11
  76.8 4.7 %all-to-all-start.1 = ((bf16[8,512,128]{2,1,0:T(8,128)(2,1)}), bf16[8,512,128]{2,1,0:T(8,128)(2,1)S(1)}, u32[]{:S(2)}, u32[]{:S(2)}) async-start(bf16[8,512,128]{2,1,0:T(8,128)(2,1)} %get-tuple-element.45), calls=%async_computation.1 | async-start | bytes 2097152 | tf_op jit(solution)/shard_map/all_to_all | solution.py:526
  81.6 0.0 collective-permute-done.8.rest_4_
  81.6 0.0 collective-permute-done.9.rest_5_
  81.6 0.1 collective-permute-done.10.rest_6_
  81.6 1.5 %collective-permute-done.11.rest_7_ = bf16[256,2048]{1,0:T(8,128)(2,1)} collective-permute-done((bf16[256,2048]{1,0:T(8,128)(2,1)}, bf16[256,2048]{1,0:T(8,128)(2,1)}, u32[]{:S(2)}, u32[]{:S(2)}) %collective-permute-start.11) | collective-permute-done | bytes 1048608 | tf_op jit(solution)/shard_map/ppermute | solution.py:486
  83.1 6.2 %shard_map.149.rest_8_ = f32[512,2048]{1,0:T(8,128)} custom-call(bf16[8,512,128]{2,1,0:T(8,128)(2,1)S(1)} %all-to-all-done.y_ref, bf16[256,2048]{1,0:T(8,128)(2,1)} %copy-done, bf16[256,2048]{1,0:T(8,128)(2,1)} %collective-permute-done.5.rest_1_, bf16[256,2048]{1,0:T(8,128)(2,1)} %collective-permute-done.6.rest_2_, ...), custom_call_target="tpu_custom_call" | custom-call | flops 2147483648 | bytes 8388608 | tf_op jit(solution)/shard_map/pallas_call | solution.py:444
  89.3 8.2 %all-to-all-done.1.y_ref = bf16[8,512,128]{2,1,0:T(8,128)(2,1)S(1)} async-done(((bf16[8,512,128]{2,1,0:T(8,128)(2,1)}), bf16[8,512,128]{2,1,0:T(8,128)(2,1)S(1)}, u32[]{:S(2)}, u32[]{:S(2)}) %all-to-all-start.1) | async-done | bytes 1048608 | tf_op jit(solution)/shard_map/all_to_all | solution.py:526
  97.5 7.6 %shard_map.150 = bf16[128,4,2048]{2,1,0:T(4,128)(2,1)} custom-call(bf16[8,512,128]{2,1,0:T(8,128)(2,1)S(1)} %all-to-all-done.1.y_ref, bf16[256,2048]{1,0:T(8,128)(2,1)} %copy-done, bf16[256,2048]{1,0:T(8,128)(2,1)} %collective-permute-done.5.rest_1_, bf16[256,2048]{1,0:T(8,128)(2,1)} %collective-permute-done.6.rest_2_, ...), custom_call_target="tpu_custom_call" | custom-call | flops 2147483648 | bytes 8388608 | tf_op jit(solution)/shard_map/pallas_call | solution.py:444
  (4 shorter events, 0.1 us)
Async XLA Ops:
  1.6 11.0 %collective-permute-start.2 = (bf16[64,2048]{1,0:T(8,128)(2,1)S(1)}, bf16[64,2048]{1,0:T(8,128)(2,1)S(1)}, u32[]{:S(2)}, u32[]{:S(2)}) collective-permute-start(bf16[64,2048]{1,0:T(8,128)(2,1)S(1)} %broadcast_select_fusion), channel_id=1, source_target_pairs={{0,24},{1,97},{2,26},{3,99},{4,28},{5,101},{6,30},{7,103},{8,0},{9... | collective-permute-start | bytes 786440 | tf_op jit(solution)/shard_map/ppermute | solution.py:475
  2.4 10.2 %collective-permute-start.1 = (bf16[64,2048]{1,0:T(8,128)(2,1)S(1)}, bf16[64,2048]{1,0:T(8,128)(2,1)S(1)}, u32[]{:S(2)}, u32[]{:S(2)}) collective-permute-start(bf16[64,2048]{1,0:T(8,128)(2,1)S(1)} %broadcast_select_fusion), channel_id=1, source_target_pairs={{0,16},{1,65},{2,18},{3,67},{4,20},{5,69},{6,22},{7,71},{8,24},{9,... | collective-permute-start | bytes 786440 | tf_op jit(solution)/shard_map/ppermute | solution.py:475
  3.3 9.7 %collective-permute-start = (bf16[64,2048]{1,0:T(8,128)(2,1)S(1)}, bf16[64,2048]{1,0:T(8,128)(2,1)S(1)}, u32[]{:S(2)}, u32[]{:S(2)}) collective-permute-start(bf16[64,2048]{1,0:T(8,128)(2,1)S(1)} %broadcast_select_fusion), channel_id=1, source_target_pairs={{0,8},{1,33},{2,10},{3,35},{4,12},{5,37},{6,14},{7,39},{8,16},{9,4... | collective-permute-start | bytes 786440 | tf_op jit(solution)/shard_map/ppermute | solution.py:475
  13.0 8.8 %collective-permute-start.3 = (bf16[4,136,128]{2,1,0:T(8,128)(2,1)}, bf16[4,136,128]{2,1,0:T(8,128)(2,1)S(1)}, u32[]{:S(2)}, u32[]{:S(2)}) collective-permute-start(bf16[4,136,128]{2,1,0:T(8,128)(2,1)} %get-tuple-element.30), channel_id=1, source_target_pairs={{0,8},{8,16},{16,24},{24,32},{32,40},{40,48},{48,56},{56,64},{64,7... | collective-permute-start | bytes 417800 | tf_op jit(solution)/shard_map/ppermute | solution.py:515
  18.9 9.3 %collective-permute-start.4 = (bf16[4,136,128]{2,1,0:T(8,128)(2,1)}, bf16[4,136,128]{2,1,0:T(8,128)(2,1)S(1)}, u32[]{:S(2)}, u32[]{:S(2)}) collective-permute-start(bf16[4,136,128]{2,1,0:T(8,128)(2,1)} %get-tuple-element.31), channel_id=1, source_target_pairs={{8,0},{16,8},{24,16},{32,24},{40,32},{48,40},{56,48},{64,56},{72,6... | collective-permute-start | bytes 417800 | tf_op jit(solution)/shard_map/ppermute | solution.py:516
  21.8 6.4 %copy-start.1 = (bf16[4,136,128]{2,1,0:T(8,128)(2,1)}, bf16[4,136,128]{2,1,0:T(8,128)(2,1)S(1)}, u32[]{:S(2)}) copy-start(bf16[4,136,128]{2,1,0:T(8,128)(2,1)S(1)} %collective-permute-done.3.before_ref) | copy-start | bytes 417796
  28.2 0.7 copy-start.2
  43.9 31.7 %copy-start = (bf16[256,2048]{1,0:T(8,128)(2,1)}, bf16[256,2048]{1,0:T(8,128)(2,1)S(1)}, u32[]{:S(2)}) copy-start(bf16[256,2048]{1,0:T(8,128)(2,1)S(1)} %constant_dynamic-update-slice_fusion.rest_0_) | copy-start | bytes 3145732
  43.9 31.7 %collective-permute-start.7 = (bf16[256,2048]{1,0:T(8,128)(2,1)S(1)}, bf16[256,2048]{1,0:T(8,128)(2,1)}, u32[]{:S(2)}, u32[]{:S(2)}) collective-permute-start(bf16[256,2048]{1,0:T(8,128)(2,1)S(1)} %constant_dynamic-update-slice_fusion.rest_0_), channel_id=1, source_target_pairs={{0,96},{1,25},{2,98},{3,27},{4,100},{5,29},{6,102},{7,31},{8,104},... | collective-permute-start | bytes 3145736 | tf_op jit(solution)/shard_map/ppermute | solution.py:481
  44.0 31.6 %collective-permute-start.6 = (bf16[256,2048]{1,0:T(8,128)(2,1)S(1)}, bf16[256,2048]{1,0:T(8,128)(2,1)}, u32[]{:S(2)}, u32[]{:S(2)}) collective-permute-start(bf16[256,2048]{1,0:T(8,128)(2,1)S(1)} %constant_dynamic-update-slice_fusion.rest_0_), channel_id=1, source_target_pairs={{0,64},{1,17},{2,66},{3,19},{4,68},{5,21},{6,70},{7,23},{8,72},{9,... | collective-permute-start | bytes 3145736 | tf_op jit(solution)/shard_map/ppermute | solution.py:481
  48.0 27.7 %collective-permute-start.5 = (bf16[256,2048]{1,0:T(8,128)(2,1)S(1)}, bf16[256,2048]{1,0:T(8,128)(2,1)}, u32[]{:S(2)}, u32[]{:S(2)}) collective-permute-start(bf16[256,2048]{1,0:T(8,128)(2,1)S(1)} %constant_dynamic-update-slice_fusion.rest_0_), channel_id=1, source_target_pairs={{0,32},{1,9},{2,34},{3,11},{4,36},{5,13},{6,38},{7,15},{8,40},{9,1... | collective-permute-start | bytes 3145736 | tf_op jit(solution)/shard_map/ppermute | solution.py:481
  49.0 26.6 %all-to-all-start = ((bf16[8,512,128]{2,1,0:T(8,128)(2,1)}), bf16[8,512,128]{2,1,0:T(8,128)(2,1)S(1)}, u32[]{:S(2)}, u32[]{:S(2)}) async-start(bf16[8,512,128]{2,1,0:T(8,128)(2,1)} %get-tuple-element.40), calls=%async_computation | async-start | bytes 2097152 | tf_op jit(solution)/shard_map/all_to_all | solution.py:520
  75.6 5.9 %collective-permute-start.8 = (bf16[256,2048]{1,0:T(8,128)(2,1)S(1)}, bf16[256,2048]{1,0:T(8,128)(2,1)}, u32[]{:S(2)}, u32[]{:S(2)}) collective-permute-start(bf16[256,2048]{1,0:T(8,128)(2,1)S(1)} %constant_dynamic-update-slice_fusion.rest_0_), channel_id=1, source_target_pairs={{0,1},{1,0},{2,3},{3,2},{4,5},{5,4},{6,7},{7,6},{8,9},{9,8},{10,11... | collective-permute-start | bytes 3145736 | tf_op jit(solution)/shard_map/ppermute | solution.py:486
  76.2 5.3 %collective-permute-start.9 = (bf16[256,2048]{1,0:T(8,128)(2,1)}, bf16[256,2048]{1,0:T(8,128)(2,1)}, u32[]{:S(2)}, u32[]{:S(2)}) collective-permute-start(bf16[256,2048]{1,0:T(8,128)(2,1)} %collective-permute-done.5.rest_1_), channel_id=1, source_target_pairs={{0,1},{1,0},{2,3},{3,2},{4,5},{5,4},{6,7},{7,6},{8,9},{9,8},{10,11... | collective-permute-start | bytes 3145736 | tf_op jit(solution)/shard_map/ppermute | solution.py:486
  76.3 5.3 %collective-permute-start.10 = (bf16[256,2048]{1,0:T(8,128)(2,1)}, bf16[256,2048]{1,0:T(8,128)(2,1)}, u32[]{:S(2)}, u32[]{:S(2)}) collective-permute-start(bf16[256,2048]{1,0:T(8,128)(2,1)} %collective-permute-done.6.rest_2_), channel_id=1, source_target_pairs={{0,1},{1,0},{2,3},{3,2},{4,5},{5,4},{6,7},{7,6},{8,9},{9,8},{10,11... | collective-permute-start | bytes 3145736 | tf_op jit(solution)/shard_map/ppermute | solution.py:486
  76.7 6.4 %collective-permute-start.11 = (bf16[256,2048]{1,0:T(8,128)(2,1)}, bf16[256,2048]{1,0:T(8,128)(2,1)}, u32[]{:S(2)}, u32[]{:S(2)}) collective-permute-start(bf16[256,2048]{1,0:T(8,128)(2,1)} %collective-permute-done.7.rest_3_), channel_id=1, source_target_pairs={{0,1},{1,0},{2,3},{3,2},{4,5},{5,4},{6,7},{7,6},{8,9},{9,8},{10,11... | collective-permute-start | bytes 3145736 | tf_op jit(solution)/shard_map/ppermute | solution.py:486
  76.8 20.7 %all-to-all-start.1 = ((bf16[8,512,128]{2,1,0:T(8,128)(2,1)}), bf16[8,512,128]{2,1,0:T(8,128)(2,1)S(1)}, u32[]{:S(2)}, u32[]{:S(2)}) async-start(bf16[8,512,128]{2,1,0:T(8,128)(2,1)} %get-tuple-element.45), calls=%async_computation.1 | async-start | bytes 2097152 | tf_op jit(solution)/shard_map/all_to_all | solution.py:526

commit v3 on v2

--- a/solution.py
+++ b/solution.py
@@ -69,34 +69,31 @@
     cols = jnp.dot(x, w_edge[...], preferred_element_type=F32) * row_scale(x)
     scr[0] = cols[:, :128]
     scr[1] = cols[:, 128:]
-    for n in range(4):
-        out = head_ref if n < 2 else tail_ref
-        part = n % 2
+    for n in range(2):
+        out = (head_ref, tail_ref)[n]
 
         @pl.when(step == n)
-        def _(n=n, out=out, part=part):
+        def _(n=n, out=out):
+            begin = n * 4 * (half - REACH)
             for s in range(4):
-                rows = scr[1, pl.ds(s, half, stride=4), :]
-                out[s, part * half : (part + 1) * half, :] = rows.astype(BF16)
-                if n == 0:
-                    out[s, 128 : 128 + REACH, :] = scr[0, pl.ds(s, REACH, stride=4), :].astype(BF16)
-                if n == 3 and s == 0:
-                    for copy in leave:
-                        copy.wait()
-                if n == 3:
-                    rows = scr[0, pl.ds(s + 4 * (half - REACH), REACH, stride=4), :]
-                    out[s, 128 : 128 + REACH, :] = rows.astype(BF16)
+                out[s, 0:half, :] = scr[1, pl.ds(s, half, stride=4), :].astype(BF16)
+                out[s, half : half + REACH, :] = scr[0, pl.ds(s + begin, REACH, stride=4), :].astype(BF16)
+
+    @pl.when(step == 1)
+    def _():
+        for copy in leave:
+            copy.wait()
 
 
 def first_rows(x, gain, pool, pgate, query, keyt, valuet, agate):
-    half = 64
+    half = BLOCK
     width = x.shape[2]
     last = x.shape[0] // half
     whole = [gain, pool, pgate, query, keyt, valuet, agate]
     return pl.pallas_call(
         first_kernel,
-        grid=(4,),
-        in_specs=[pl.BlockSpec((half, 4, width), lambda i: (i + (last - 4) * (i // 2), 0, 0))]
+        grid=(2,),
+        in_specs=[pl.BlockSpec((half, 4, width), lambda i: (i * (last - 1), 0, 0))]
         + [pl.BlockSpec(a.shape, lambda i: (0, 0)) for a in whole],
         out_specs=(
             pl.BlockSpec((4, 136, 128), lambda i: (0, 0, 0)),
@@ -124,37 +121,44 @@
     )(x, *whole)
 
 
-def pool_kernel(x_ref, w_ref, mix_ref, before_ref, after_ref, y_ref, scale_ref, pool, gate, inverse, xs, xv, sems):
-    step = pl.program_id(0)
-    blocks = pl.num_programs(0) - 1
+def pool_kernel(
+    x_ref, w_hbm, mix_ref, before_ref, after_ref, y_hbm, scale_hbm, pool, gate, inverse, xs, xv, w_ref, yv, sv, sems, w_sem
+):
     rows = BLOCK * 4
+    blocks = xv.shape[0] // BLOCK
     pad = 64
     total_rows = blocks * rows
-    length_blocks = xv.shape[0] // BLOCK
     power = lax.axis_index("tp") % 4
     half = jnp.left_shift(jnp.int32(1), power)
 
     def fetch(n):
         span = pl.ds(n * BLOCK, BLOCK)
-        return pltpu.make_async_copy(x_ref.at[span], xv.at[span], sems.at[n])
-
-    @pl.when(step == 0)
-    def _():
-        for n in range(length_blocks):
-            fetch(n).start()
-        for s in range(4):
-            pool[pl.ds(pad - 4 * REACH + s, REACH, stride=4), :] = before_ref[s, 128 : 128 + REACH, :].astype(F32)
-            pool[pl.ds(pad + total_rows + s, REACH, stride=4), :] = after_ref[s, 128 : 128 + REACH, :].astype(F32)
-        length = blocks * BLOCK
-        begin = lax.axis_index("sp") * length
-        total = lax.axis_size("sp") * length
-        for k in range(3):
-            where = (0, BLOCK, length - BLOCK)[k]
-            position = begin + where + lax.broadcasted_iota(jnp.int32, (rows, 128), 0) // 4
-            count = jnp.minimum(position + half - 1, total - 1) - jnp.maximum(position - half, 0) + 1
-            inverse[k] = 1.0 / count.astype(F32)
-
-    def finish():
+        return pltpu.make_async_copy(x_ref.at[span], xv.at[span], sems.at[0, n])
+
+    def leave(n):
+        span = pl.ds(pl.multiple_of(n * rows, rows), rows)
+        return (
+            pltpu.make_async_copy(yv.at[n], y_hbm.at[n], sems.at[1, n]),
+            pltpu.make_async_copy(sv.at[n], scale_hbm.at[span], sems.at[2, n]),
+        )
+
+    weights = pltpu.make_async_copy(w_hbm, w_ref, w_sem)
+    weights.start()
+    fetch(0).start()
+    fetch(1).start()
+    for s in range(4):
+        pool[pl.ds(pad - 4 * REACH + s, REACH, stride=4), :] = before_ref[s, 128 : 128 + REACH, :].astype(F32)
+        pool[pl.ds(pad + total_rows + s, REACH, stride=4), :] = after_ref[s, 128 : 128 + REACH, :].astype(F32)
+    length = blocks * BLOCK
+    begin = lax.axis_index("sp") * length
+    total = lax.axis_size("sp") * length
+    for k in range(3):
+        where = (0, BLOCK, length - BLOCK)[k]
+        position = begin + where + lax.broadcasted_iota(jnp.int32, (rows, 128), 0) // 4
+        count = jnp.minimum(position + half - 1, total - 1) - jnp.maximum(position - half, 0) + 1
+        inverse[k] = 1.0 / count.astype(F32)
+
+    def finish(step):
         at = pl.multiple_of((step - 1) * rows, rows)
         base = pad + at
         reach = 4 * REACH
@@ -176,51 +180,50 @@
         kind = jnp.where(step == 1, 0, jnp.where(step == blocks, 2, 1))
         pooled = (sums * inverse[kind] - window[reach : reach + rows]).astype(BF16)
         mixed = jnp.dot(pooled, mix_ref[0], preferred_element_type=F32)
-        y_ref[0] = (mixed * silu(gate[pl.ds(at, rows), :])).astype(BF16)
-
-    def project():
+        yv[step - 1] = (mixed * silu(gate[pl.ds(at, rows), :])).astype(BF16)
+        for copy in leave(step - 1):
+            copy.start()
+
+    def project(step):
         fetch(step).wait()
+
+        @pl.when(step + 2 < blocks)
+        def _():
+            fetch(step + 2).start()
+
         xs[...] = xv.at[pl.ds(pl.multiple_of(step * BLOCK, BLOCK), BLOCK)].reshape(rows, xv.shape[2])[...]
         x = xs[...]
         scale = row_scale(x)
-        scale_ref[...] = jnp.broadcast_to(scale, (rows, 128))
+        sv[step] = jnp.broadcast_to(scale, (rows, 128))
         both = jnp.dot(x, w_ref[...], preferred_element_type=F32) * scale
         at = pl.multiple_of(step * rows, rows)
         pool[pl.ds(pad + at, rows), :] = both[:, :128]
         gate[pl.ds(at, rows), :] = both[:, 128:]
 
-    @pl.when(step == 0)
-    def _():
-        project()
-
-    @pl.when((step > 0) & (step < blocks))
-    def _():
-        project()
-        finish()
-
-    @pl.when(step == blocks)
-    def _():
-        finish()
+    weights.wait()
+    project(0)
+
+    @pl.loop(1, blocks)
+    def _(step):
+        project(step)
+        finish(step)
+
+    finish(blocks)
+    for n in range(blocks):
+        for copy in leave(n):
+            copy.wait()
 
 
 def pool_branch(x, w, mix, before, after):
     length, _, width = x.shape
     blocks = length // BLOCK
     rows = BLOCK * 4
+    whole = pl.BlockSpec(memory_space=pltpu.VMEM)
+    far = pl.BlockSpec(memory_space=pl.ANY)
     return pl.pallas_call(
         pool_kernel,
-        grid=(blocks + 1,),
-        in_specs=[
-            pl.BlockSpec(memory_space=pl.ANY),
-            pl.BlockSpec(w.shape, lambda i: (0, 0)),
-            pl.BlockSpec(mix.shape, lambda i: (0, 0, 0)),
-            pl.BlockSpec(before.shape, lambda i: (0, 0, 0)),
-            pl.BlockSpec(after.shape, lambda i: (0, 0, 0)),
-        ],
-        out_specs=(
-            pl.BlockSpec((1, rows, 128), lambda i: (jnp.maximum(i - 1, 0), 0, 0)),
-            pl.BlockSpec((rows, 128), lambda i: (jnp.minimum(i, blocks - 1), 0)),
-        ),
+        in_specs=[far, far, whole, whole, whole],
+        out_specs=(far, far),
         out_shape=(
             jax.ShapeDtypeStruct((blocks, rows, 128), BF16),
             jax.ShapeDtypeStruct((length * 4, 128), F32),
@@ -231,9 +234,12 @@
             pltpu.VMEM((3, rows, 128), F32),
             pltpu.VMEM((rows, width), BF16),
             pltpu.VMEM(x.shape, BF16),
-            pltpu.SemaphoreType.DMA((blocks,)),
+            pltpu.VMEM(w.shape, BF16),
+            pltpu.VMEM((blocks, rows, 128), BF16),
+            pltpu.VMEM((blocks, rows, 128), F32),
+            pltpu.SemaphoreType.DMA((3, blocks)),
+            pltpu.SemaphoreType.DMA,
         ],
-        compiler_params=pltpu.CompilerParams(dimension_semantics=("arbitrary",)),
         cost_estimate=pl.CostEstimate(flops=2 * 4096 * 2048 * 256, transcendentals=0, bytes_accessed=18 << 20),
         name="pool_branch",
     )(x, w, mix, before, after)
@@ -425,19 +431,19 @@
     lanes = jnp.concatenate([y_ref[j] for j in range(y_ref.shape[0])], axis=1)
     acc = jnp.dot(lanes, w[step], preferred_element_type=F32)
     if which == 0:
-        o_ref[...] = acc
+        o_ref[...] = acc.astype(BF16)
     else:
-        o_ref.reshape(rows, tile)[...] = (acc + add_ref[...]).astype(BF16)
+        o_ref.reshape(rows, tile)[...] = (acc + add_ref[...].astype(F32)).astype(BF16)
 
 
 def half_matmul(which, y, pieces, add=None):
     parts, rows, cols = y.shape
     width = pieces[0].shape[1]
-    tile = 512
+    tile = 1024
     steps = width // tile
     if which == 0:
         out_spec = pl.BlockSpec((rows, tile), lambda n: (0, n))
-        out_shape = jax.ShapeDtypeStruct((rows, width), F32)
+        out_shape = jax.ShapeDtypeStruct((rows, width), BF16)
     else:
         out_spec = pl.BlockSpec((rows // 4, 4, tile), lambda n: (0, 0, n))
         out_shape = jax.ShapeDtypeStruct((rows // 4, 4, width), BF16)

time: 106 us -> 103 us (0.972)
  Pallas kernels: 58.1 us -> 54.4 us
  waiting for transfers between devices: 17.4 us -> 19.2 us
    pallas_call x2, Pallas kernels: 22 us -> 20 us  [the longest x1 13.9 us: pool_branch(): pl.pallas_call(pool_kernel, in_specs=[far, far, whole, whole, whole], out...]
    pallas_call x2, Pallas kernels: 13.8 us -> 12.1 us  [half_matmul(): pl.pallas_call(functools.partial(half_kernel, which), grid=(steps,), in_s...]
  transfers between devices with their start and end apart: 14 -> 14, of which waited for: 6 -> 7; matrix products, arithmetic and copies ran while one was open for 0% -> 0% of each run, Pallas kernels for 34% -> 33%
where the time goes in v3:
time: 103 us
  Pallas kernels  54.4 us (53%)
  starting transfers between devices  27 us (26%)
  waiting for transfers between devices  19.2 us (19%)
    pallas_call x1, Pallas kernels, attn_branch(): pl.pallas_call(attn_kernel, grid=(blocks + 1,), in_specs=[pl.BlockSpec(me...  22.3 us
    pallas_call x1, Pallas kernels, pool_branch(): pl.pallas_call(pool_kernel, in_specs=[far, far, whole, whole, whole], out...  13.9 us
    pallas_call x2, Pallas kernels, half_matmul(): pl.pallas_call(functools.partial(half_kernel, which), grid=(steps,), in_s...  12.1 us
    all_to_all x1, waiting for transfers between devices, body(): lax.all_to_all(y_attn, 'tp', split_axis=0, concat_axis=0, tiled=True)  8.87 us
    ppermute x1, waiting for transfers between devices, body(): after = lax.ppermute(head, 'sp', down)  6.37 us
    pallas_call x1, Pallas kernels, first_rows(): pl.pallas_call(first_kernel, grid=(2,), in_specs=[pl.BlockSpec((half, 4,...  6.04 us
    ppermute x1, starting transfers between devices, body(): before = lax.ppermute(tail, 'sp', up)  5.88 us
    ppermute x3, starting transfers between devices, gather_rest(): lax.ppermute(block, both, ring_pairs(k, False))  5.07 us
  transfers between devices with their start and end apart: 14, of which 7 were waited for; matrix products, arithmetic and copies ran while one was open for 0% of the time, Pallas kernels for 33%

profile of v3, /device:TPU:24, one launch (start us, length us, event | category | flops | bytes accessed | tf_op | source)
XLA Modules:
  0.0 103.1 jit_solution(15971384328193690878)
XLA Ops:
  0.6 1.0 broadcast_select_fusion
  1.6 0.8 collective-permute-start.2
  2.4 0.8 collective-permute-start.1
  3.3 2.3 %collective-permute-start = (bf16[64,2048]{1,0:T(8,128)(2,1)S(1)}, bf16[64,2048]{1,0:T(8,128)(2,1)S(1)}, u32[]{:S(2)}, u32[]{:S(2)}) collective-permute-start(bf16[64,2048]{1,0:T(8,128)(2,1)S(1)} %broadcast_select_fusion), channel_id=1, source_target_pairs={{0,8},{1,33},{2,10},{3,35},{4,12},{5,37},{6,14},{7,39},{8,16},{9,4... | collective-permute-start | bytes 786440 | tf_op jit(solution)/shard_map/ppermute | solution.py:481
  5.6 6.0 %first_rows.1 = (bf16[4,136,128]{2,1,0:T(8,128)(2,1)}, bf16[4,136,128]{2,1,0:T(8,128)(2,1)}, bf16[2048,256]{1,0:T(8,128)(2,1)}, bf16[2048,512]{1,0:T(8,128)(2,1)}) custom-call(bf16[1024,4,2048]{2,1,0:T(4,128)(2,1)} %x_ref.5, f32[1,2048]{1,0:T(1,128)} %bitcast.8, bf16[2048,128]{1,0:T(8,128)(2,1)} %pool_ref.1, bf16[2048,128]{1,0:T(8,128)(2,1)} %pgate_ref.1, ...), custom_call_target="tpu_custom_call" | custom-call | flops 1073741824 | bytes 12582912 | tf_op jit(solution)/shard_map/first_rows/pallas_call | solution.py:93
  11.6 0.5 collective-permute-done.2
  12.1 0.0 collective-permute-done.1
  12.1 0.9 collective-permute-done
  13.0 5.9 %collective-permute-start.3 = (bf16[4,136,128]{2,1,0:T(8,128)(2,1)}, bf16[4,136,128]{2,1,0:T(8,128)(2,1)S(1)}, u32[]{:S(2)}, u32[]{:S(2)}) collective-permute-start(bf16[4,136,128]{2,1,0:T(8,128)(2,1)} %get-tuple-element.30), channel_id=1, source_target_pairs={{0,8},{8,16},{16,24},{24,32},{32,40},{40,48},{48,56},{56,64},{64,7... | collective-permute-start | bytes 417800 | tf_op jit(solution)/shard_map/ppermute | solution.py:521
  18.9 1.9 %collective-permute-start.4 = (bf16[4,136,128]{2,1,0:T(8,128)(2,1)}, bf16[4,136,128]{2,1,0:T(8,128)(2,1)S(1)}, u32[]{:S(2)}, u32[]{:S(2)}) collective-permute-start(bf16[4,136,128]{2,1,0:T(8,128)(2,1)} %get-tuple-element.31), channel_id=1, source_target_pairs={{8,0},{16,8},{24,16},{32,24},{40,32},{48,40},{56,48},{64,56},{72,6... | collective-permute-start | bytes 417800 | tf_op jit(solution)/shard_map/ppermute | solution.py:522
  20.8 1.0 collective-permute-done.3.before_ref
  21.8 0.0 copy-start.1
  21.8 6.4 %collective-permute-done.4.after_ref = bf16[4,136,128]{2,1,0:T(8,128)(2,1)S(1)} collective-permute-done((bf16[4,136,128]{2,1,0:T(8,128)(2,1)}, bf16[4,136,128]{2,1,0:T(8,128)(2,1)S(1)}, u32[]{:S(2)}, u32[]{:S(2)}) %collective-permute-start.4) | collective-permute-done | bytes 139296 | tf_op jit(solution)/shard_map/ppermute | solution.py:522
  28.2 0.0 copy-start.2
  28.2 0.0 copy-done.1
  28.2 0.7 copy-done.2
  28.8 13.9 %pool_branch.1 = (bf16[8,512,128]{2,1,0:T(8,128)(2,1)}, f32[4096,128]{1,0:T(8,128)}) custom-call(bf16[1024,4,2048]{2,1,0:T(4,128)(2,1)} %x_ref.5, bf16[2048,256]{1,0:T(8,128)(2,1)} %get-tuple-element.27.w_hbm, bf16[1,128,128]{2,1,0:T(8,128)(2,1)} %mix_ref.1, bf16[4,136,128]{2,1,0:T(8,128)(2,1)} %copy-done.1, bf16[4,136,128]{2,1,0:T(8,128)(2,1)} %copy-done.2), custom_call_target="tpu_custom_call" | custom-call | flops 4294967296 | bytes 18874368 | tf_op jit(solution)/shard_map/pool_branch/pallas_call | solution.py:223
  42.9 0.0 copy-start
  42.9 0.1 collective-permute-start.7
  43.0 4.0 %collective-permute-start.6 = (bf16[256,2048]{1,0:T(8,128)(2,1)S(1)}, bf16[256,2048]{1,0:T(8,128)(2,1)}, u32[]{:S(2)}, u32[]{:S(2)}) collective-permute-start(bf16[256,2048]{1,0:T(8,128)(2,1)S(1)} %constant_dynamic-update-slice_fusion.rest_0_), channel_id=1, source_target_pairs={{0,64},{1,17},{2,66},{3,19},{4,68},{5,21},{6,70},{7,23},{8,72},{9,... | collective-permute-start | bytes 3145736 | tf_op jit(solution)/shard_map/ppermute | solution.py:487
  46.9 1.0 collective-permute-start.5
  48.0 4.3 %all-to-all-start = ((bf16[8,512,128]{2,1,0:T(8,128)(2,1)}), bf16[8,512,128]{2,1,0:T(8,128)(2,1)S(1)}, u32[]{:S(2)}, u32[]{:S(2)}) async-start(bf16[8,512,128]{2,1,0:T(8,128)(2,1)} %get-tuple-element.40), calls=%async_computation | async-start | bytes 2097152 | tf_op jit(solution)/shard_map/all_to_all | solution.py:526
  52.3 22.3 %attn_branch.1 = (bf16[8,512,128]{2,1,0:T(8,128)(2,1)}, f32[4,2,1024]{2,1,0:T(2,128)}) custom-call(f32[2]{0:T(128)} %sink_ref.1, bf16[1024,4,2048]{2,1,0:T(4,128)(2,1)} %x_ref.5, f32[4096,128]{1,0:T(8,128)} %get-tuple-element.32.scale_ref, bf16[2048,512]{1,0:T(8,128)(2,1)} %get-tuple-element.33.w_ref, f32[1,64]{1,0:T(1,128)} %bitcast.9, f32[1,64]{1,0:T(1,128)} %bitcast.10, ...), custom_call_target="tpu_custom_call" | custom-call | flops 12884901888 | bytes 20971520 | tf_op jit(solution)/shard_map/attn_branch/pallas_call | solution.py:355
  74.6 0.0 all-to-all-done.y_ref
  74.6 0.0 collective-permute-done.7.rest_3_
  74.6 0.0 collective-permute-done.6.rest_2_
  74.6 0.0 collective-permute-done.5.rest_1_
  74.6 0.0 copy-done
  74.6 0.6 collective-permute-start.8
  75.2 0.1 collective-permute-start.9
  75.3 0.4 collective-permute-start.10
  75.7 0.1 collective-permute-start.11
  75.8 4.7 %all-to-all-start.1 = ((bf16[8,512,128]{2,1,0:T(8,128)(2,1)}), bf16[8,512,128]{2,1,0:T(8,128)(2,1)S(1)}, u32[]{:S(2)}, u32[]{:S(2)}) async-start(bf16[8,512,128]{2,1,0:T(8,128)(2,1)} %get-tuple-element.45), calls=%async_computation.1 | async-start | bytes 2097152 | tf_op jit(solution)/shard_map/all_to_all | solution.py:532
  80.5 0.0 collective-permute-done.8.rest_4_
  80.5 0.0 collective-permute-done.9.rest_5_
  80.6 0.1 collective-permute-done.10.rest_6_
  80.6 1.5 %collective-permute-done.11.rest_7_ = bf16[256,2048]{1,0:T(8,128)(2,1)} collective-permute-done((bf16[256,2048]{1,0:T(8,128)(2,1)}, bf16[256,2048]{1,0:T(8,128)(2,1)}, u32[]{:S(2)}, u32[]{:S(2)}) %collective-permute-start.11) | collective-permute-done | bytes 1048608 | tf_op jit(solution)/shard_map/ppermute | solution.py:492
  82.1 5.5 %shard_map.149.rest_8_ = bf16[512,2048]{1,0:T(8,128)(2,1)} custom-call(bf16[8,512,128]{2,1,0:T(8,128)(2,1)S(1)} %all-to-all-done.y_ref, bf16[256,2048]{1,0:T(8,128)(2,1)} %copy-done, bf16[256,2048]{1,0:T(8,128)(2,1)} %collective-permute-done.5.rest_1_, bf16[256,2048]{1,0:T(8,128)(2,1)} %collective-permute-done.6.rest_2_, ...), custom_call_target="tpu_custom_call" | custom-call | flops 2147483648 | bytes 8388608 | tf_op jit(solution)/shard_map/pallas_call | solution.py:450
  87.6 8.9 %all-to-all-done.1.y_ref = bf16[8,512,128]{2,1,0:T(8,128)(2,1)S(1)} async-done(((bf16[8,512,128]{2,1,0:T(8,128)(2,1)}), bf16[8,512,128]{2,1,0:T(8,128)(2,1)S(1)}, u32[]{:S(2)}, u32[]{:S(2)}) %all-to-all-start.1) | async-done | bytes 1048608 | tf_op jit(solution)/shard_map/all_to_all | solution.py:532
  96.5 6.7 %shard_map.150 = bf16[128,4,2048]{2,1,0:T(4,128)(2,1)} custom-call(bf16[8,512,128]{2,1,0:T(8,128)(2,1)S(1)} %all-to-all-done.1.y_ref, bf16[256,2048]{1,0:T(8,128)(2,1)} %copy-done, bf16[256,2048]{1,0:T(8,128)(2,1)} %collective-permute-done.5.rest_1_, bf16[256,2048]{1,0:T(8,128)(2,1)} %collective-permute-done.6.rest_2_, ...), custom_call_target="tpu_custom_call" | custom-call | flops 2147483648 | bytes 8388608 | tf_op jit(solution)/shard_map/pallas_call | solution.py:450
  (4 shorter events, 0.1 us)
Async XLA Ops:
  1.6 10.5 %collective-permute-start.2 = (bf16[64,2048]{1,0:T(8,128)(2,1)S(1)}, bf16[64,2048]{1,0:T(8,128)(2,1)S(1)}, u32[]{:S(2)}, u32[]{:S(2)}) collective-permute-start(bf16[64,2048]{1,0:T(8,128)(2,1)S(1)} %broadcast_select_fusion), channel_id=1, source_target_pairs={{0,24},{1,97},{2,26},{3,99},{4,28},{5,101},{6,30},{7,103},{8,0},{9... | collective-permute-start | bytes 786440 | tf_op jit(solution)/shard_map/ppermute | solution.py:481
  2.4 9.7 %collective-permute-start.1 = (bf16[64,2048]{1,0:T(8,128)(2,1)S(1)}, bf16[64,2048]{1,0:T(8,128)(2,1)S(1)}, u32[]{:S(2)}, u32[]{:S(2)}) collective-permute-start(bf16[64,2048]{1,0:T(8,128)(2,1)S(1)} %broadcast_select_fusion), channel_id=1, source_target_pairs={{0,16},{1,65},{2,18},{3,67},{4,20},{5,69},{6,22},{7,71},{8,24},{9,... | collective-permute-start | bytes 786440 | tf_op jit(solution)/shard_map/ppermute | solution.py:481
  3.3 9.7 %collective-permute-start = (bf16[64,2048]{1,0:T(8,128)(2,1)S(1)}, bf16[64,2048]{1,0:T(8,128)(2,1)S(1)}, u32[]{:S(2)}, u32[]{:S(2)}) collective-permute-start(bf16[64,2048]{1,0:T(8,128)(2,1)S(1)} %broadcast_select_fusion), channel_id=1, source_target_pairs={{0,8},{1,33},{2,10},{3,35},{4,12},{5,37},{6,14},{7,39},{8,16},{9,4... | collective-permute-start | bytes 786440 | tf_op jit(solution)/shard_map/ppermute | solution.py:481
  13.0 8.8 %collective-permute-start.3 = (bf16[4,136,128]{2,1,0:T(8,128)(2,1)}, bf16[4,136,128]{2,1,0:T(8,128)(2,1)S(1)}, u32[]{:S(2)}, u32[]{:S(2)}) collective-permute-start(bf16[4,136,128]{2,1,0:T(8,128)(2,1)} %get-tuple-element.30), channel_id=1, source_target_pairs={{0,8},{8,16},{16,24},{24,32},{32,40},{40,48},{48,56},{56,64},{64,7... | collective-permute-start | bytes 417800 | tf_op jit(solution)/shard_map/ppermute | solution.py:521
  18.9 9.3 %collective-permute-start.4 = (bf16[4,136,128]{2,1,0:T(8,128)(2,1)}, bf16[4,136,128]{2,1,0:T(8,128)(2,1)S(1)}, u32[]{:S(2)}, u32[]{:S(2)}) collective-permute-start(bf16[4,136,128]{2,1,0:T(8,128)(2,1)} %get-tuple-element.31), channel_id=1, source_target_pairs={{8,0},{16,8},{24,16},{32,24},{40,32},{48,40},{56,48},{64,56},{72,6... | collective-permute-start | bytes 417800 | tf_op jit(solution)/shard_map/ppermute | solution.py:522
  21.8 6.4 %copy-start.1 = (bf16[4,136,128]{2,1,0:T(8,128)(2,1)}, bf16[4,136,128]{2,1,0:T(8,128)(2,1)S(1)}, u32[]{:S(2)}) copy-start(bf16[4,136,128]{2,1,0:T(8,128)(2,1)S(1)} %collective-permute-done.3.before_ref) | copy-start | bytes 417796
  28.2 0.7 copy-start.2
  42.9 31.8 %copy-start = (bf16[256,2048]{1,0:T(8,128)(2,1)}, bf16[256,2048]{1,0:T(8,128)(2,1)S(1)}, u32[]{:S(2)}) copy-start(bf16[256,2048]{1,0:T(8,128)(2,1)S(1)} %constant_dynamic-update-slice_fusion.rest_0_) | copy-start | bytes 3145732
  42.9 31.7 %collective-permute-start.7 = (bf16[256,2048]{1,0:T(8,128)(2,1)S(1)}, bf16[256,2048]{1,0:T(8,128)(2,1)}, u32[]{:S(2)}, u32[]{:S(2)}) collective-permute-start(bf16[256,2048]{1,0:T(8,128)(2,1)S(1)} %constant_dynamic-update-slice_fusion.rest_0_), channel_id=1, source_target_pairs={{0,96},{1,25},{2,98},{3,27},{4,100},{5,29},{6,102},{7,31},{8,104},... | collective-permute-start | bytes 3145736 | tf_op jit(solution)/shard_map/ppermute | solution.py:487
  43.0 31.6 %collective-permute-start.6 = (bf16[256,2048]{1,0:T(8,128)(2,1)S(1)}, bf16[256,2048]{1,0:T(8,128)(2,1)}, u32[]{:S(2)}, u32[]{:S(2)}) collective-permute-start(bf16[256,2048]{1,0:T(8,128)(2,1)S(1)} %constant_dynamic-update-slice_fusion.rest_0_), channel_id=1, source_target_pairs={{0,64},{1,17},{2,66},{3,19},{4,68},{5,21},{6,70},{7,23},{8,72},{9,... | collective-permute-start | bytes 3145736 | tf_op jit(solution)/shard_map/ppermute | solution.py:487
  46.9 27.7 %collective-permute-start.5 = (bf16[256,2048]{1,0:T(8,128)(2,1)S(1)}, bf16[256,2048]{1,0:T(8,128)(2,1)}, u32[]{:S(2)}, u32[]{:S(2)}) collective-permute-start(bf16[256,2048]{1,0:T(8,128)(2,1)S(1)} %constant_dynamic-update-slice_fusion.rest_0_), channel_id=1, source_target_pairs={{0,32},{1,9},{2,34},{3,11},{4,36},{5,13},{6,38},{7,15},{8,40},{9,1... | collective-permute-start | bytes 3145736 | tf_op jit(solution)/shard_map/ppermute | solution.py:487
  48.0 26.6 %all-to-all-start = ((bf16[8,512,128]{2,1,0:T(8,128)(2,1)}), bf16[8,512,128]{2,1,0:T(8,128)(2,1)S(1)}, u32[]{:S(2)}, u32[]{:S(2)}) async-start(bf16[8,512,128]{2,1,0:T(8,128)(2,1)} %get-tuple-element.40), calls=%async_computation | async-start | bytes 2097152 | tf_op jit(solution)/shard_map/all_to_all | solution.py:526
  74.6 5.9 %collective-permute-start.8 = (bf16[256,2048]{1,0:T(8,128)(2,1)S(1)}, bf16[256,2048]{1,0:T(8,128)(2,1)}, u32[]{:S(2)}, u32[]{:S(2)}) collective-permute-start(bf16[256,2048]{1,0:T(8,128)(2,1)S(1)} %constant_dynamic-update-slice_fusion.rest_0_), channel_id=1, source_target_pairs={{0,1},{1,0},{2,3},{3,2},{4,5},{5,4},{6,7},{7,6},{8,9},{9,8},{10,11... | collective-permute-start | bytes 3145736 | tf_op jit(solution)/shard_map/ppermute | solution.py:492
  75.2 5.3 %collective-permute-start.9 = (bf16[256,2048]{1,0:T(8,128)(2,1)}, bf16[256,2048]{1,0:T(8,128)(2,1)}, u32[]{:S(2)}, u32[]{:S(2)}) collective-permute-start(bf16[256,2048]{1,0:T(8,128)(2,1)} %collective-permute-done.5.rest_1_), channel_id=1, source_target_pairs={{0,1},{1,0},{2,3},{3,2},{4,5},{5,4},{6,7},{7,6},{8,9},{9,8},{10,11... | collective-permute-start | bytes 3145736 | tf_op jit(solution)/shard_map/ppermute | solution.py:492
  75.3 5.3 %collective-permute-start.10 = (bf16[256,2048]{1,0:T(8,128)(2,1)}, bf16[256,2048]{1,0:T(8,128)(2,1)}, u32[]{:S(2)}, u32[]{:S(2)}) collective-permute-start(bf16[256,2048]{1,0:T(8,128)(2,1)} %collective-permute-done.6.rest_2_), channel_id=1, source_target_pairs={{0,1},{1,0},{2,3},{3,2},{4,5},{5,4},{6,7},{7,6},{8,9},{9,8},{10,11... | collective-permute-start | bytes 3145736 | tf_op jit(solution)/shard_map/ppermute | solution.py:492
  75.7 6.4 %collective-permute-start.11 = (bf16[256,2048]{1,0:T(8,128)(2,1)}, bf16[256,2048]{1,0:T(8,128)(2,1)}, u32[]{:S(2)}, u32[]{:S(2)}) collective-permute-start(bf16[256,2048]{1,0:T(8,128)(2,1)} %collective-permute-done.7.rest_3_), channel_id=1, source_target_pairs={{0,1},{1,0},{2,3},{3,2},{4,5},{5,4},{6,7},{7,6},{8,9},{9,8},{10,11... | collective-permute-start | bytes 3145736 | tf_op jit(solution)/shard_map/ppermute | solution.py:492
  75.8 20.6 %all-to-all-start.1 = ((bf16[8,512,128]{2,1,0:T(8,128)(2,1)}), bf16[8,512,128]{2,1,0:T(8,128)(2,1)S(1)}, u32[]{:S(2)}, u32[]{:S(2)}) async-start(bf16[8,512,128]{2,1,0:T(8,128)(2,1)} %get-tuple-element.45), calls=%async_computation.1 | async-start | bytes 2097152 | tf_op jit(solution)/shard_map/all_to_all | solution.py:532

commit v4 on v3

--- a/solution.py
+++ b/solution.py
@@ -7,6 +7,7 @@
 from jax.experimental import pallas as pl
 from jax.experimental.pallas import tpu as pltpu
 from jax.sharding import PartitionSpec as P
+
 
 HEAD_DIM = 64
 WINDOW = 128
@@ -292,11 +293,10 @@
                 vs[s, pl.ds(at, BLOCK), 0:128] = vv.astype(BF16)
                 vs[s, pl.ds(at, BLOCK), 128:256] = jnp.full((BLOCK, 128), live, F32).astype(BF16)
 
-    def project(part):
-        size = rows // 2
-        at = part * size
-        xs[at : at + size, :] = x_ref.at[part * (BLOCK // 2) : (part + 1) * (BLOCK // 2)].reshape(size, x_ref.shape[2])[...]
-        x = xs[at : at + size, :]
+    def project():
+        size, at = rows, 0
+        xs[...] = x_ref.reshape(rows, x_ref.shape[2])[...]
+        x = xs[...]
         cols = jnp.dot(x, w_ref[...], preferred_element_type=F32)
         scale = scale_ref[at : at + size, :]
         qk = cols[:, :256] * jnp.concatenate([scale, scale], axis=1)
@@ -337,8 +337,7 @@
 
     @pl.when(step < blocks)
     def _():
-        project(0)
-        project(1)
+        project()
         separate()
 
     @pl.when(step > 0)
@@ -475,9 +474,8 @@
     return pairs
 
 
-def gather_weights(out_pool, out_attn, core):
+def gather_line(half):
     both = ("sp", "tp")
-    half = jnp.where(core == 0, out_pool, out_attn)
     return [half] + [lax.ppermute(half, both, ring_pairs(k, True)) for k in (1, 2, 3)]
 
 
@@ -511,15 +509,16 @@
     tp = lax.axis_index("tp")
     sp_size = lax.axis_size("sp")
     core = tp % 2
-    line = gather_weights(out_pool, out_attn, core)
+    half = jnp.where(core == 0, out_pool, out_attn)
     head, tail, w_pool, w_attn = first_rows(
         inputs, norm_gain[None, :], pool_proj, pool_gate_proj, query_proj, key_proj.T, value_proj.T, attn_gate_proj
     )
     up = [(i, i + 1) for i in range(sp_size - 1)]
     down = [(j, i) for i, j in up]
-    *line, head, tail = lax.optimization_barrier((*line, head, tail))
+    half, head, tail = lax.optimization_barrier((half, head, tail))
     before = lax.ppermute(tail, "sp", up)
     after = lax.ppermute(head, "sp", down)
+    line = gather_line(half)
     y_pool, scale = pool_branch(inputs, w_pool, pool_mix, before, after)
     *line, y_pool = lax.optimization_barrier((*line, y_pool))
     mine = gather_rest(line)

time: 103 us -> 95.8 us (0.930)
  waiting for transfers between devices: 19.2 us -> 13.6 us
  starting transfers between devices: 27 us -> 25 us
    ppermute x1, waiting for transfers between devices: 6.37 us -> 3.14 us  [body(): after = lax.ppermute(head, 'sp', down)]
    ppermute x1, starting transfers between devices: 5.88 us -> 3.46 us  [body(): before = lax.ppermute(tail, 'sp', up)]
    ppermute x3, waiting for transfers between devices: 1.38 us -> 0.01 us  [gather_line(): lax.ppermute(half, both, ring_pairs(k, True))]
  transfers between devices with their start and end apart: 14 -> 14, of which waited for: 7 -> 4; matrix products, arithmetic and copies ran while one was open for 0% -> 0% of each run, Pallas kernels for 33% -> 43%
where the time goes in v4:
time: 95.8 us; the launch traced here: 95.4 us
  Pallas kernels  54.2 us (57%)
  starting transfers between devices  25 us (26%)
  waiting for transfers between devices  13.6 us (14%)
  other arithmetic  0.99 us (1%)
    pallas_call x1, Pallas kernels, attn_branch(): pl.pallas_call(attn_kernel, grid=(blocks + 1,), in_specs=[pl.BlockSpec(me...  22.1 us
    pallas_call x1, Pallas kernels, pool_branch(): pl.pallas_call(pool_kernel, in_specs=[far, far, whole, whole, whole], out...  13.9 us
    pallas_call x2, Pallas kernels, half_matmul(): pl.pallas_call(functools.partial(half_kernel, which), grid=(steps,), in_s...  12.1 us
    all_to_all x1, waiting for transfers between devices, body(): lax.all_to_all(y_attn, 'tp', split_axis=0, concat_axis=0, tiled=True)  8.86 us
    pallas_call x1, Pallas kernels, first_rows(): pl.pallas_call(first_kernel, grid=(2,), in_specs=[pl.BlockSpec((half, 4,...  6.09 us
    ppermute x3, starting transfers between devices, gather_rest(): lax.ppermute(block, both, ring_pairs(k, False))  5.07 us
    all_to_all x1, starting transfers between devices, body(): lax.all_to_all(y_attn, 'tp', split_axis=0, concat_axis=0, tiled=True)  4.71 us
    all_to_all x1, starting transfers between devices, body(): lax.all_to_all(y_pool, 'tp', split_axis=0, concat_axis=0, tiled=True)  4.3 us
  transfers between devices with their start and end apart: 14, of which 4 were waited for; matrix products, arithmetic and copies ran while one was open for 0% of the time, Pallas kernels for 43%

profile of v4, /device:TPU:24, one launch (start us, length us, event | category | flops | bytes accessed | tf_op | source)
XLA Modules:
  0.0 95.4 jit_solution(12613603037512596356)
XLA Ops:
  0.6 1.0 %broadcast_select_fusion = bf16[64,2048]{1,0:T(8,128)(2,1)S(1)} fusion(bf16[64,2048]{1,0:T(8,128)(2,1)} %param.26, bf16[64,2048]{1,0:T(8,128)(2,1)} %param.27, pred[]{:T(512)S(6)} %eq.5), kind=kLoop, calls=%fused_computation | loop fusion | flops 131072 | bytes 786433 | tf_op jit(solution)/shard_map/jit(_where)/select_n | solution.py:512
  1.6 6.1 %first_rows.1 = (bf16[4,136,128]{2,1,0:T(8,128)(2,1)}, bf16[4,136,128]{2,1,0:T(8,128)(2,1)}, bf16[2048,256]{1,0:T(8,128)(2,1)}, bf16[2048,512]{1,0:T(8,128)(2,1)}) custom-call(bf16[1024,4,2048]{2,1,0:T(4,128)(2,1)} %x_ref.5, f32[1,2048]{1,0:T(1,128)} %bitcast.8, bf16[2048,128]{1,0:T(8,128)(2,1)} %pool_ref.1, bf16[2048,128]{1,0:T(8,128)(2,1)} %pgate_ref.1, ...), custom_call_target="tpu_custom_call" | custom-call | flops 1073741824 | bytes 12582912 | tf_op jit(solution)/shard_map/first_rows/pallas_call | solution.py:94
  7.7 3.5 %collective-permute-start = (bf16[4,136,128]{2,1,0:T(8,128)(2,1)}, bf16[4,136,128]{2,1,0:T(8,128)(2,1)S(1)}, u32[]{:S(2)}, u32[]{:S(2)}) collective-permute-start(bf16[4,136,128]{2,1,0:T(8,128)(2,1)} %get-tuple-element.27), channel_id=1, source_target_pairs={{0,8},{8,16},{16,24},{24,32},{32,40},{40,48},{48,56},{56,64},{64,7... | collective-permute-start | bytes 417800 | tf_op jit(solution)/shard_map/ppermute | solution.py:519
  11.2 2.4 %collective-permute-start.1 = (bf16[4,136,128]{2,1,0:T(8,128)(2,1)}, bf16[4,136,128]{2,1,0:T(8,128)(2,1)S(1)}, u32[]{:S(2)}, u32[]{:S(2)}) collective-permute-start(bf16[4,136,128]{2,1,0:T(8,128)(2,1)} %get-tuple-element.28), channel_id=1, source_target_pairs={{8,0},{16,8},{24,16},{32,24},{40,32},{48,40},{56,48},{64,56},{72,6... | collective-permute-start | bytes 417800 | tf_op jit(solution)/shard_map/ppermute | solution.py:520
  13.6 0.8 collective-permute-start.4
  14.4 0.6 collective-permute-start.3
  15.0 2.5 %collective-permute-start.2 = (bf16[64,2048]{1,0:T(8,128)(2,1)S(1)}, bf16[64,2048]{1,0:T(8,128)(2,1)S(1)}, u32[]{:S(2)}, u32[]{:S(2)}) collective-permute-start(bf16[64,2048]{1,0:T(8,128)(2,1)S(1)} %broadcast_select_fusion), channel_id=1, source_target_pairs={{0,8},{1,33},{2,10},{3,35},{4,12},{5,37},{6,14},{7,39},{8,16},{9,4... | collective-permute-start | bytes 786440 | tf_op jit(solution)/shard_map/ppermute | solution.py:479
  17.5 0.0 collective-permute-done.before_ref
  17.5 0.0 copy-start.1
  17.5 3.1 %collective-permute-done.1.after_ref = bf16[4,136,128]{2,1,0:T(8,128)(2,1)S(1)} collective-permute-done((bf16[4,136,128]{2,1,0:T(8,128)(2,1)}, bf16[4,136,128]{2,1,0:T(8,128)(2,1)S(1)}, u32[]{:S(2)}, u32[]{:S(2)}) %collective-permute-start.1) | collective-permute-done | bytes 139296 | tf_op jit(solution)/shard_map/ppermute | solution.py:520
  20.7 0.0 copy-start.2
  20.7 0.0 copy-done.1
  20.7 0.7 copy-done.2
  21.3 13.9 %pool_branch.1 = (bf16[8,512,128]{2,1,0:T(8,128)(2,1)}, f32[4096,128]{1,0:T(8,128)}) custom-call(bf16[1024,4,2048]{2,1,0:T(4,128)(2,1)} %x_ref.5, bf16[2048,256]{1,0:T(8,128)(2,1)} %get-tuple-element.24.w_hbm, bf16[1,128,128]{2,1,0:T(8,128)(2,1)} %mix_ref.1, bf16[4,136,128]{2,1,0:T(8,128)(2,1)} %copy-done.1, bf16[4,136,128]{2,1,0:T(8,128)(2,1)} %copy-done.2), custom_call_target="tpu_custom_call" | custom-call | flops 4294967296 | bytes 18874368 | tf_op jit(solution)/shard_map/pool_branch/pallas_call | solution.py:224
  35.3 0.0 collective-permute-done.4
  35.3 0.0 collective-permute-done.3
  35.3 0.0 collective-permute-done.2
  35.4 0.0 copy-start
  35.4 1.0 %collective-permute-start.7 = (bf16[256,2048]{1,0:T(8,128)(2,1)S(1)}, bf16[256,2048]{1,0:T(8,128)(2,1)}, u32[]{:S(2)}, u32[]{:S(2)}) collective-permute-start(bf16[256,2048]{1,0:T(8,128)(2,1)S(1)} %constant_dynamic-update-slice_fusion.rest_0_), channel_id=1, source_target_pairs={{0,96},{1,25},{2,98},{3,27},{4,100},{5,29},{6,102},{7,31},{8,104},... | collective-permute-start | bytes 3145736 | tf_op jit(solution)/shard_map/ppermute | solution.py:485
  36.4 3.1 %collective-permute-start.6 = (bf16[256,2048]{1,0:T(8,128)(2,1)S(1)}, bf16[256,2048]{1,0:T(8,128)(2,1)}, u32[]{:S(2)}, u32[]{:S(2)}) collective-permute-start(bf16[256,2048]{1,0:T(8,128)(2,1)S(1)} %constant_dynamic-update-slice_fusion.rest_0_), channel_id=1, source_target_pairs={{0,64},{1,17},{2,66},{3,19},{4,68},{5,21},{6,70},{7,23},{8,72},{9,... | collective-permute-start | bytes 3145736 | tf_op jit(solution)/shard_map/ppermute | solution.py:485
  39.5 1.0 %collective-permute-start.5 = (bf16[256,2048]{1,0:T(8,128)(2,1)S(1)}, bf16[256,2048]{1,0:T(8,128)(2,1)}, u32[]{:S(2)}, u32[]{:S(2)}) collective-permute-start(bf16[256,2048]{1,0:T(8,128)(2,1)S(1)} %constant_dynamic-update-slice_fusion.rest_0_), channel_id=1, source_target_pairs={{0,32},{1,9},{2,34},{3,11},{4,36},{5,13},{6,38},{7,15},{8,40},{9,1... | collective-permute-start | bytes 3145736 | tf_op jit(solution)/shard_map/ppermute | solution.py:485
  40.5 4.3 %all-to-all-start = ((bf16[8,512,128]{2,1,0:T(8,128)(2,1)}), bf16[8,512,128]{2,1,0:T(8,128)(2,1)S(1)}, u32[]{:S(2)}, u32[]{:S(2)}) async-start(bf16[8,512,128]{2,1,0:T(8,128)(2,1)} %get-tuple-element.34), calls=%async_computation | async-start | bytes 2097152 | tf_op jit(solution)/shard_map/all_to_all | solution.py:525
  44.8 22.1 %attn_branch.1 = (bf16[8,512,128]{2,1,0:T(8,128)(2,1)}, f32[4,2,1024]{2,1,0:T(2,128)}) custom-call(f32[2]{0:T(128)} %sink_ref.1, bf16[1024,4,2048]{2,1,0:T(4,128)(2,1)} %x_ref.5, f32[4096,128]{1,0:T(8,128)} %get-tuple-element.29.scale_ref, bf16[2048,512]{1,0:T(8,128)(2,1)} %get-tuple-element.30.w_ref, f32[1,64]{1,0:T(1,128)} %bitcast.9, f32[1,64]{1,0:T(1,128)} %bitcast.10, ...), custom_call_target="tpu_custom_call" | custom-call | flops 12884901888 | bytes 20971520 | tf_op jit(solution)/shard_map/attn_branch/pallas_call | solution.py:354
  66.9 0.0 all-to-all-done.y_ref
  66.9 0.0 collective-permute-done.7.rest_3_
  66.9 0.0 collective-permute-done.6.rest_2_
  66.9 0.0 collective-permute-done.5.rest_1_
  66.9 0.0 copy-done
  66.9 0.6 collective-permute-start.8
  67.5 0.1 collective-permute-start.9
  67.6 0.4 collective-permute-start.10
  68.0 0.1 collective-permute-start.11
  68.1 4.7 %all-to-all-start.1 = ((bf16[8,512,128]{2,1,0:T(8,128)(2,1)}), bf16[8,512,128]{2,1,0:T(8,128)(2,1)S(1)}, u32[]{:S(2)}, u32[]{:S(2)}) async-start(bf16[8,512,128]{2,1,0:T(8,128)(2,1)} %get-tuple-element.39), calls=%async_computation.1 | async-start | bytes 2097152 | tf_op jit(solution)/shard_map/all_to_all | solution.py:531
  72.8 0.0 collective-permute-done.8.rest_4_
  72.8 0.0 collective-permute-done.9.rest_5_
  72.8 0.1 collective-permute-done.10.rest_6_
  72.9 1.5 %collective-permute-done.11.rest_7_ = bf16[256,2048]{1,0:T(8,128)(2,1)} collective-permute-done((bf16[256,2048]{1,0:T(8,128)(2,1)}, bf16[256,2048]{1,0:T(8,128)(2,1)}, u32[]{:S(2)}, u32[]{:S(2)}) %collective-permute-start.11) | collective-permute-done | bytes 1048608 | tf_op jit(solution)/shard_map/ppermute | solution.py:490
  74.4 5.5 %shard_map.149.rest_8_ = bf16[512,2048]{1,0:T(8,128)(2,1)} custom-call(bf16[8,512,128]{2,1,0:T(8,128)(2,1)S(1)} %all-to-all-done.y_ref, bf16[256,2048]{1,0:T(8,128)(2,1)} %copy-done, bf16[256,2048]{1,0:T(8,128)(2,1)} %collective-permute-done.5.rest_1_, bf16[256,2048]{1,0:T(8,128)(2,1)} %collective-permute-done.6.rest_2_, ...), custom_call_target="tpu_custom_call" | custom-call | flops 2147483648 | bytes 8388608 | tf_op jit(solution)/shard_map/pallas_call | solution.py:449
  79.9 8.9 %all-to-all-done.1.y_ref = bf16[8,512,128]{2,1,0:T(8,128)(2,1)S(1)} async-done(((bf16[8,512,128]{2,1,0:T(8,128)(2,1)}), bf16[8,512,128]{2,1,0:T(8,128)(2,1)S(1)}, u32[]{:S(2)}, u32[]{:S(2)}) %all-to-all-start.1) | async-done | bytes 1048608 | tf_op jit(solution)/shard_map/all_to_all | solution.py:531
  88.8 6.7 %shard_map.150 = bf16[128,4,2048]{2,1,0:T(4,128)(2,1)} custom-call(bf16[8,512,128]{2,1,0:T(8,128)(2,1)S(1)} %all-to-all-done.1.y_ref, bf16[256,2048]{1,0:T(8,128)(2,1)} %copy-done, bf16[256,2048]{1,0:T(8,128)(2,1)} %collective-permute-done.5.rest_1_, bf16[256,2048]{1,0:T(8,128)(2,1)} %collective-permute-done.6.rest_2_, ...), custom_call_target="tpu_custom_call" | custom-call | flops 2147483648 | bytes 8388608 | tf_op jit(solution)/shard_map/pallas_call | solution.py:449
  (4 shorter events, 0.1 us)
Async XLA Ops:
  7.7 9.8 %collective-permute-start = (bf16[4,136,128]{2,1,0:T(8,128)(2,1)}, bf16[4,136,128]{2,1,0:T(8,128)(2,1)S(1)}, u32[]{:S(2)}, u32[]{:S(2)}) collective-permute-start(bf16[4,136,128]{2,1,0:T(8,128)(2,1)} %get-tuple-element.27), channel_id=1, source_target_pairs={{0,8},{8,16},{16,24},{24,32},{32,40},{40,48},{48,56},{56,64},{64,7... | collective-permute-start | bytes 417800 | tf_op jit(solution)/shard_map/ppermute | solution.py:519
  11.2 9.5 %collective-permute-start.1 = (bf16[4,136,128]{2,1,0:T(8,128)(2,1)}, bf16[4,136,128]{2,1,0:T(8,128)(2,1)S(1)}, u32[]{:S(2)}, u32[]{:S(2)}) collective-permute-start(bf16[4,136,128]{2,1,0:T(8,128)(2,1)} %get-tuple-element.28), channel_id=1, source_target_pairs={{8,0},{16,8},{24,16},{32,24},{40,32},{48,40},{56,48},{64,56},{72,6... | collective-permute-start | bytes 417800 | tf_op jit(solution)/shard_map/ppermute | solution.py:520
  13.6 21.7 %collective-permute-start.4 = (bf16[64,2048]{1,0:T(8,128)(2,1)S(1)}, bf16[64,2048]{1,0:T(8,128)(2,1)S(1)}, u32[]{:S(2)}, u32[]{:S(2)}) collective-permute-start(bf16[64,2048]{1,0:T(8,128)(2,1)S(1)} %broadcast_select_fusion), channel_id=1, source_target_pairs={{0,24},{1,97},{2,26},{3,99},{4,28},{5,101},{6,30},{7,103},{8,0},{9... | collective-permute-start | bytes 786440 | tf_op jit(solution)/shard_map/ppermute | solution.py:479
  14.4 20.9 %collective-permute-start.3 = (bf16[64,2048]{1,0:T(8,128)(2,1)S(1)}, bf16[64,2048]{1,0:T(8,128)(2,1)S(1)}, u32[]{:S(2)}, u32[]{:S(2)}) collective-permute-start(bf16[64,2048]{1,0:T(8,128)(2,1)S(1)} %broadcast_select_fusion), channel_id=1, source_target_pairs={{0,16},{1,65},{2,18},{3,67},{4,20},{5,69},{6,22},{7,71},{8,24},{9,... | collective-permute-start | bytes 786440 | tf_op jit(solution)/shard_map/ppermute | solution.py:479
  15.0 20.3 %collective-permute-start.2 = (bf16[64,2048]{1,0:T(8,128)(2,1)S(1)}, bf16[64,2048]{1,0:T(8,128)(2,1)S(1)}, u32[]{:S(2)}, u32[]{:S(2)}) collective-permute-start(bf16[64,2048]{1,0:T(8,128)(2,1)S(1)} %broadcast_select_fusion), channel_id=1, source_target_pairs={{0,8},{1,33},{2,10},{3,35},{4,12},{5,37},{6,14},{7,39},{8,16},{9,4... | collective-permute-start | bytes 786440 | tf_op jit(solution)/shard_map/ppermute | solution.py:479
  17.5 3.1 %copy-start.1 = (bf16[4,136,128]{2,1,0:T(8,128)(2,1)}, bf16[4,136,128]{2,1,0:T(8,128)(2,1)S(1)}, u32[]{:S(2)}) copy-start(bf16[4,136,128]{2,1,0:T(8,128)(2,1)S(1)} %collective-permute-done.before_ref) | copy-start | bytes 417796
  20.7 0.7 copy-start.2
  35.4 31.5 %copy-start = (bf16[256,2048]{1,0:T(8,128)(2,1)}, bf16[256,2048]{1,0:T(8,128)(2,1)S(1)}, u32[]{:S(2)}) copy-start(bf16[256,2048]{1,0:T(8,128)(2,1)S(1)} %constant_dynamic-update-slice_fusion.rest_0_) | copy-start | bytes 3145732
  35.4 31.5 %collective-permute-start.7 = (bf16[256,2048]{1,0:T(8,128)(2,1)S(1)}, bf16[256,2048]{1,0:T(8,128)(2,1)}, u32[]{:S(2)}, u32[]{:S(2)}) collective-permute-start(bf16[256,2048]{1,0:T(8,128)(2,1)S(1)} %constant_dynamic-update-slice_fusion.rest_0_), channel_id=1, source_target_pairs={{0,96},{1,25},{2,98},{3,27},{4,100},{5,29},{6,102},{7,31},{8,104},... | collective-permute-start | bytes 3145736 | tf_op jit(solution)/shard_map/ppermute | solution.py:485
  36.4 30.5 %collective-permute-start.6 = (bf16[256,2048]{1,0:T(8,128)(2,1)S(1)}, bf16[256,2048]{1,0:T(8,128)(2,1)}, u32[]{:S(2)}, u32[]{:S(2)}) collective-permute-start(bf16[256,2048]{1,0:T(8,128)(2,1)S(1)} %constant_dynamic-update-slice_fusion.rest_0_), channel_id=1, source_target_pairs={{0,64},{1,17},{2,66},{3,19},{4,68},{5,21},{6,70},{7,23},{8,72},{9,... | collective-permute-start | bytes 3145736 | tf_op jit(solution)/shard_map/ppermute | solution.py:485
  39.5 27.4 %collective-permute-start.5 = (bf16[256,2048]{1,0:T(8,128)(2,1)S(1)}, bf16[256,2048]{1,0:T(8,128)(2,1)}, u32[]{:S(2)}, u32[]{:S(2)}) collective-permute-start(bf16[256,2048]{1,0:T(8,128)(2,1)S(1)} %constant_dynamic-update-slice_fusion.rest_0_), channel_id=1, source_target_pairs={{0,32},{1,9},{2,34},{3,11},{4,36},{5,13},{6,38},{7,15},{8,40},{9,1... | collective-permute-start | bytes 3145736 | tf_op jit(solution)/shard_map/ppermute | solution.py:485
  40.5 26.4 %all-to-all-start = ((bf16[8,512,128]{2,1,0:T(8,128)(2,1)}), bf16[8,512,128]{2,1,0:T(8,128)(2,1)S(1)}, u32[]{:S(2)}, u32[]{:S(2)}) async-start(bf16[8,512,128]{2,1,0:T(8,128)(2,1)} %get-tuple-element.34), calls=%async_computation | async-start | bytes 2097152 | tf_op jit(solution)/shard_map/all_to_all | solution.py:525
  66.9 5.9 %collective-permute-start.8 = (bf16[256,2048]{1,0:T(8,128)(2,1)S(1)}, bf16[256,2048]{1,0:T(8,128)(2,1)}, u32[]{:S(2)}, u32[]{:S(2)}) collective-permute-start(bf16[256,2048]{1,0:T(8,128)(2,1)S(1)} %constant_dynamic-update-slice_fusion.rest_0_), channel_id=1, source_target_pairs={{0,1},{1,0},{2,3},{3,2},{4,5},{5,4},{6,7},{7,6},{8,9},{9,8},{10,11... | collective-permute-start | bytes 3145736 | tf_op jit(solution)/shard_map/ppermute | solution.py:490
  67.5 5.3 %collective-permute-start.9 = (bf16[256,2048]{1,0:T(8,128)(2,1)}, bf16[256,2048]{1,0:T(8,128)(2,1)}, u32[]{:S(2)}, u32[]{:S(2)}) collective-permute-start(bf16[256,2048]{1,0:T(8,128)(2,1)} %collective-permute-done.5.rest_1_), channel_id=1, source_target_pairs={{0,1},{1,0},{2,3},{3,2},{4,5},{5,4},{6,7},{7,6},{8,9},{9,8},{10,11... | collective-permute-start | bytes 3145736 | tf_op jit(solution)/shard_map/ppermute | solution.py:490
  67.6 5.3 %collective-permute-start.10 = (bf16[256,2048]{1,0:T(8,128)(2,1)}, bf16[256,2048]{1,0:T(8,128)(2,1)}, u32[]{:S(2)}, u32[]{:S(2)}) collective-permute-start(bf16[256,2048]{1,0:T(8,128)(2,1)} %collective-permute-done.6.rest_2_), channel_id=1, source_target_pairs={{0,1},{1,0},{2,3},{3,2},{4,5},{5,4},{6,7},{7,6},{8,9},{9,8},{10,11... | collective-permute-start | bytes 3145736 | tf_op jit(solution)/shard_map/ppermute | solution.py:490
  68.0 6.4 %collective-permute-start.11 = (bf16[256,2048]{1,0:T(8,128)(2,1)}, bf16[256,2048]{1,0:T(8,128)(2,1)}, u32[]{:S(2)}, u32[]{:S(2)}) collective-permute-start(bf16[256,2048]{1,0:T(8,128)(2,1)} %collective-permute-done.7.rest_3_), channel_id=1, source_target_pairs={{0,1},{1,0},{2,3},{3,2},{4,5},{5,4},{6,7},{7,6},{8,9},{9,8},{10,11... | collective-permute-start | bytes 3145736 | tf_op jit(solution)/shard_map/ppermute | solution.py:490
  68.1 20.6 %all-to-all-start.1 = ((bf16[8,512,128]{2,1,0:T(8,128)(2,1)}), bf16[8,512,128]{2,1,0:T(8,128)(2,1)S(1)}, u32[]{:S(2)}, u32[]{:S(2)}) async-start(bf16[8,512,128]{2,1,0:T(8,128)(2,1)} %get-tuple-element.39), calls=%async_computation.1 | async-start | bytes 2097152 | tf_op jit(solution)/shard_map/all_to_all | solution.py:531

commit v5 on v4

--- a/solution.py
+++ b/solution.py
@@ -23,11 +23,10 @@
 def row_scale(x):
     width = x.shape[1]
     acc = None
-    for c in range(0, width, 512):
-        parts = [x[:, c + d : c + d + 128] for d in range(0, 512, 128)]
-        parts = [p * p for p in parts]
-        four = ((parts[0] + parts[1]) + (parts[2] + parts[3])).astype(F32)
-        acc = four if acc is None else acc + four
+    for c in range(0, width, 128):
+        part = x[:, c : c + 128].astype(F32)
+        part = part * part
+        acc = part if acc is None else acc + part
     total = jnp.sum(acc, axis=-1, keepdims=True)
     return lax.rsqrt(total * (1.0 / width) + EPS)
 
@@ -527,7 +526,7 @@
         sink_logit, inputs, scale, w_attn, query_gain[None, :], key_gain[None, :], before, after
     )
     y_attn, pool_rows, *mine = lax.optimization_barrier((y_attn, pool_rows, *mine))
-    pieces = with_partner(mine)
+    pieces = [pltpu.with_memory_space_constraint(piece, pltpu.HBM) for piece in with_partner(mine)]
     attn_rows = lax.all_to_all(y_attn, "tp", split_axis=0, concat_axis=0, tiled=True)
     partial = half_matmul(0, pool_rows, pieces)
     mixed = half_matmul(1, attn_rows, pieces, partial)

time: 95.8 us -> 95.6 us (level)
  no operation moved by 1% of the time
where the time goes in v5:
time: 95.6 us; the launch traced here: 95.2 us
  Pallas kernels  54 us (56%)
  starting transfers between devices  25.1 us (26%)
  waiting for transfers between devices  13.6 us (14%)
  other arithmetic  0.99 us (1%)
    pallas_call x1, Pallas kernels, attn_branch(): pl.pallas_call(attn_kernel, grid=(blocks + 1,), in_specs=[pl.BlockSpec(me...  22.1 us
    pallas_call x1, Pallas kernels, pool_branch(): pl.pallas_call(pool_kernel, in_specs=[far, far, whole, whole, whole], out...  13.7 us
    pallas_call x2, Pallas kernels, half_matmul(): pl.pallas_call(functools.partial(half_kernel, which), grid=(steps,), in_s...  12.1 us
    all_to_all x1, waiting for transfers between devices, body(): lax.all_to_all(y_attn, 'tp', split_axis=0, concat_axis=0, tiled=True)  8.87 us
    pallas_call x1, Pallas kernels, first_rows(): pl.pallas_call(first_kernel, grid=(2,), in_specs=[pl.BlockSpec((half, 4,...  6.1 us
    ppermute x3, starting transfers between devices, gather_rest(): lax.ppermute(block, both, ring_pairs(k, False))  5.06 us
    all_to_all x1, starting transfers between devices, body(): lax.all_to_all(y_attn, 'tp', split_axis=0, concat_axis=0, tiled=True)  4.72 us
    all_to_all x1, starting transfers between devices, body(): lax.all_to_all(y_pool, 'tp', split_axis=0, concat_axis=0, tiled=True)  4.31 us
  transfers between devices with their start and end apart: 14, of which 4 were waited for; matrix products, arithmetic and copies ran while one was open for 0% of the time, Pallas kernels for 43%

profile of v5, /device:TPU:24, one launch (start us, length us, event | category | flops | bytes accessed | tf_op | source)
XLA Modules:
  0.0 95.2 jit_solution(17174473772835526853)
XLA Ops:
  0.6 1.0 %broadcast_select_fusion = bf16[64,2048]{1,0:T(8,128)(2,1)S(1)} fusion(bf16[64,2048]{1,0:T(8,128)(2,1)} %param.26, bf16[64,2048]{1,0:T(8,128)(2,1)} %param.27, pred[]{:T(512)S(6)} %eq.5), kind=kLoop, calls=%fused_computation | loop fusion | flops 131072 | bytes 786433 | tf_op jit(solution)/shard_map/jit(_where)/select_n | solution.py:511
  1.6 6.1 %first_rows.1 = (bf16[4,136,128]{2,1,0:T(8,128)(2,1)}, bf16[4,136,128]{2,1,0:T(8,128)(2,1)}, bf16[2048,256]{1,0:T(8,128)(2,1)}, bf16[2048,512]{1,0:T(8,128)(2,1)}) custom-call(bf16[1024,4,2048]{2,1,0:T(4,128)(2,1)} %x_ref.5, f32[1,2048]{1,0:T(1,128)} %bitcast.8, bf16[2048,128]{1,0:T(8,128)(2,1)} %pool_ref.1, bf16[2048,128]{1,0:T(8,128)(2,1)} %pgate_ref.1, ...), custom_call_target="tpu_custom_call" | custom-call | flops 1073741824 | bytes 12582912 | tf_op jit(solution)/shard_map/first_rows/pallas_call | solution.py:93
  7.7 3.5 %collective-permute-start = (bf16[4,136,128]{2,1,0:T(8,128)(2,1)}, bf16[4,136,128]{2,1,0:T(8,128)(2,1)S(1)}, u32[]{:S(2)}, u32[]{:S(2)}) collective-permute-start(bf16[4,136,128]{2,1,0:T(8,128)(2,1)} %get-tuple-element.27), channel_id=1, source_target_pairs={{0,8},{8,16},{16,24},{24,32},{32,40},{40,48},{48,56},{56,64},{64,7... | collective-permute-start | bytes 417800 | tf_op jit(solution)/shard_map/ppermute | solution.py:518
  11.2 2.4 %collective-permute-start.1 = (bf16[4,136,128]{2,1,0:T(8,128)(2,1)}, bf16[4,136,128]{2,1,0:T(8,128)(2,1)S(1)}, u32[]{:S(2)}, u32[]{:S(2)}) collective-permute-start(bf16[4,136,128]{2,1,0:T(8,128)(2,1)} %get-tuple-element.28), channel_id=1, source_target_pairs={{8,0},{16,8},{24,16},{32,24},{40,32},{48,40},{56,48},{64,56},{72,6... | collective-permute-start | bytes 417800 | tf_op jit(solution)/shard_map/ppermute | solution.py:519
  13.6 0.8 collective-permute-start.4
  14.4 0.6 collective-permute-start.3
  15.0 2.5 %collective-permute-start.2 = (bf16[64,2048]{1,0:T(8,128)(2,1)S(1)}, bf16[64,2048]{1,0:T(8,128)(2,1)S(1)}, u32[]{:S(2)}, u32[]{:S(2)}) collective-permute-start(bf16[64,2048]{1,0:T(8,128)(2,1)S(1)} %broadcast_select_fusion), channel_id=1, source_target_pairs={{0,8},{1,33},{2,10},{3,35},{4,12},{5,37},{6,14},{7,39},{8,16},{9,4... | collective-permute-start | bytes 786440 | tf_op jit(solution)/shard_map/ppermute | solution.py:478
  17.5 0.0 collective-permute-done.before_ref
  17.6 0.0 copy-start.1
  17.6 3.1 %collective-permute-done.1.after_ref = bf16[4,136,128]{2,1,0:T(8,128)(2,1)S(1)} collective-permute-done((bf16[4,136,128]{2,1,0:T(8,128)(2,1)}, bf16[4,136,128]{2,1,0:T(8,128)(2,1)S(1)}, u32[]{:S(2)}, u32[]{:S(2)}) %collective-permute-start.1) | collective-permute-done | bytes 139296 | tf_op jit(solution)/shard_map/ppermute | solution.py:519
  20.7 0.0 copy-start.2
  20.7 0.0 copy-done.1
  20.7 0.7 copy-done.2
  21.4 13.7 %pool_branch.1 = (bf16[8,512,128]{2,1,0:T(8,128)(2,1)}, f32[4096,128]{1,0:T(8,128)}) custom-call(bf16[1024,4,2048]{2,1,0:T(4,128)(2,1)} %x_ref.5, bf16[2048,256]{1,0:T(8,128)(2,1)} %get-tuple-element.24.w_hbm, bf16[1,128,128]{2,1,0:T(8,128)(2,1)} %mix_ref.1, bf16[4,136,128]{2,1,0:T(8,128)(2,1)} %copy-done.1, bf16[4,136,128]{2,1,0:T(8,128)(2,1)} %copy-done.2), custom_call_target="tpu_custom_call" | custom-call | flops 4294967296 | bytes 18874368 | tf_op jit(solution)/shard_map/pool_branch/pallas_call | solution.py:223
  35.1 0.0 collective-permute-done.4
  35.1 0.0 collective-permute-done.3
  35.1 0.0 collective-permute-done.2
  35.2 0.0 copy-start
  35.2 1.0 %collective-permute-start.7 = (bf16[256,2048]{1,0:T(8,128)(2,1)S(1)}, bf16[256,2048]{1,0:T(8,128)(2,1)}, u32[]{:S(2)}, u32[]{:S(2)}) collective-permute-start(bf16[256,2048]{1,0:T(8,128)(2,1)S(1)} %constant_dynamic-update-slice_fusion.rest_0_), channel_id=1, source_target_pairs={{0,96},{1,25},{2,98},{3,27},{4,100},{5,29},{6,102},{7,31},{8,104},... | collective-permute-start | bytes 3145736 | tf_op jit(solution)/shard_map/ppermute | solution.py:484
  36.2 3.0 %collective-permute-start.6 = (bf16[256,2048]{1,0:T(8,128)(2,1)S(1)}, bf16[256,2048]{1,0:T(8,128)(2,1)}, u32[]{:S(2)}, u32[]{:S(2)}) collective-permute-start(bf16[256,2048]{1,0:T(8,128)(2,1)S(1)} %constant_dynamic-update-slice_fusion.rest_0_), channel_id=1, source_target_pairs={{0,64},{1,17},{2,66},{3,19},{4,68},{5,21},{6,70},{7,23},{8,72},{9,... | collective-permute-start | bytes 3145736 | tf_op jit(solution)/shard_map/ppermute | solution.py:484
  39.3 1.0 %collective-permute-start.5 = (bf16[256,2048]{1,0:T(8,128)(2,1)S(1)}, bf16[256,2048]{1,0:T(8,128)(2,1)}, u32[]{:S(2)}, u32[]{:S(2)}) collective-permute-start(bf16[256,2048]{1,0:T(8,128)(2,1)S(1)} %constant_dynamic-update-slice_fusion.rest_0_), channel_id=1, source_target_pairs={{0,32},{1,9},{2,34},{3,11},{4,36},{5,13},{6,38},{7,15},{8,40},{9,1... | collective-permute-start | bytes 3145736 | tf_op jit(solution)/shard_map/ppermute | solution.py:484
  40.3 4.3 %all-to-all-start = ((bf16[8,512,128]{2,1,0:T(8,128)(2,1)}), bf16[8,512,128]{2,1,0:T(8,128)(2,1)S(1)}, u32[]{:S(2)}, u32[]{:S(2)}) async-start(bf16[8,512,128]{2,1,0:T(8,128)(2,1)} %get-tuple-element.34), calls=%async_computation | async-start | bytes 2097152 | tf_op jit(solution)/shard_map/all_to_all | solution.py:524
  44.6 22.1 %attn_branch.1 = (bf16[8,512,128]{2,1,0:T(8,128)(2,1)}, f32[4,2,1024]{2,1,0:T(2,128)}) custom-call(f32[2]{0:T(128)} %sink_ref.1, bf16[1024,4,2048]{2,1,0:T(4,128)(2,1)} %x_ref.5, f32[4096,128]{1,0:T(8,128)} %get-tuple-element.29.scale_ref, bf16[2048,512]{1,0:T(8,128)(2,1)} %get-tuple-element.30.w_ref, f32[1,64]{1,0:T(1,128)} %bitcast.9, f32[1,64]{1,0:T(1,128)} %bitcast.10, ...), custom_call_target="tpu_custom_call" | custom-call | flops 12884901888 | bytes 20971520 | tf_op jit(solution)/shard_map/attn_branch/pallas_call | solution.py:353
  66.7 0.0 all-to-all-done.y_ref
  66.7 0.0 collective-permute-done.7.rest_3_
  66.7 0.0 collective-permute-done.6.rest_2_
  66.7 0.0 collective-permute-done.5.rest_1_
  66.7 0.0 copy-done
  66.7 0.6 collective-permute-start.8
  67.3 0.1 collective-permute-start.9
  67.4 0.4 collective-permute-start.10
  67.8 0.1 collective-permute-start.11
  67.9 4.7 %all-to-all-start.1 = ((bf16[8,512,128]{2,1,0:T(8,128)(2,1)}), bf16[8,512,128]{2,1,0:T(8,128)(2,1)S(1)}, u32[]{:S(2)}, u32[]{:S(2)}) async-start(bf16[8,512,128]{2,1,0:T(8,128)(2,1)} %get-tuple-element.39), calls=%async_computation.1 | async-start | bytes 2097152 | tf_op jit(solution)/shard_map/all_to_all | solution.py:530
  72.6 0.0 collective-permute-done.8.rest_4_
  72.6 0.0 collective-permute-done.9.rest_5_
  72.6 0.1 collective-permute-done.10.rest_6_
  72.7 1.5 %collective-permute-done.11.rest_7_ = bf16[256,2048]{1,0:T(8,128)(2,1)} collective-permute-done((bf16[256,2048]{1,0:T(8,128)(2,1)}, bf16[256,2048]{1,0:T(8,128)(2,1)}, u32[]{:S(2)}, u32[]{:S(2)}) %collective-permute-start.11) | collective-permute-done | bytes 1048608 | tf_op jit(solution)/shard_map/ppermute | solution.py:489
  74.2 5.5 %shard_map.149.rest_8_ = bf16[512,2048]{1,0:T(8,128)(2,1)} custom-call(bf16[8,512,128]{2,1,0:T(8,128)(2,1)S(1)} %all-to-all-done.y_ref, bf16[256,2048]{1,0:T(8,128)(2,1)} %copy-done, bf16[256,2048]{1,0:T(8,128)(2,1)} %collective-permute-done.5.rest_1_, bf16[256,2048]{1,0:T(8,128)(2,1)} %collective-permute-done.6.rest_2_, ...), custom_call_target="tpu_custom_call" | custom-call | flops 2147483648 | bytes 8388608 | tf_op jit(solution)/shard_map/pallas_call | solution.py:448
  79.7 8.9 %all-to-all-done.1.y_ref = bf16[8,512,128]{2,1,0:T(8,128)(2,1)S(1)} async-done(((bf16[8,512,128]{2,1,0:T(8,128)(2,1)}), bf16[8,512,128]{2,1,0:T(8,128)(2,1)S(1)}, u32[]{:S(2)}, u32[]{:S(2)}) %all-to-all-start.1) | async-done | bytes 1048608 | tf_op jit(solution)/shard_map/all_to_all | solution.py:530
  88.6 6.7 %shard_map.150 = bf16[128,4,2048]{2,1,0:T(4,128)(2,1)} custom-call(bf16[8,512,128]{2,1,0:T(8,128)(2,1)S(1)} %all-to-all-done.1.y_ref, bf16[256,2048]{1,0:T(8,128)(2,1)} %copy-done, bf16[256,2048]{1,0:T(8,128)(2,1)} %collective-permute-done.5.rest_1_, bf16[256,2048]{1,0:T(8,128)(2,1)} %collective-permute-done.6.rest_2_, ...), custom_call_target="tpu_custom_call" | custom-call | flops 2147483648 | bytes 8388608 | tf_op jit(solution)/shard_map/pallas_call | solution.py:448
  (4 shorter events, 0.1 us)
Async XLA Ops:
  7.7 9.8 %collective-permute-start = (bf16[4,136,128]{2,1,0:T(8,128)(2,1)}, bf16[4,136,128]{2,1,0:T(8,128)(2,1)S(1)}, u32[]{:S(2)}, u32[]{:S(2)}) collective-permute-start(bf16[4,136,128]{2,1,0:T(8,128)(2,1)} %get-tuple-element.27), channel_id=1, source_target_pairs={{0,8},{8,16},{16,24},{24,32},{32,40},{40,48},{48,56},{56,64},{64,7... | collective-permute-start | bytes 417800 | tf_op jit(solution)/shard_map/ppermute | solution.py:518
  11.2 9.4 %collective-permute-start.1 = (bf16[4,136,128]{2,1,0:T(8,128)(2,1)}, bf16[4,136,128]{2,1,0:T(8,128)(2,1)S(1)}, u32[]{:S(2)}, u32[]{:S(2)}) collective-permute-start(bf16[4,136,128]{2,1,0:T(8,128)(2,1)} %get-tuple-element.28), channel_id=1, source_target_pairs={{8,0},{16,8},{24,16},{32,24},{40,32},{48,40},{56,48},{64,56},{72,6... | collective-permute-start | bytes 417800 | tf_op jit(solution)/shard_map/ppermute | solution.py:519
  13.6 21.5 %collective-permute-start.4 = (bf16[64,2048]{1,0:T(8,128)(2,1)S(1)}, bf16[64,2048]{1,0:T(8,128)(2,1)S(1)}, u32[]{:S(2)}, u32[]{:S(2)}) collective-permute-start(bf16[64,2048]{1,0:T(8,128)(2,1)S(1)} %broadcast_select_fusion), channel_id=1, source_target_pairs={{0,24},{1,97},{2,26},{3,99},{4,28},{5,101},{6,30},{7,103},{8,0},{9... | collective-permute-start | bytes 786440 | tf_op jit(solution)/shard_map/ppermute | solution.py:478
  14.4 20.7 %collective-permute-start.3 = (bf16[64,2048]{1,0:T(8,128)(2,1)S(1)}, bf16[64,2048]{1,0:T(8,128)(2,1)S(1)}, u32[]{:S(2)}, u32[]{:S(2)}) collective-permute-start(bf16[64,2048]{1,0:T(8,128)(2,1)S(1)} %broadcast_select_fusion), channel_id=1, source_target_pairs={{0,16},{1,65},{2,18},{3,67},{4,20},{5,69},{6,22},{7,71},{8,24},{9,... | collective-permute-start | bytes 786440 | tf_op jit(solution)/shard_map/ppermute | solution.py:478
  15.0 20.1 %collective-permute-start.2 = (bf16[64,2048]{1,0:T(8,128)(2,1)S(1)}, bf16[64,2048]{1,0:T(8,128)(2,1)S(1)}, u32[]{:S(2)}, u32[]{:S(2)}) collective-permute-start(bf16[64,2048]{1,0:T(8,128)(2,1)S(1)} %broadcast_select_fusion), channel_id=1, source_target_pairs={{0,8},{1,33},{2,10},{3,35},{4,12},{5,37},{6,14},{7,39},{8,16},{9,4... | collective-permute-start | bytes 786440 | tf_op jit(solution)/shard_map/ppermute | solution.py:478
  17.6 3.1 %copy-start.1 = (bf16[4,136,128]{2,1,0:T(8,128)(2,1)}, bf16[4,136,128]{2,1,0:T(8,128)(2,1)S(1)}, u32[]{:S(2)}) copy-start(bf16[4,136,128]{2,1,0:T(8,128)(2,1)S(1)} %collective-permute-done.before_ref) | copy-start | bytes 417796
  20.7 0.7 copy-start.2
  35.2 31.5 %copy-start = (bf16[256,2048]{1,0:T(8,128)(2,1)}, bf16[256,2048]{1,0:T(8,128)(2,1)S(1)}, u32[]{:S(2)}) copy-start(bf16[256,2048]{1,0:T(8,128)(2,1)S(1)} %constant_dynamic-update-slice_fusion.rest_0_) | copy-start | bytes 3145732
  35.2 31.5 %collective-permute-start.7 = (bf16[256,2048]{1,0:T(8,128)(2,1)S(1)}, bf16[256,2048]{1,0:T(8,128)(2,1)}, u32[]{:S(2)}, u32[]{:S(2)}) collective-permute-start(bf16[256,2048]{1,0:T(8,128)(2,1)S(1)} %constant_dynamic-update-slice_fusion.rest_0_), channel_id=1, source_target_pairs={{0,96},{1,25},{2,98},{3,27},{4,100},{5,29},{6,102},{7,31},{8,104},... | collective-permute-start | bytes 3145736 | tf_op jit(solution)/shard_map/ppermute | solution.py:484
  36.2 30.5 %collective-permute-start.6 = (bf16[256,2048]{1,0:T(8,128)(2,1)S(1)}, bf16[256,2048]{1,0:T(8,128)(2,1)}, u32[]{:S(2)}, u32[]{:S(2)}) collective-permute-start(bf16[256,2048]{1,0:T(8,128)(2,1)S(1)} %constant_dynamic-update-slice_fusion.rest_0_), channel_id=1, source_target_pairs={{0,64},{1,17},{2,66},{3,19},{4,68},{5,21},{6,70},{7,23},{8,72},{9,... | collective-permute-start | bytes 3145736 | tf_op jit(solution)/shard_map/ppermute | solution.py:484
  39.3 27.4 %collective-permute-start.5 = (bf16[256,2048]{1,0:T(8,128)(2,1)S(1)}, bf16[256,2048]{1,0:T(8,128)(2,1)}, u32[]{:S(2)}, u32[]{:S(2)}) collective-permute-start(bf16[256,2048]{1,0:T(8,128)(2,1)S(1)} %constant_dynamic-update-slice_fusion.rest_0_), channel_id=1, source_target_pairs={{0,32},{1,9},{2,34},{3,11},{4,36},{5,13},{6,38},{7,15},{8,40},{9,1... | collective-permute-start | bytes 3145736 | tf_op jit(solution)/shard_map/ppermute | solution.py:484
  40.3 26.4 %all-to-all-start = ((bf16[8,512,128]{2,1,0:T(8,128)(2,1)}), bf16[8,512,128]{2,1,0:T(8,128)(2,1)S(1)}, u32[]{:S(2)}, u32[]{:S(2)}) async-start(bf16[8,512,128]{2,1,0:T(8,128)(2,1)} %get-tuple-element.34), calls=%async_computation | async-start | bytes 2097152 | tf_op jit(solution)/shard_map/all_to_all | solution.py:524
  66.7 5.9 %collective-permute-start.8 = (bf16[256,2048]{1,0:T(8,128)(2,1)S(1)}, bf16[256,2048]{1,0:T(8,128)(2,1)}, u32[]{:S(2)}, u32[]{:S(2)}) collective-permute-start(bf16[256,2048]{1,0:T(8,128)(2,1)S(1)} %constant_dynamic-update-slice_fusion.rest_0_), channel_id=1, source_target_pairs={{0,1},{1,0},{2,3},{3,2},{4,5},{5,4},{6,7},{7,6},{8,9},{9,8},{10,11... | collective-permute-start | bytes 3145736 | tf_op jit(solution)/shard_map/ppermute | solution.py:489
  67.3 5.3 %collective-permute-start.9 = (bf16[256,2048]{1,0:T(8,128)(2,1)}, bf16[256,2048]{1,0:T(8,128)(2,1)}, u32[]{:S(2)}, u32[]{:S(2)}) collective-permute-start(bf16[256,2048]{1,0:T(8,128)(2,1)} %collective-permute-done.5.rest_1_), channel_id=1, source_target_pairs={{0,1},{1,0},{2,3},{3,2},{4,5},{5,4},{6,7},{7,6},{8,9},{9,8},{10,11... | collective-permute-start | bytes 3145736 | tf_op jit(solution)/shard_map/ppermute | solution.py:489
  67.4 5.3 %collective-permute-start.10 = (bf16[256,2048]{1,0:T(8,128)(2,1)}, bf16[256,2048]{1,0:T(8,128)(2,1)}, u32[]{:S(2)}, u32[]{:S(2)}) collective-permute-start(bf16[256,2048]{1,0:T(8,128)(2,1)} %collective-permute-done.6.rest_2_), channel_id=1, source_target_pairs={{0,1},{1,0},{2,3},{3,2},{4,5},{5,4},{6,7},{7,6},{8,9},{9,8},{10,11... | collective-permute-start | bytes 3145736 | tf_op jit(solution)/shard_map/ppermute | solution.py:489
  67.8 6.4 %collective-permute-start.11 = (bf16[256,2048]{1,0:T(8,128)(2,1)}, bf16[256,2048]{1,0:T(8,128)(2,1)}, u32[]{:S(2)}, u32[]{:S(2)}) collective-permute-start(bf16[256,2048]{1,0:T(8,128)(2,1)} %collective-permute-done.7.rest_3_), channel_id=1, source_target_pairs={{0,1},{1,0},{2,3},{3,2},{4,5},{5,4},{6,7},{7,6},{8,9},{9,8},{10,11... | collective-permute-start | bytes 3145736 | tf_op jit(solution)/shard_map/ppermute | solution.py:489
  67.9 20.6 %all-to-all-start.1 = ((bf16[8,512,128]{2,1,0:T(8,128)(2,1)}), bf16[8,512,128]{2,1,0:T(8,128)(2,1)S(1)}, u32[]{:S(2)}, u32[]{:S(2)}) async-start(bf16[8,512,128]{2,1,0:T(8,128)(2,1)} %get-tuple-element.39), calls=%async_computation.1 | async-start | bytes 2097152 | tf_op jit(solution)/shard_map/all_to_all | solution.py:530
